TPU v7x, 32 devices: a whole 2x2x4 slice. The times are simulated.
32 devices in a mesh: sp: 4 (over z), fs: 4 (over y, x), tp: 2 (over core).
Axes of the slice: x: 2, y: 2, z: 4, core: 2. Of those that a mesh axis runs over, the one named last changes fastest.
Arguments:
- tokens: bfloat16 [4, 1024, 2048], P('fs', 'sp', 'tp'), may hold values from -6 to 6
- norm_gain: float32 [2048], replicated, may hold values from 0.1 to 1.9
- query_weight: bfloat16 [2048, 1024], P(('sp', 'fs'), 'tp'), may hold values from -0.125 to 0.125
- forget_weight: bfloat16 [2048, 1024], P(('sp', 'fs'), 'tp'), may hold values from -0.125 to 0.125
- value_weight: bfloat16 [2048, 1024], P(('sp', 'fs'), 'tp'), may hold values from -0.125 to 0.125
- outgate_weight: bfloat16 [2048, 1024], P(('sp', 'fs'), 'tp'), may hold values from -0.125 to 0.125
- pool_in_weight: bfloat16 [2048, 1024], P(('sp', 'fs'), 'tp'), may hold values from -0.125 to 0.125
- forget_room: float32 [1024], P('tp'), may hold values from 0 to 0.06
- decay_shift: float32 [4, 1024, 8], P('fs', 'sp', 'tp'), may hold values from -0.6 to 0
- head_gain: float32 [128], replicated, may hold values from 0.1 to 1.9
- start_state: float32 [4, 8, 128, 128], P('fs', 'tp'), may hold values from -0.09375 to 0.09375
- pool_map: bfloat16 [4, 256, 256], P('tp'), may hold values from -0.375 to 0.375
- pool_scale: float32 [1024], P('tp'), may hold values from 0.1 to 1.9
- out_rec_weight: bfloat16 [1024, 2048], P('tp', ('sp', 'fs')), may hold values from -0.125 to 0.125
- out_pool_weight: bfloat16 [1024, 2048], P('tp', ('sp', 'fs')), may hold values from -0.125 to 0.125
Outputs:
- mixed: bfloat16 [4, 1024, 2048], P('fs', ('sp', 'tp'))
All inputs are finite; a program needn't handle non-finite values.
Results may differ from a plain program's by a relative error of at most 0.013.
Values may be sent and summed in bfloat16 or wider, within the bound.
No kernel may reach another device: no remote copies, remote signals or barrier semaphores. Data moves between devices by JAX's collectives and lax.ppermute only.
A program may use at most 128 MiB of HBM per device.

v0:
```python
import functools

import jax
import jax.numpy as jnp
from jax import lax
from jax.experimental import pallas as pl
from jax.experimental.pallas import tpu as pltpu
from jax.sharding import PartitionSpec as P


HEAD = 128
WIDEST = 16
BLOCK = 128
PAIR = 2
EPSILON = 1e-06
F32 = jnp.float32
BF16 = jnp.bfloat16


def dot(a, b, contract):
    return lax.dot_general(a, b, (contract, ((), ())), preferred_element_type=F32)


def swapped(value, axis, distance):
    count = lax.axis_size(axis)
    return lax.ppermute(value, axis, [(i, i ^ distance) for i in range(count)])


def passed_on(value, axis, steps, first=0, stride=1):
    count = lax.axis_size(axis)
    return lax.ppermute(value, axis, [(i, i + steps) for i in range(first, count - steps, stride)])


def call(kernel, outs, *args, scratch=(), outside=(), room=24):
    vmem = pl.BlockSpec(memory_space=pltpu.VMEM)
    anywhere = pl.BlockSpec(memory_space=pltpu.HBM)
    return pl.pallas_call(
        kernel,
        out_shape=[jax.ShapeDtypeStruct(shape, dtype) for shape, dtype in outs],
        in_specs=[anywhere if k in outside else vmem for k in range(len(args))],
        out_specs=[vmem] * len(outs),
        scratch_shapes=list(scratch),
        compiler_params=pltpu.CompilerParams(vmem_limit_bytes=room * 2**20),
    )(*args)


def along_line(same, other):
    return [same] + [swapped(other if d % PAIR else same, "sp", d) for d in range(1, lax.axis_size("sp"))]


def over_plane(arrived, groups, routes):
    pieces = []
    for group, route in zip(groups, routes):
        plane = arrived[group[0]] if len(group) == 1 else jnp.concatenate([arrived[d] for d in group], axis=0)
        by_x = swapped(plane, "fs", 1)
        by_y = swapped(plane, "fs", 2)
        if route == "x":
            across = swapped(by_y, "fs", 1)
        else:
            across = swapped(by_x, "fs", 2)
        for c, piece in enumerate((plane, by_x, by_y, across)):
            pieces.append((piece, c, tuple(group)))
    return pieces


def split(pieces):
    return [piece[0] for piece in pieces], tuple(piece[1:] for piece in pieces)


def assemble(refs, where, whole, rows, leading=0):
    sp, fs, n_fs = lax.axis_index("sp"), lax.axis_index("fs"), lax.axis_size("fs")
    for ref, (c, distances) in zip(refs, where):
        for k, d in enumerate(distances):
            block = (d // PAIR - leading) * PAIR * n_fs * rows
            spot = block + (((sp ^ d) % PAIR) * n_fs + (fs ^ c)) * rows
            whole[pl.ds(pl.multiple_of(spot, rows), rows), :] = ref[k * rows : (k + 1) * rows, :]


def projected_by(normed, whole, rows, leading):
    pair, wide = lax.axis_index("sp") // PAIR, PAIR * lax.axis_size("fs") * rows
    total = None
    for k in range(whole.shape[0] // wide):
        features = pl.ds(pl.multiple_of((pair ^ (k + leading)) * wide, wide), wide)
        part = dot(normed[:, features], whole[k * wide : (k + 1) * wide, :], ((1,), (0,)))
        total = part if total is None else total + part
    return total


def pack_kernel(*refs):
    sources, (same, other), sems = refs[:-3], refs[-3:-1], refs[-1]
    part = lax.axis_index("sp") % PAIR
    columns = sources[0].shape[1] // PAIR
    copies = []
    for j, (target, which) in enumerate(((same, part), (other, 1 - part))):
        for k, source in enumerate(sources):
            cut = source.at[:, pl.ds(pl.multiple_of(which * columns, columns), columns)]
            place = target.at[:, k * columns : (k + 1) * columns]
            copies.append(pltpu.make_async_copy(cut, place, sems.at[j, k]))
    for copy in copies:
        copy.start()
    for copy in copies:
        copy.wait()


def pack_rows_kernel(*refs):
    sources, (same, other), held, sems = refs[:-4], refs[-4:-2], refs[-2], refs[-1]
    part = lax.axis_index("sp") % PAIR
    rows = sources[0].shape[0] // PAIR
    copies = []
    for k, source in enumerate(sources):
        copies.append(pltpu.make_async_copy(source, held.at[k], sems.at[k]))
    for copy in copies:
        copy.start()
    for copy in copies:
        copy.wait()
    for target, which in ((same, part), (other, 1 - part)):
        for k in range(len(sources)):
            cut = held[k, pl.ds(pl.multiple_of(which * rows, rows), rows), :]
            target[:, k * rows : (k + 1) * rows] = cut.T


def norm_kernel(mine, mine_other, gain, own_out, other_out, tail_out):
    tp = lax.axis_index("tp")
    width = mine.shape[1]
    here = pl.ds(pl.multiple_of(tp * width, width), width)
    there = pl.ds(pl.multiple_of((1 - tp) * width, width), width)
    a, b = mine[...].astype(F32), mine_other[...].astype(F32)
    total = jnp.sum(a * a, axis=1, keepdims=True) + jnp.sum(b * b, axis=1, keepdims=True)
    scale = lax.rsqrt(total / (2 * width) + EPSILON)
    own = (a * scale * gain[:, here]).astype(BF16)
    own_out[...] = own
    tail_out[...] = own[own.shape[0] - WIDEST :, :]
    other_out[...] = (b * scale * gain[:, there]).astype(BF16)


def merge_kernel(adjacent, second, out):
    out[...] = adjacent[...] + second[...]


def cumulative(ones_below, value):
    high = value.astype(BF16)
    rest = value - high.astype(F32)
    middle = rest.astype(BF16)
    low = (rest - middle.astype(F32)).astype(BF16)
    contract = ((1,), (0,))
    return dot(ones_below, high, contract) + (dot(ones_below, middle, contract) + dot(ones_below, low, contract))


def first_kernel(*refs, where, rows):
    mine, mine_other, near, near_other, before, before_other = refs[:6]
    shards, (normed, sum_out, whole) = refs[6:-3], refs[-3:]
    part, tp = lax.axis_index("sp") % PAIR, lax.axis_index("tp")
    length, width = mine.shape
    here = pl.ds(pl.multiple_of(tp * width, width), width)
    there = pl.ds(pl.multiple_of((1 - tp) * width, width), width)
    for spot, left, right in ((part, mine, mine_other), (1 - part, near, near_other)):
        place = pl.ds(pl.multiple_of(spot * length, length), length)
        normed[place, here] = left[...]
        normed[place, there] = right[...]
    normed[PAIR * length :, here] = before[...]
    normed[PAIR * length :, there] = before_other[...]
    assemble(shards, where, whole, rows)
    sum_out[...] = projected_by(normed, whole, rows, 0)


def mix_kernel(*refs, where, rows):
    normed, earlier, room_whole, shift_mine, shift_near, start = refs[:6]
    shards = refs[6 : 6 + len(where)]
    projected_out, keyed_out, within_out, state_out, fade_out, leaving_out, opening_out, total_out, last_out, border_out = refs[
        6 + len(where) : 16 + len(where)
    ]
    whole, shift, first, sem = refs[16 + len(where) :]
    part = lax.axis_index("sp") % PAIR
    length, width = keyed_out.shape
    heads = width // HEAD
    fetch = pltpu.make_async_copy(start.at[pl.ds(part * heads, heads)], first, sem)
    fetch.start()
    lines, own = shift_mine.shape
    shift[...] = jnp.zeros_like(shift)
    shift[0:lines, pl.ds(pl.multiple_of(part * own, own), own)] = shift_mine[...]
    shift[0:lines, pl.ds(pl.multiple_of((1 - part) * own, own), own)] = shift_near[...]
    shifts = shift[...].T
    assemble(shards, where, whole, rows, 1)
    projected = (earlier[...] + projected_by(normed, whole, rows, 1)).astype(BF16)
    projected_out[...] = projected[0:length, :]
    border_out[...] = projected[length:, 4 * width :]
    room = room_whole[:, pl.ds(pl.multiple_of(part * width, width), width)]
    t = lax.broadcasted_iota(jnp.int32, (BLOCK, BLOCK), 0)
    s = lax.broadcasted_iota(jnp.int32, (BLOCK, BLOCK), 1)
    ones_below = (s <= t).astype(F32).astype(BF16)
    state = [jnp.zeros((HEAD, HEAD), F32) for _ in range(heads)]
    faded = [jnp.zeros((1, HEAD), F32) for _ in range(heads)]
    for n in range(length // BLOCK):
        span = slice(n * BLOCK, (n + 1) * BLOCK)
        logits = projected[span, 0:width].astype(F32)
        value = projected[span, 2 * width : 3 * width]
        keyed = room * (1.0 - jax.nn.sigmoid(logits))
        every = shifts[span, :]
        lags = [
            jnp.where(part == 0, every[:, h : h + 1], every[:, heads + h : heads + h + 1]) for h in range(heads)
        ]
        lag = jnp.concatenate([jnp.broadcast_to(column, (BLOCK, HEAD)) for column in lags], axis=1)
        within = cumulative(ones_below, jnp.log1p(-keyed) + lag)
        keyed_out[span, :] = keyed
        within_out[span, :] = within
        ending = within[BLOCK - 1 : BLOCK]
        late_k = (keyed * jnp.exp(ending - within)).astype(BF16)
        for h in range(heads):
            lanes = slice(h * HEAD, (h + 1) * HEAD)
            state_out[n, h] = state[h]
            fade_out[n, h : h + 1] = jnp.exp(faded[h])
            added = dot(value[:, lanes], late_k[:, lanes], ((0,), (0,)))
            state[h] = jnp.exp(ending[:, lanes]) * state[h] + added
            faded[h] = faded[h] + ending[:, lanes]
    fetch.wait()
    for h in range(heads):
        total = jnp.exp(faded[h])
        opening = first[h].T
        opening_out[h] = opening
        leaving_out[h] = (total * opening + state[h]).astype(BF16)
        last_out[h] = state[h]
        total_out[h] = total


def inside_kernel(projected, keyed, within_all, inside_out, reach_out):
    length, width = keyed.shape
    t = lax.broadcasted_iota(jnp.int32, (BLOCK, BLOCK), 0)
    s = lax.broadcasted_iota(jnp.int32, (BLOCK, BLOCK), 1)
    causal = s <= t
    for n in range(length // BLOCK):
        span = slice(n * BLOCK, (n + 1) * BLOCK)
        queries = jax.nn.silu(projected[span, width : 2 * width].astype(F32)) * HEAD ** (-0.5)
        value = projected[span, 2 * width : 3 * width]
        within = within_all[span, :]
        centre = within[BLOCK // 2 - 1 : BLOCK // 2]
        near_q = (queries * jnp.exp(within - centre)).astype(BF16)
        near_k = (keyed[span, :] * jnp.exp(centre - within)).astype(BF16)
        reach_out[span, :] = (queries * jnp.exp(within)).astype(BF16)
        for h in range(width // HEAD):
            lanes = slice(h * HEAD, (h + 1) * HEAD)
            scores = jnp.where(causal, dot(near_q[:, lanes], near_k[:, lanes], ((1,), (1,))), 0.0)
            inside_out[span, lanes] = dot(scores.astype(BF16), value[:, lanes], ((1,), (0,)))


def join_kernel(
    inside, reach, states, fades, opening, arrived, projected, head_gain, border, mappings, scales, joined, extended
):
    length, width = inside.shape
    heads = width // HEAD
    sp, tp = lax.axis_index("sp"), lax.axis_index("tp")
    part, pair = sp % PAIR, sp // PAIR
    for h in range(heads):
        lanes = slice(h * HEAD, (h + 1) * HEAD)
        entering = jnp.where(pair == 0, opening[h], arrived[h].astype(F32))
        for n in range(length // BLOCK):
            span = slice(n * BLOCK, (n + 1) * BLOCK)
            memory = states[n, h] + fades[n, h : h + 1] * entering
            raw = inside[span, lanes] + dot(reach[span, lanes], memory.astype(BF16), ((1,), (1,)))
            level = lax.rsqrt(jnp.mean(raw * raw, axis=1, keepdims=True) + EPSILON)
            gating = jax.nn.silu(projected[span, 3 * width + h * HEAD : 3 * width + (h + 1) * HEAD].astype(F32))
            joined[span, lanes] = (raw * level * head_gain[...] * gating).astype(BF16)
    extended[0:WIDEST, :] = border[...].astype(F32)
    extended[WIDEST:, :] = projected[:, 4 * width :].astype(F32)
    sums = extended[...]
    grouping = tp * PAIR + part
    chosen = jnp.zeros((length, width), F32)
    step = 1
    for level in range(4):
        sums = sums[step:, :] + sums[:-step, :]
        step *= 2
        chosen = jnp.where(grouping == level, sums[sums.shape[0] - length :, :], chosen)
    span_length = jnp.left_shift(jnp.int32(2), grouping)
    position = pair * length + lax.broadcasted_iota(jnp.int32, (length, 1), 0)
    amount = jnp.minimum(position + 1, span_length).astype(F32)
    pooled = (chosen / amount - extended[WIDEST:, :]).astype(BF16)
    mapped = dot(pooled, mappings[part], ((1,), (0,)))
    scale = scales[:, pl.ds(pl.multiple_of(part * width, width), width)]
    joined[:, width:] = (mapped * scale).astype(BF16)


def out_kernel(*refs, count, sort):
    joined = refs[0]
    shards = refs[1 : 1 + count]
    keep_out, far_out, send_out, whole = refs[1 + count :]
    part, tp = lax.axis_index("sp") % PAIR, lax.axis_index("tp")
    quarter = keep_out.shape[0]
    if sort is None:
        spot = 0
        for shard in shards:
            whole[spot : spot + shard.shape[0], :] = shard[...]
            spot += shard.shape[0]
    else:
        where, rows = sort
        sp, fs, n_fs = lax.axis_index("sp"), lax.axis_index("fs"), lax.axis_size("fs")
        for shard, (c, distances) in zip(shards, where):
            for k, d in enumerate(distances):
                spot = ((sp ^ d) * n_fs + (fs ^ c)) * rows
                whole[pl.ds(pl.multiple_of(spot, rows), rows), :] = shard[k * rows : (k + 1) * rows, :]

    def mixed(owner_part, owner_tp):
        spot = (owner_part * 2 + owner_tp) * quarter
        return dot(joined[pl.ds(pl.multiple_of(spot, quarter), quarter), :], whole[...], ((1,), (1,)))

    send_out[0:quarter, :] = mixed(part, 1 - tp).astype(BF16)
    send_out[quarter:, :] = mixed(1 - part, 1 - tp).astype(BF16)
    far_out[...] = mixed(1 - part, tp).astype(BF16)
    keep_out[...] = mixed(part, tp).astype(BF16)


def final_kernel(*refs, order, columns):
    out = refs[-1]
    sp, fs, n_fs = lax.axis_index("sp"), lax.axis_index("fs"), lax.axis_size("fs")
    quarter = out.shape[0]
    for k, places in enumerate(order):
        keep, met, back = refs[3 * k : 3 * k + 3]
        if places is None:
            out[...] = (keep[...].astype(F32) + met[0:quarter].astype(F32) + back[...].astype(F32)).astype(BF16)
            continue
        for j, (c, d) in enumerate(places):
            twin = places.index((c, d ^ 1))
            lanes = slice(j * columns, (j + 1) * columns)
            other = slice(twin * columns, (twin + 1) * columns)
            value = keep[:, lanes].astype(F32) + met[0:quarter, lanes].astype(F32) + back[:, other].astype(F32)
            spot = ((sp ^ d) * n_fs + (fs ^ c)) * columns
            out[:, pl.ds(pl.multiple_of(spot, columns), columns)] = value.astype(BF16)


def per_device(
    tokens,
    norm_gain,
    query_weight,
    forget_weight,
    value_weight,
    outgate_weight,
    pool_in_weight,
    forget_room,
    decay_shift,
    head_gain,
    start_state,
    pool_map,
    pool_scale,
    out_rec_weight,
    out_pool_weight,
):
    n_sp, n_fs = lax.axis_size("sp"), lax.axis_size("fs")
    pair = lax.axis_index("sp") // PAIR
    model = norm_gain.shape[0]
    rows = query_weight.shape[0]
    columns = query_weight.shape[1] // PAIR
    heads = columns // HEAD
    length = tokens.shape[1] * PAIR
    blocks = length // BLOCK
    mine = tokens[0]
    mine_other = swapped(mine, "tp", 1)
    pack_out = [((rows, 5 * columns), BF16)] * 2
    mix_same, mix_other = call(
        pack_kernel,
        pack_out,
        forget_weight,
        query_weight,
        value_weight,
        outgate_weight,
        pool_in_weight,
        scratch=[pltpu.SemaphoreType.DMA((2, 5))],
        outside=range(5),
        room=62,
    )
    line_a = along_line(mix_same, mix_other)
    pack_out = [((out_rec_weight.shape[1], 2 * columns), BF16)] * 2
    out_same, out_other = call(
        pack_rows_kernel,
        pack_out,
        out_rec_weight,
        out_pool_weight,
        scratch=[pltpu.VMEM((2,) + out_rec_weight.shape, BF16), pltpu.SemaphoreType.DMA((2,))],
        outside=range(2),
        room=62,
    )
    half = ((tokens.shape[1], tokens.shape[2]), BF16)
    tail = ((WIDEST, tokens.shape[2]), BF16)
    normed_own, normed_other, ends = call(norm_kernel, [half, half, tail], mine, mine_other, norm_gain[None])
    (before,) = call(merge_kernel, [tail], passed_on(ends, "sp", 1, 1, PAIR), passed_on(ends, "sp", 2, 1, PAIR))
    before_other = swapped(before, "tp", 1)
    near = swapped(normed_own, "sp", 1)
    shift_mine = decay_shift[0].T
    shift_near = swapped(shift_mine, "sp", 1)
    line_c = along_line(out_same, out_other)
    cut = (n_sp + 2) // 2
    fine = [[0], [1], list(range(2, cut)), list(range(cut, n_sp))]
    coarse = [[0], [1], list(range(2, n_sp))]
    mix_pieces = over_plane(line_a, fine, "xyyx")
    first_shards, first_where = split([p for p in mix_pieces if p[2][0] < PAIR])
    mix_shards, mix_where = split([p for p in mix_pieces if p[2][0] >= PAIR])
    out_pieces = over_plane(line_c, coarse, "yyx")
    near_other = swapped(near, "tp", 1)
    wide = PAIR * n_fs * rows
    normed, earlier = call(
        functools.partial(first_kernel, where=first_where, rows=rows),
        [((length + WIDEST, model), BF16), ((length + WIDEST, 5 * columns), F32)],
        normed_own,
        normed_other,
        near,
        near_other,
        before,
        before_other,
        *first_shards,
        scratch=[pltpu.VMEM((wide, 5 * columns), BF16)],
    )
    projected, keyed, within, states, fades, leaving, opening, total, last, border = call(
        functools.partial(mix_kernel, where=mix_where, rows=rows),
        [
            ((length, 5 * columns), BF16),
            ((length, columns), F32),
            ((length, columns), F32),
            ((blocks, heads, HEAD, HEAD), F32),
            ((blocks, heads, HEAD), F32),
            ((heads, HEAD, HEAD), BF16),
            ((heads, HEAD, HEAD), F32),
            ((heads, 1, HEAD), F32),
            ((heads, HEAD, HEAD), F32),
            ((WIDEST, columns), BF16),
        ],
        normed,
        earlier,
        forget_room[None],
        shift_mine,
        shift_near,
        start_state[0],
        *mix_shards,
        scratch=[
            pltpu.VMEM((model - wide, 5 * columns), BF16),
            pltpu.VMEM((8, length), F32),
            pltpu.VMEM((heads, HEAD, HEAD), F32),
            pltpu.SemaphoreType.DMA(()),
        ],
        outside=(5,),
        room=30,
    )
    arrived = passed_on(leaving, "sp", PAIR)

    def handoff(turn, arrived):
        onward = (total * arrived.astype(F32) + last).astype(BF16)
        onward = jnp.where(pair == 0, leaving, onward)
        return passed_on(onward, "sp", PAIR)

    if n_sp // PAIR > 2:
        arrived = lax.fori_loop(0, n_sp // PAIR - 2, handoff, arrived)
    inside, reach = call(inside_kernel, [((length, columns), F32), ((length, columns), BF16)], projected, keyed, within)
    (joined,) = call(
        join_kernel,
        [((length, 2 * columns), BF16)],
        inside,
        reach,
        states,
        fades,
        opening,
        arrived,
        projected,
        head_gain[None],
        border,
        pool_map,
        pool_scale[None],
        scratch=[pltpu.VMEM((WIDEST + length, columns), F32)],
    )
    quarter = length // (PAIR * 2)
    out_rows = out_rec_weight.shape[1]
    if out_rows % 128:
        sets = [out_pieces]
    else:
        sets = [[p for p in out_pieces if p[1] in near_by] for near_by in ((0, 1, 2), (3,))]
    shares, order = [], []
    for pieces in sets:
        shards, where = split(pieces)
        sort = (where, out_rows) if out_rows % 128 else None
        wide = sum(shard.shape[0] for shard in shards)
        keep, far, send = call(
            functools.partial(out_kernel, count=len(shards), sort=sort),
            [((quarter, wide), BF16), ((quarter, wide), BF16), ((2 * quarter, wide), BF16)],
            joined,
            *shards,
            scratch=[pltpu.VMEM((wide, 2 * columns), BF16)],
        )
        met = swapped(send, "tp", 1)
        owed = (far.astype(F32) + met[quarter:].astype(F32)).astype(BF16)
        shares += [keep, met, swapped(owed, "sp", 1)]
        order.append(None if sort else tuple((c, d) for c, group in where for d in group))
    (mixed,) = call(
        functools.partial(final_kernel, order=tuple(order), columns=out_rows), [((quarter, model), BF16)], *shares
    )
    return mixed[None]


def solution(mesh):
    return jax.shard_map(
        per_device,
        mesh=mesh,
        in_specs=(
            P("fs", "sp", "tp"),
            P(),
            P(("sp", "fs"), "tp"),
            P(("sp", "fs"), "tp"),
            P(("sp", "fs"), "tp"),
            P(("sp", "fs"), "tp"),
            P(("sp", "fs"), "tp"),
            P("tp"),
            P("fs", "sp", "tp"),
            P(),
            P("fs", "tp", None, None),
            P("tp", None, None),
            P("tp"),
            P("tp", ("sp", "fs")),
            P("tp", ("sp", "fs")),
        ),
        out_specs=P("fs", ("sp", "tp"), None),
        check_vma=False,
    )
```

profile of v0, /device:TPU:0, one launch (start us, length us, event | category | flops | bytes accessed | tf_op | source)
XLA Modules:
  0.0 147.3 jit_solution(9020231339045786233)
XLA Ops:
  0.5 1.8 %shard_map.152 = (bf16[128,512]{1,0:T(8,128)(2,1)}, bf16[128,512]{1,0:T(8,128)(2,1)}) custom-call(bf16[512,128]{1,0:T(8,128)(2,1)} %refs_0_.3, bf16[512,128]{1,0:T(8,128)(2,1)} %refs_1_.3), custom_call_target="tpu_custom_call" | custom-call | tf_op jit(solution)/shard_map/pallas_call | solution.py:37
  2.3 3.6 %collective-permute-start.28 = (bf16[128,512]{1,0:T(8,128)(2,1)}, bf16[128,512]{1,0:T(8,128)(2,1)S(1)}, u32[]{:S(2)}, u32[]{:S(2)}) collective-permute-start(bf16[128,512]{1,0:T(8,128)(2,1)} %get-tuple-element.47.refs_1_), channel_id=1, source_target_pairs={{0,16},{8,24},{16,0},{24,8},{1,17},{9,25},{17,1},{25,9},{2,18},{10... | collective-permute-start | bytes 393224 | tf_op jit(solution)/shard_map/ppermute | solution.py:26
  5.9 2.0 %shard_map.147 = (bf16[128,1280]{1,0:T(8,128)(2,1)}, bf16[128,1280]{1,0:T(8,128)(2,1)}) custom-call(bf16[128,512]{1,0:T(8,128)(2,1)} %refs_0_.2, bf16[128,512]{1,0:T(8,128)(2,1)} %refs_1_.2, bf16[128,512]{1,0:T(8,128)(2,1)} %refs_2_.1, bf16[128,512]{1,0:T(8,128)(2,1)} %refs_3_.1, bf16[128,512]{1,0:T(8,128)(2,1)} %refs_4_.1), custom_call_target="tpu_custom_call" | custom-call | tf_op jit(solution)/shard_map/pallas_call | solution.py:37
  8.0 1.6 %collective-permute-start.9 = (bf16[128,1280]{1,0:T(8,128)(2,1)}, bf16[128,1280]{1,0:T(8,128)(2,1)S(1)}, u32[]{:S(2)}, u32[]{:S(2)}) collective-permute-start(bf16[128,1280]{1,0:T(8,128)(2,1)} %get-tuple-element.34), channel_id=1, source_target_pairs={{0,8},{8,0},{16,24},{24,16},{1,9},{9,1},{17,25},{25,17},{2,10},{10... | collective-permute-start | bytes 983048 | tf_op jit(solution)/shard_map/ppermute | solution.py:26
  10.1 1.5 %collective-permute-start.7 = (bf16[128,1280]{1,0:T(8,128)(2,1)}, bf16[128,1280]{1,0:T(8,128)(2,1)S(1)}, u32[]{:S(2)}, u32[]{:S(2)}) collective-permute-start(bf16[128,1280]{1,0:T(8,128)(2,1)} %get-tuple-element.33.refs_6_), channel_id=1, source_target_pairs={{0,4},{2,6},{4,0},{6,2},{1,5},{3,7},{5,1},{7,3},{8,12},{10,14},{12... | collective-permute-start | bytes 983048 | tf_op jit(solution)/shard_map/ppermute | solution.py:26
  11.6 8.2 %collective-permute-done.13.refs_4_ = f32[4,256]{1,0:T(4,128)S(1)} collective-permute-done((f32[4,256]{1,0:T(4,128)}, f32[4,256]{1,0:T(4,128)S(1)}, u32[]{:S(2)}, u32[]{:S(2)}) %collective-permute-start.13) | collective-permute-done | bytes 4128 | tf_op jit(solution)/shard_map/ppermute | solution.py:26
  19.8 1.5 %collective-permute-start.6 = (bf16[128,1280]{1,0:T(8,128)(2,1)}, bf16[128,1280]{1,0:T(8,128)(2,1)S(1)}, u32[]{:S(2)}, u32[]{:S(2)}) collective-permute-start(bf16[128,1280]{1,0:T(8,128)(2,1)} %get-tuple-element.33.refs_6_), channel_id=1, source_target_pairs={{0,2},{2,0},{4,6},{6,4},{1,3},{3,1},{5,7},{7,5},{8,10},{10,8},{12,... | collective-permute-start | bytes 983048 | tf_op jit(solution)/shard_map/ppermute | solution.py:26
  21.4 2.4 %collective-permute-start.29 = (bf16[128,512]{1,0:T(8,128)(2,1)}, bf16[128,512]{1,0:T(8,128)(2,1)S(1)}, u32[]{:S(2)}, u32[]{:S(2)}) collective-permute-start(bf16[128,512]{1,0:T(8,128)(2,1)} %get-tuple-element.48), channel_id=1, source_target_pairs={{0,24},{8,16},{16,8},{24,0},{1,25},{9,17},{17,9},{25,1},{2,26},{10... | collective-permute-start | bytes 393224 | tf_op jit(solution)/shard_map/ppermute | solution.py:26
  23.7 4.6 %collective-permute-done.29 = bf16[128,512]{1,0:T(8,128)(2,1)S(1)} collective-permute-done((bf16[128,512]{1,0:T(8,128)(2,1)}, bf16[128,512]{1,0:T(8,128)(2,1)S(1)}, u32[]{:S(2)}, u32[]{:S(2)}) %collective-permute-start.29) | collective-permute-done | bytes 131104 | tf_op jit(solution)/shard_map/ppermute | solution.py:26
  28.4 1.5 %collective-permute-start.14 = (bf16[128,1280]{1,0:T(8,128)(2,1)}, bf16[128,1280]{1,0:T(8,128)(2,1)S(1)}, u32[]{:S(2)}, u32[]{:S(2)}) collective-permute-start(bf16[128,1280]{1,0:T(8,128)(2,1)} %get-tuple-element.33.refs_6_), channel_id=1, source_target_pairs={{0,16},{8,24},{16,0},{24,8},{1,17},{9,25},{17,1},{25,9},{2,18},{10... | collective-permute-start | bytes 983048 | tf_op jit(solution)/shard_map/ppermute | solution.py:26
  29.9 1.7 %collective-permute-start.18 = (bf16[128,1280]{1,0:T(8,128)(2,1)}, bf16[128,1280]{1,0:T(8,128)(2,1)S(1)}, u32[]{:S(2)}, u32[]{:S(2)}) collective-permute-start(bf16[128,1280]{1,0:T(8,128)(2,1)} %get-tuple-element.34), channel_id=1, source_target_pairs={{0,24},{8,16},{16,8},{24,0},{1,25},{9,17},{17,9},{25,1},{2,26},{10... | collective-permute-start | bytes 983048 | tf_op jit(solution)/shard_map/ppermute | solution.py:26
  36.0 1.6 %collective-permute-start.8 = (bf16[128,1280]{1,0:T(8,128)(2,1)S(1)}, bf16[128,1280]{1,0:T(8,128)(2,1)S(1)}, u32[]{:S(2)}, u32[]{:S(2)}) collective-permute-start(bf16[128,1280]{1,0:T(8,128)(2,1)S(1)} %collective-permute-done.7.refs_8_), channel_id=1, source_target_pairs={{0,2},{2,0},{4,6},{6,4},{1,3},{3,1},{5,7},{7,5},{8,10},{10,8},{12,... | collective-permute-start | bytes 983048 | tf_op jit(solution)/shard_map/ppermute | solution.py:26
  37.6 13.4 %collective-permute-done.14.refs_6_ = bf16[128,1280]{1,0:T(8,128)(2,1)S(1)} collective-permute-done((bf16[128,1280]{1,0:T(8,128)(2,1)}, bf16[128,1280]{1,0:T(8,128)(2,1)S(1)}, u32[]{:S(2)}, u32[]{:S(2)}) %collective-permute-start.14) | collective-permute-done | bytes 327712 | tf_op jit(solution)/shard_map/ppermute | solution.py:26
  51.0 1.5 %collective-permute-start.11 = (bf16[128,1280]{1,0:T(8,128)(2,1)S(1)}, bf16[128,1280]{1,0:T(8,128)(2,1)S(1)}, u32[]{:S(2)}, u32[]{:S(2)}) collective-permute-start(bf16[128,1280]{1,0:T(8,128)(2,1)S(1)} %collective-permute-done.9.refs_10_), channel_id=1, source_target_pairs={{0,4},{2,6},{4,0},{6,2},{1,5},{3,7},{5,1},{7,3},{8,12},{10,14},{12... | collective-permute-start | bytes 983048 | tf_op jit(solution)/shard_map/ppermute | solution.py:26
  55.1 3.3 %collective-permute-done.1.refs_2_ = bf16[256,1024]{1,0:T(8,128)(2,1)S(1)} collective-permute-done((bf16[256,1024]{1,0:T(8,128)(2,1)S(1)}, bf16[256,1024]{1,0:T(8,128)(2,1)S(1)}, u32[]{:S(2)}, u32[]{:S(2)}) %collective-permute-start.1) | collective-permute-done | bytes 524320 | tf_op jit(solution)/shard_map/ppermute | solution.py:26
  58.5 3.1 %collective-permute-done.11.refs_12_ = bf16[128,1280]{1,0:T(8,128)(2,1)S(1)} collective-permute-done((bf16[128,1280]{1,0:T(8,128)(2,1)S(1)}, bf16[128,1280]{1,0:T(8,128)(2,1)S(1)}, u32[]{:S(2)}, u32[]{:S(2)}) %collective-permute-start.11) | collective-permute-done | bytes 327712 | tf_op jit(solution)/shard_map/ppermute | solution.py:26
  63.7 5.0 %collective-permute-done.16.refs_8_ = bf16[128,1280]{1,0:T(8,128)(2,1)S(1)} collective-permute-done((bf16[128,1280]{1,0:T(8,128)(2,1)S(1)}, bf16[128,1280]{1,0:T(8,128)(2,1)S(1)}, u32[]{:S(2)}, u32[]{:S(2)}) %collective-permute-start.16) | collective-permute-done | bytes 327712 | tf_op jit(solution)/shard_map/ppermute | solution.py:26
  68.6 1.5 %collective-permute-start.17 = (bf16[128,1280]{1,0:T(8,128)(2,1)S(1)}, bf16[128,1280]{1,0:T(8,128)(2,1)S(1)}, u32[]{:S(2)}, u32[]{:S(2)}) collective-permute-start(bf16[128,1280]{1,0:T(8,128)(2,1)S(1)} %collective-permute-done.15.refs_7_), channel_id=1, source_target_pairs={{0,4},{2,6},{4,0},{6,2},{1,5},{3,7},{5,1},{7,3},{8,12},{10,14},{12... | collective-permute-start | bytes 983048 | tf_op jit(solution)/shard_map/ppermute | solution.py:26
  70.2 5.5 %collective-permute-done.20.refs_12_ = bf16[128,1280]{1,0:T(8,128)(2,1)S(1)} collective-permute-done((bf16[128,1280]{1,0:T(8,128)(2,1)S(1)}, bf16[128,1280]{1,0:T(8,128)(2,1)S(1)}, u32[]{:S(2)}, u32[]{:S(2)}) %collective-permute-start.20) | collective-permute-done | bytes 327712 | tf_op jit(solution)/shard_map/ppermute | solution.py:26
  76.2 11.2 %collective-permute-start.25 = (bf16[128,512]{1,0:T(8,128)(2,1)}, bf16[128,512]{1,0:T(8,128)(2,1)S(1)}, u32[]{:S(2)}, u32[]{:S(2)}) collective-permute-start(bf16[128,512]{1,0:T(8,128)(2,1)} %get-tuple-element.48), channel_id=1, source_target_pairs={{0,8},{8,0},{16,24},{24,16},{1,9},{9,1},{17,25},{25,17},{2,10},{10... | collective-permute-start | bytes 393224 | tf_op jit(solution)/shard_map/ppermute | solution.py:26
  89.2 1.5 %collective-permute-start.31 = (bf16[256,512]{1,0:T(8,128)(2,1)S(1)}, bf16[256,512]{1,0:T(8,128)(2,1)S(1)}, u32[]{:S(2)}, u32[]{:S(2)}) collective-permute-start(bf16[256,512]{1,0:T(8,128)(2,1)S(1)} %constant_dynamic-update-slice_fusion.refs_7_), channel_id=1, source_target_pairs={{0,4},{2,6},{4,0},{6,2},{1,5},{3,7},{5,1},{7,3},{8,12},{10,14},{12... | collective-permute-start | bytes 786440 | tf_op jit(solution)/shard_map/ppermute | solution.py:26
  92.3 1.9 %shard_map.148 = (bf16[528,2048]{1,0:T(8,128)(2,1)S(1)}, f32[528,1280]{1,0:T(8,128)S(1)}) custom-call(bf16[256,1024]{1,0:T(8,128)(2,1)S(1)} %get-tuple-element.30.refs_0_, bf16[256,1024]{1,0:T(8,128)(2,1)S(1)} %get-tuple-element.31.refs_1_, bf16[256,1024]{1,0:T(8,128)(2,1)S(1)} %collective-permute-done.1.refs_2_, ...), custom_call_target="tpu_custom_call" | custom-call | tf_op jit(solution)/shard_map/pallas_call | solution.py:37
  94.2 3.5 %shard_map.149 = (bf16[512,1280]{1,0:T(8,128)(2,1)S(1)}, f32[512,256]{1,0:T(8,128)S(1)}, f32[512,256]{1,0:T(8,128)S(1)}, f32[4,2,128,128]{3,2,1,0:T(8,128)S(1)},...) custom-call(bf16[528,2048]{1,0:T(8,128)(2,1)S(1)} %get-tuple-element, ...), custom_call_target="tpu_custom_call" | custom-call | tf_op jit(solution)/shard_map/pallas_call | solution.py:37
  97.7 12.8 %collective-permute-start.22 = (bf16[2,128,128]{2,1,0:T(8,128)(2,1)S(1)}, bf16[2,128,128]{2,1,0:T(8,128)(2,1)S(1)}, u32[]{:S(2)}, u32[]{:S(2)}) collective-permute-start(bf16[2,128,128]{2,1,0:T(8,128)(2,1)S(1)} %get-tuple-element.45), channel_id=1, source_target_pairs={{0,16},{8,24},{1,17},{9,25},{2,18},{10,26},{3,19},{11,27},{4,20},{... | collective-permute-start | bytes 196616 | tf_op jit(solution)/shard_map/ppermute | solution.py:31
  116.2 1.4 collective-permute-done.27.refs_6_
  117.6 2.1 %shard_map.153 = (bf16[128,1536]{1,0:T(8,128)(2,1)S(1)}, bf16[128,1536]{1,0:T(8,128)(2,1)S(1)}, bf16[256,1536]{1,0:T(8,128)(2,1)S(1)}) custom-call(bf16[512,512]{1,0:T(8,128)(2,1)S(1)} %shard_map.151.refs_0_, bf16[128,512]{1,0:T(8,128)(2,1)S(1)} %copy-done.4, bf16[128,512]{1,0:T(8,128)(2,1)S(1)} %collective-permute-done.23.refs_2_, ...), custom_call_target="tpu_custom_call" | custom-call | tf_op jit(solution)/shard_map/pallas_call | solution.py:37
  120.5 1.5 %collective-permute-start.34 = (bf16[128,512]{1,0:T(8,128)(2,1)S(1)}, bf16[128,512]{1,0:T(8,128)(2,1)S(1)}, u32[]{:S(2)}, u32[]{:S(2)}) collective-permute-start(bf16[128,512]{1,0:T(8,128)(2,1)S(1)} %collective-permute-done.23.refs_2_), channel_id=1, source_target_pairs={{0,4},{2,6},{4,0},{6,2},{1,5},{3,7},{5,1},{7,3},{8,12},{10,14},{12... | collective-permute-start | bytes 393224 | tf_op jit(solution)/shard_map/ppermute | solution.py:26
  122.5 4.3 %collective-permute-done.34.refs_1_ = bf16[128,512]{1,0:T(8,128)(2,1)S(1)} collective-permute-done((bf16[128,512]{1,0:T(8,128)(2,1)S(1)}, bf16[128,512]{1,0:T(8,128)(2,1)S(1)}, u32[]{:S(2)}, u32[]{:S(2)}) %collective-permute-start.34) | collective-permute-done | bytes 131104 | tf_op jit(solution)/shard_map/ppermute | solution.py:26
  126.9 2.0 %collective-permute-done.35.refs_2_ = bf16[128,512]{1,0:T(8,128)(2,1)S(1)} collective-permute-done((bf16[128,512]{1,0:T(8,128)(2,1)S(1)}, bf16[128,512]{1,0:T(8,128)(2,1)S(1)}, u32[]{:S(2)}, u32[]{:S(2)}) %collective-permute-start.35) | collective-permute-done | bytes 131104 | tf_op jit(solution)/shard_map/ppermute | solution.py:26
  129.9 3.9 %collective-permute-start.33 = (bf16[128,1536]{1,0:T(8,128)(2,1)S(1)}, bf16[128,1536]{1,0:T(8,128)(2,1)S(1)}, u32[]{:S(2)}, u32[]{:S(2)}) collective-permute-start(bf16[128,1536]{1,0:T(8,128)(2,1)S(1)} %add_convert_fusion), channel_id=1, source_target_pairs={{0,8},{8,0},{16,24},{24,16},{1,9},{9,1},{17,25},{25,17},{2,10},{10... | collective-permute-start | bytes 1179656 | tf_op jit(solution)/shard_map/ppermute | solution.py:26
  133.8 1.4 collective-permute-start.38
  135.2 11.1 %collective-permute-done.38.refs_5_ = bf16[128,512]{1,0:T(8,128)(2,1)S(1)} collective-permute-done((bf16[128,512]{1,0:T(8,128)(2,1)S(1)}, bf16[128,512]{1,0:T(8,128)(2,1)S(1)}, u32[]{:S(2)}, u32[]{:S(2)}) %collective-permute-start.38) | collective-permute-done | bytes 131104 | tf_op jit(solution)/shard_map/ppermute | solution.py:26
  (81 shorter events, 22.7 us)
Async XLA Ops:
  0.0 29.9 %collective-permute-start = (bf16[256,1024]{1,0:T(8,128)(2,1)}, bf16[256,1024]{1,0:T(8,128)(2,1)S(1)}, u32[]{:S(2)}, u32[]{:S(2)}) collective-permute-start(bf16[256,1024]{1,0:T(8,128)(2,1)} %bitcast.10), channel_id=1, source_target_pairs={{0,1},{1,0},{2,3},{3,2},{4,5},{5,4},{6,7},{7,6},{8,9},{9,8},{10,11... | collective-permute-start | bytes 1572872 | tf_op jit(solution)/shard_map/ppermute | solution.py:26
  2.3 19.1 %collective-permute-start.28 = (bf16[128,512]{1,0:T(8,128)(2,1)}, bf16[128,512]{1,0:T(8,128)(2,1)S(1)}, u32[]{:S(2)}, u32[]{:S(2)}) collective-permute-start(bf16[128,512]{1,0:T(8,128)(2,1)} %get-tuple-element.47.refs_1_), channel_id=1, source_target_pairs={{0,16},{8,24},{16,0},{24,8},{1,17},{9,25},{17,1},{25,9},{2,18},{10... | collective-permute-start | bytes 393224 | tf_op jit(solution)/shard_map/ppermute | solution.py:26
  8.0 25.8 %collective-permute-start.9 = (bf16[128,1280]{1,0:T(8,128)(2,1)}, bf16[128,1280]{1,0:T(8,128)(2,1)S(1)}, u32[]{:S(2)}, u32[]{:S(2)}) collective-permute-start(bf16[128,1280]{1,0:T(8,128)(2,1)} %get-tuple-element.34), channel_id=1, source_target_pairs={{0,8},{8,0},{16,24},{24,16},{1,9},{9,1},{17,25},{25,17},{2,10},{10... | collective-permute-start | bytes 983048 | tf_op jit(solution)/shard_map/ppermute | solution.py:26
  9.6 10.2 %collective-permute-start.13 = (f32[4,256]{1,0:T(4,128)}, f32[4,256]{1,0:T(4,128)S(1)}, u32[]{:S(2)}, u32[]{:S(2)}) collective-permute-start(f32[4,256]{1,0:T(4,128)} %bitcast.14), channel_id=1, source_target_pairs={{0,8},{8,0},{16,24},{24,16},{1,9},{9,1},{17,25},{25,17},{2,10},{10... | collective-permute-start | bytes 12296 | tf_op jit(solution)/shard_map/ppermute | solution.py:26
  10.1 24.0 %collective-permute-start.7 = (bf16[128,1280]{1,0:T(8,128)(2,1)}, bf16[128,1280]{1,0:T(8,128)(2,1)S(1)}, u32[]{:S(2)}, u32[]{:S(2)}) collective-permute-start(bf16[128,1280]{1,0:T(8,128)(2,1)} %get-tuple-element.33.refs_6_), channel_id=1, source_target_pairs={{0,4},{2,6},{4,0},{6,2},{1,5},{3,7},{5,1},{7,3},{8,12},{10,14},{12... | collective-permute-start | bytes 983048 | tf_op jit(solution)/shard_map/ppermute | solution.py:26
  19.8 14.9 %collective-permute-start.6 = (bf16[128,1280]{1,0:T(8,128)(2,1)}, bf16[128,1280]{1,0:T(8,128)(2,1)S(1)}, u32[]{:S(2)}, u32[]{:S(2)}) collective-permute-start(bf16[128,1280]{1,0:T(8,128)(2,1)} %get-tuple-element.33.refs_6_), channel_id=1, source_target_pairs={{0,2},{2,0},{4,6},{6,4},{1,3},{3,1},{5,7},{7,5},{8,10},{10,8},{12,... | collective-permute-start | bytes 983048 | tf_op jit(solution)/shard_map/ppermute | solution.py:26
  21.4 7.0 %collective-permute-start.29 = (bf16[128,512]{1,0:T(8,128)(2,1)}, bf16[128,512]{1,0:T(8,128)(2,1)S(1)}, u32[]{:S(2)}, u32[]{:S(2)}) collective-permute-start(bf16[128,512]{1,0:T(8,128)(2,1)} %get-tuple-element.48), channel_id=1, source_target_pairs={{0,24},{8,16},{16,8},{24,0},{1,25},{9,17},{17,9},{25,1},{2,26},{10... | collective-permute-start | bytes 393224 | tf_op jit(solution)/shard_map/ppermute | solution.py:26
  28.4 22.7 %collective-permute-start.14 = (bf16[128,1280]{1,0:T(8,128)(2,1)}, bf16[128,1280]{1,0:T(8,128)(2,1)S(1)}, u32[]{:S(2)}, u32[]{:S(2)}) collective-permute-start(bf16[128,1280]{1,0:T(8,128)(2,1)} %get-tuple-element.33.refs_6_), channel_id=1, source_target_pairs={{0,16},{8,24},{16,0},{24,8},{1,17},{9,25},{17,1},{25,9},{2,18},{10... | collective-permute-start | bytes 983048 | tf_op jit(solution)/shard_map/ppermute | solution.py:26
  29.9 21.2 %collective-permute-start.18 = (bf16[128,1280]{1,0:T(8,128)(2,1)}, bf16[128,1280]{1,0:T(8,128)(2,1)S(1)}, u32[]{:S(2)}, u32[]{:S(2)}) collective-permute-start(bf16[128,1280]{1,0:T(8,128)(2,1)} %get-tuple-element.34), channel_id=1, source_target_pairs={{0,24},{8,16},{16,8},{24,0},{1,25},{9,17},{17,9},{25,1},{2,26},{10... | collective-permute-start | bytes 983048 | tf_op jit(solution)/shard_map/ppermute | solution.py:26
  33.8 24.7 %collective-permute-start.1 = (bf16[256,1024]{1,0:T(8,128)(2,1)S(1)}, bf16[256,1024]{1,0:T(8,128)(2,1)S(1)}, u32[]{:S(2)}, u32[]{:S(2)}) collective-permute-start(bf16[256,1024]{1,0:T(8,128)(2,1)S(1)} %get-tuple-element.30.refs_0_), channel_id=1, source_target_pairs={{0,8},{8,0},{16,24},{24,16},{1,9},{9,1},{17,25},{25,17},{2,10},{10... | collective-permute-start | bytes 1572872 | tf_op jit(solution)/shard_map/ppermute | solution.py:26
  34.7 18.4 %collective-permute-start.10 = (bf16[128,1280]{1,0:T(8,128)(2,1)S(1)}, bf16[128,1280]{1,0:T(8,128)(2,1)S(1)}, u32[]{:S(2)}, u32[]{:S(2)}) collective-permute-start(bf16[128,1280]{1,0:T(8,128)(2,1)S(1)} %collective-permute-done.9.refs_10_), channel_id=1, source_target_pairs={{0,2},{2,0},{4,6},{6,4},{1,3},{3,1},{5,7},{7,5},{8,10},{10,8},{12,... | collective-permute-start | bytes 983048 | tf_op jit(solution)/shard_map/ppermute | solution.py:26
  36.0 18.3 %collective-permute-start.8 = (bf16[128,1280]{1,0:T(8,128)(2,1)S(1)}, bf16[128,1280]{1,0:T(8,128)(2,1)S(1)}, u32[]{:S(2)}, u32[]{:S(2)}) collective-permute-start(bf16[128,1280]{1,0:T(8,128)(2,1)S(1)} %collective-permute-done.7.refs_8_), channel_id=1, source_target_pairs={{0,2},{2,0},{4,6},{6,4},{1,3},{3,1},{5,7},{7,5},{8,10},{10,8},{12,... | collective-permute-start | bytes 983048 | tf_op jit(solution)/shard_map/ppermute | solution.py:26
  51.0 10.6 %collective-permute-start.11 = (bf16[128,1280]{1,0:T(8,128)(2,1)S(1)}, bf16[128,1280]{1,0:T(8,128)(2,1)S(1)}, u32[]{:S(2)}, u32[]{:S(2)}) collective-permute-start(bf16[128,1280]{1,0:T(8,128)(2,1)S(1)} %collective-permute-done.9.refs_10_), channel_id=1, source_target_pairs={{0,4},{2,6},{4,0},{6,2},{1,5},{3,7},{5,1},{7,3},{8,12},{10,14},{12... | collective-permute-start | bytes 983048 | tf_op jit(solution)/shard_map/ppermute | solution.py:26
  52.6 9.8 %collective-permute-start.15 = (bf16[128,1280]{1,0:T(8,128)(2,1)S(1)}, bf16[128,1280]{1,0:T(8,128)(2,1)S(1)}, u32[]{:S(2)}, u32[]{:S(2)}) collective-permute-start(bf16[128,1280]{1,0:T(8,128)(2,1)S(1)} %collective-permute-done.14.refs_6_), channel_id=1, source_target_pairs={{0,2},{2,0},{4,6},{6,4},{1,3},{3,1},{5,7},{7,5},{8,10},{10,8},{12,... | collective-permute-start | bytes 983048 | tf_op jit(solution)/shard_map/ppermute | solution.py:26
  53.1 15.5 %collective-permute-start.16 = (bf16[128,1280]{1,0:T(8,128)(2,1)S(1)}, bf16[128,1280]{1,0:T(8,128)(2,1)S(1)}, u32[]{:S(2)}, u32[]{:S(2)}) collective-permute-start(bf16[128,1280]{1,0:T(8,128)(2,1)S(1)} %collective-permute-done.14.refs_6_), channel_id=1, source_target_pairs={{0,4},{2,6},{4,0},{6,2},{1,5},{3,7},{5,1},{7,3},{8,12},{10,14},{12... | collective-permute-start | bytes 983048 | tf_op jit(solution)/shard_map/ppermute | solution.py:26
  54.3 21.4 %collective-permute-start.20 = (bf16[128,1280]{1,0:T(8,128)(2,1)S(1)}, bf16[128,1280]{1,0:T(8,128)(2,1)S(1)}, u32[]{:S(2)}, u32[]{:S(2)}) collective-permute-start(bf16[128,1280]{1,0:T(8,128)(2,1)S(1)} %collective-permute-done.18.refs_10_), channel_id=1, source_target_pairs={{0,4},{2,6},{4,0},{6,2},{1,5},{3,7},{5,1},{7,3},{8,12},{10,14},{12... | collective-permute-start | bytes 983048 | tf_op jit(solution)/shard_map/ppermute | solution.py:26
  58.5 32.3 %collective-permute-start.2 = (bf16[256,1024]{1,0:T(8,128)(2,1)S(1)}, bf16[256,1024]{1,0:T(8,128)(2,1)S(1)}, u32[]{:S(2)}, u32[]{:S(2)}) collective-permute-start(bf16[256,1024]{1,0:T(8,128)(2,1)S(1)} %collective-permute-done.1.refs_2_), channel_id=1, source_target_pairs={{0,1},{1,0},{2,3},{3,2},{4,5},{5,4},{6,7},{7,6},{8,9},{9,8},{10,11... | collective-permute-start | bytes 1572872 | tf_op jit(solution)/shard_map/ppermute | solution.py:26
  61.6 14.6 %collective-permute-start.19 = (bf16[128,1280]{1,0:T(8,128)(2,1)S(1)}, bf16[128,1280]{1,0:T(8,128)(2,1)S(1)}, u32[]{:S(2)}, u32[]{:S(2)}) collective-permute-start(bf16[128,1280]{1,0:T(8,128)(2,1)S(1)} %collective-permute-done.18.refs_10_), channel_id=1, source_target_pairs={{0,2},{2,0},{4,6},{6,4},{1,3},{3,1},{5,7},{7,5},{8,10},{10,8},{12,... | collective-permute-start | bytes 983048 | tf_op jit(solution)/shard_map/ppermute | solution.py:26
  62.4 25.0 %collective-permute-start.12 = (bf16[128,1280]{1,0:T(8,128)(2,1)S(1)}, bf16[128,1280]{1,0:T(8,128)(2,1)S(1)}, u32[]{:S(2)}, u32[]{:S(2)}) collective-permute-start(bf16[128,1280]{1,0:T(8,128)(2,1)S(1)} %collective-permute-done.10.refs_11_), channel_id=1, source_target_pairs={{0,4},{2,6},{4,0},{6,2},{1,5},{3,7},{5,1},{7,3},{8,12},{10,14},{12... | collective-permute-start | bytes 983048 | tf_op jit(solution)/shard_map/ppermute | solution.py:26
  68.6 20.6 %collective-permute-start.17 = (bf16[128,1280]{1,0:T(8,128)(2,1)S(1)}, bf16[128,1280]{1,0:T(8,128)(2,1)S(1)}, u32[]{:S(2)}, u32[]{:S(2)}) collective-permute-start(bf16[128,1280]{1,0:T(8,128)(2,1)S(1)} %collective-permute-done.15.refs_7_), channel_id=1, source_target_pairs={{0,4},{2,6},{4,0},{6,2},{1,5},{3,7},{5,1},{7,3},{8,12},{10,14},{12... | collective-permute-start | bytes 983048 | tf_op jit(solution)/shard_map/ppermute | solution.py:26
  75.7 18.5 %collective-permute-start.21 = (bf16[128,1280]{1,0:T(8,128)(2,1)S(1)}, bf16[128,1280]{1,0:T(8,128)(2,1)S(1)}, u32[]{:S(2)}, u32[]{:S(2)}) collective-permute-start(bf16[128,1280]{1,0:T(8,128)(2,1)S(1)} %collective-permute-done.20.refs_12_), channel_id=1, source_target_pairs={{0,2},{2,0},{4,6},{6,4},{1,3},{3,1},{5,7},{7,5},{8,10},{10,8},{12,... | collective-permute-start | bytes 983048 | tf_op jit(solution)/shard_map/ppermute | solution.py:26
  76.2 34.4 %collective-permute-start.25 = (bf16[128,512]{1,0:T(8,128)(2,1)}, bf16[128,512]{1,0:T(8,128)(2,1)S(1)}, u32[]{:S(2)}, u32[]{:S(2)}) collective-permute-start(bf16[128,512]{1,0:T(8,128)(2,1)} %get-tuple-element.48), channel_id=1, source_target_pairs={{0,8},{8,0},{16,24},{24,16},{1,9},{9,1},{17,25},{25,17},{2,10},{10... | collective-permute-start | bytes 393224 | tf_op jit(solution)/shard_map/ppermute | solution.py:26
  87.4 23.8 %collective-permute-start.23 = (bf16[128,512]{1,0:T(8,128)(2,1)}, bf16[128,512]{1,0:T(8,128)(2,1)S(1)}, u32[]{:S(2)}, u32[]{:S(2)}) collective-permute-start(bf16[128,512]{1,0:T(8,128)(2,1)} %get-tuple-element.47.refs_1_), channel_id=1, source_target_pairs={{0,2},{2,0},{4,6},{6,4},{1,3},{3,1},{5,7},{7,5},{8,10},{10,8},{12,... | collective-permute-start | bytes 393224 | tf_op jit(solution)/shard_map/ppermute | solution.py:26
  89.2 28.4 %collective-permute-start.31 = (bf16[256,512]{1,0:T(8,128)(2,1)S(1)}, bf16[256,512]{1,0:T(8,128)(2,1)S(1)}, u32[]{:S(2)}, u32[]{:S(2)}) collective-permute-start(bf16[256,512]{1,0:T(8,128)(2,1)S(1)} %constant_dynamic-update-slice_fusion.refs_7_), channel_id=1, source_target_pairs={{0,4},{2,6},{4,0},{6,2},{1,5},{3,7},{5,1},{7,3},{8,12},{10,14},{12... | collective-permute-start | bytes 786440 | tf_op jit(solution)/shard_map/ppermute | solution.py:26
  90.8 26.9 %collective-permute-start.30 = (bf16[256,512]{1,0:T(8,128)(2,1)S(1)}, bf16[256,512]{1,0:T(8,128)(2,1)S(1)}, u32[]{:S(2)}, u32[]{:S(2)}) collective-permute-start(bf16[256,512]{1,0:T(8,128)(2,1)S(1)} %constant_dynamic-update-slice_fusion.refs_7_), channel_id=1, source_target_pairs={{0,2},{2,0},{4,6},{6,4},{1,3},{3,1},{5,7},{7,5},{8,10},{10,8},{12,... | collective-permute-start | bytes 786440 | tf_op jit(solution)/shard_map/ppermute | solution.py:26
  97.7 14.7 %collective-permute-start.22 = (bf16[2,128,128]{2,1,0:T(8,128)(2,1)S(1)}, bf16[2,128,128]{2,1,0:T(8,128)(2,1)S(1)}, u32[]{:S(2)}, u32[]{:S(2)}) collective-permute-start(bf16[2,128,128]{2,1,0:T(8,128)(2,1)S(1)} %get-tuple-element.45), channel_id=1, source_target_pairs={{0,16},{8,24},{1,17},{9,25},{2,18},{10,26},{3,19},{11,27},{4,20},{... | collective-permute-start | bytes 196616 | tf_op jit(solution)/shard_map/ppermute | solution.py:31
  119.8 10.0 %collective-permute-start.32 = (bf16[256,1536]{1,0:T(8,128)(2,1)S(1)}, bf16[256,1536]{1,0:T(8,128)(2,1)S(1)}, u32[]{:S(2)}, u32[]{:S(2)}) collective-permute-start(bf16[256,1536]{1,0:T(8,128)(2,1)S(1)} %get-tuple-element.50), channel_id=1, source_target_pairs={{0,1},{1,0},{2,3},{3,2},{4,5},{5,4},{6,7},{7,6},{8,9},{9,8},{10,11... | collective-permute-start | bytes 2359304 | tf_op jit(solution)/shard_map/ppermute | solution.py:26
  119.8 9.0 %collective-permute-start.36 = (bf16[256,512]{1,0:T(8,128)(2,1)S(1)}, bf16[256,512]{1,0:T(8,128)(2,1)S(1)}, u32[]{:S(2)}, u32[]{:S(2)}) collective-permute-start(bf16[256,512]{1,0:T(8,128)(2,1)S(1)} %collective-permute-done.31.refs_9_), channel_id=1, source_target_pairs={{0,2},{2,0},{4,6},{6,4},{1,3},{3,1},{5,7},{7,5},{8,10},{10,8},{12,... | collective-permute-start | bytes 786440 | tf_op jit(solution)/shard_map/ppermute | solution.py:26
  120.5 6.4 %collective-permute-start.34 = (bf16[128,512]{1,0:T(8,128)(2,1)S(1)}, bf16[128,512]{1,0:T(8,128)(2,1)S(1)}, u32[]{:S(2)}, u32[]{:S(2)}) collective-permute-start(bf16[128,512]{1,0:T(8,128)(2,1)S(1)} %collective-permute-done.23.refs_2_), channel_id=1, source_target_pairs={{0,4},{2,6},{4,0},{6,2},{1,5},{3,7},{5,1},{7,3},{8,12},{10,14},{12... | collective-permute-start | bytes 393224 | tf_op jit(solution)/shard_map/ppermute | solution.py:26
  122.0 6.9 %collective-permute-start.35 = (bf16[128,512]{1,0:T(8,128)(2,1)S(1)}, bf16[128,512]{1,0:T(8,128)(2,1)S(1)}, u32[]{:S(2)}, u32[]{:S(2)}) collective-permute-start(bf16[128,512]{1,0:T(8,128)(2,1)S(1)} %collective-permute-done.26.refs_5_), channel_id=1, source_target_pairs={{0,4},{2,6},{4,0},{6,2},{1,5},{3,7},{5,1},{7,3},{8,12},{10,14},{12... | collective-permute-start | bytes 393224 | tf_op jit(solution)/shard_map/ppermute | solution.py:26
  129.9 16.4 %collective-permute-start.33 = (bf16[128,1536]{1,0:T(8,128)(2,1)S(1)}, bf16[128,1536]{1,0:T(8,128)(2,1)S(1)}, u32[]{:S(2)}, u32[]{:S(2)}) collective-permute-start(bf16[128,1536]{1,0:T(8,128)(2,1)S(1)} %add_convert_fusion), channel_id=1, source_target_pairs={{0,8},{8,0},{16,24},{24,16},{1,9},{9,1},{17,25},{25,17},{2,10},{10... | collective-permute-start | bytes 1179656 | tf_op jit(solution)/shard_map/ppermute | solution.py:26
  133.8 12.5 %collective-permute-start.38 = (bf16[128,512]{1,0:T(8,128)(2,1)S(1)}, bf16[128,512]{1,0:T(8,128)(2,1)S(1)}, u32[]{:S(2)}, u32[]{:S(2)}) collective-permute-start(bf16[128,512]{1,0:T(8,128)(2,1)S(1)} %add_convert_fusion.1), channel_id=1, source_target_pairs={{0,8},{8,0},{16,24},{24,16},{1,9},{9,1},{17,25},{25,17},{2,10},{10... | collective-permute-start | bytes 393224 | tf_op jit(solution)/shard_map/ppermute | solution.py:26
  (17 other events, 98.8 us)
where the time goes:
time: 148 us; the launch traced here: 147 us
  waiting for transfers between devices  65.3 us (44%)
  starting transfers between devices  63.1 us (43%)
  Pallas kernels  15.7 us (11%)
  local copies, waits for them, and re-layouts  2.76 us (2%)
    ppermute x36, waiting for transfers between devices, swapped(): return lax.ppermute(value, axis, [(i, i ^ distance) for i in range(count)])  64.5 us
    ppermute x36, starting transfers between devices, swapped(): return lax.ppermute(value, axis, [(i, i ^ distance) for i in range(count)])  49 us
    pallas_call x11, Pallas kernels, call(): pl.pallas_call(kernel, out_shape=[jax.ShapeDtypeStruct(shape, dtype) for...  15.7 us
    ppermute x3, starting transfers between devices, passed_on(): lax.ppermute(value, axis, [(i, i + steps) for i in range(first, count - s...  14.2 us
  transfers between devices with their start and end apart: 39, of which 15 were waited for; matrix products, arithmetic and copies ran while one was open for 0% of the time, Pallas kernels for 9%

commit v1 on v0

--- a/solution.py
+++ b/solution.py
@@ -31,7 +31,7 @@
     return lax.ppermute(value, axis, [(i, i + steps) for i in range(first, count - steps, stride)])
 
 
-def call(kernel, outs, *args, scratch=(), outside=(), room=24):
+def call(kernel, outs, *args, scratch=(), outside=(), room=16):
     vmem = pl.BlockSpec(memory_space=pltpu.VMEM)
     anywhere = pl.BlockSpec(memory_space=pltpu.HBM)
     return pl.pallas_call(
@@ -51,7 +51,10 @@
 def over_plane(arrived, groups, routes):
     pieces = []
     for group, route in zip(groups, routes):
-        plane = arrived[group[0]] if len(group) == 1 else jnp.concatenate([arrived[d] for d in group], axis=0)
+        plane = arrived[group[0]]
+        if len(group) > 1:
+            shape = (len(group) * plane.shape[0], plane.shape[1])
+            (plane,) = call(stack_kernel, [(shape, BF16)], *(arrived[d] for d in group))
         by_x = swapped(plane, "fs", 1)
         by_y = swapped(plane, "fs", 2)
         if route == "x":
@@ -63,25 +66,33 @@
     return pieces
 
 
+def stack_kernel(*refs):
+    pieces, out = refs[:-1], refs[-1]
+    rows = pieces[0].shape[0]
+    for k, piece in enumerate(pieces):
+        out[k * rows : (k + 1) * rows, :] = piece[...]
+
+
 def split(pieces):
     return [piece[0] for piece in pieces], tuple(piece[1:] for piece in pieces)
 
 
-def assemble(refs, where, whole, rows, leading=0):
+def assemble(refs, where, whole, rows, leading=0, first=0):
     sp, fs, n_fs = lax.axis_index("sp"), lax.axis_index("fs"), lax.axis_size("fs")
     for ref, (c, distances) in zip(refs, where):
         for k, d in enumerate(distances):
             block = (d // PAIR - leading) * PAIR * n_fs * rows
             spot = block + (((sp ^ d) % PAIR) * n_fs + (fs ^ c)) * rows
-            whole[pl.ds(pl.multiple_of(spot, rows), rows), :] = ref[k * rows : (k + 1) * rows, :]
-
-
-def projected_by(normed, whole, rows, leading):
+            cut = ref[k * rows : (k + 1) * rows, first : first + whole.shape[1]]
+            whole[pl.ds(pl.multiple_of(spot, rows), rows), :] = cut
+
+
+def projected_by(normed, whole, rows, leading, upto=None):
     pair, wide = lax.axis_index("sp") // PAIR, PAIR * lax.axis_size("fs") * rows
     total = None
     for k in range(whole.shape[0] // wide):
         features = pl.ds(pl.multiple_of((pair ^ (k + leading)) * wide, wide), wide)
-        part = dot(normed[:, features], whole[k * wide : (k + 1) * wide, :], ((1,), (0,)))
+        part = dot(normed[0 : upto or normed.shape[0], features], whole[k * wide : (k + 1) * wide, :], ((1,), (0,)))
         total = part if total is None else total + part
     return total
 
@@ -166,10 +177,10 @@
 def mix_kernel(*refs, where, rows):
     normed, earlier, room_whole, shift_mine, shift_near, start = refs[:6]
     shards = refs[6 : 6 + len(where)]
-    projected_out, keyed_out, within_out, state_out, fade_out, leaving_out, opening_out, total_out, last_out, border_out = refs[
-        6 + len(where) : 16 + len(where)
+    value_out, keyed_out, within_out, state_out, fade_out, leaving_out, opening_out, total_out, last_out = refs[
+        6 + len(where) : 15 + len(where)
     ]
-    whole, shift, first, sem = refs[16 + len(where) :]
+    whole, shift, first, sem = refs[15 + len(where) :]
     part = lax.axis_index("sp") % PAIR
     length, width = keyed_out.shape
     heads = width // HEAD
@@ -181,9 +192,9 @@
     shift[0:lines, pl.ds(pl.multiple_of((1 - part) * own, own), own)] = shift_near[...]
     shifts = shift[...].T
     assemble(shards, where, whole, rows, 1)
-    projected = (earlier[...] + projected_by(normed, whole, rows, 1)).astype(BF16)
-    projected_out[...] = projected[0:length, :]
-    border_out[...] = projected[length:, 4 * width :]
+    projected = earlier[0:length, 0 : 2 * width] + projected_by(normed, whole, rows, 1, length)
+    projected = projected.astype(BF16)
+    value_out[...] = projected[:, width:]
     room = room_whole[:, pl.ds(pl.multiple_of(part * width, width), width)]
     t = lax.broadcasted_iota(jnp.int32, (BLOCK, BLOCK), 0)
     s = lax.broadcasted_iota(jnp.int32, (BLOCK, BLOCK), 1)
@@ -193,7 +204,7 @@
     for n in range(length // BLOCK):
         span = slice(n * BLOCK, (n + 1) * BLOCK)
         logits = projected[span, 0:width].astype(F32)
-        value = projected[span, 2 * width : 3 * width]
+        value = projected[span, width:]
         keyed = room * (1.0 - jax.nn.sigmoid(logits))
         every = shifts[span, :]
         lags = [
@@ -222,15 +233,23 @@
         total_out[h] = total
 
 
-def inside_kernel(projected, keyed, within_all, inside_out, reach_out):
+def inside_kernel(*refs, where, rows):
+    normed, earlier, value_all, keyed, within_all = refs[:5]
+    shards = refs[5 : 5 + len(where)]
+    inside_out, reach_out, gate_out, pool_out, border_out, whole = refs[5 + len(where) :]
     length, width = keyed.shape
+    assemble(shards, where, whole, rows, 1, 2 * width)
+    projected = (earlier[:, 2 * width :] + projected_by(normed, whole, rows, 1)).astype(BF16)
+    gate_out[...] = projected[0:length, width : 2 * width]
+    pool_out[...] = projected[0:length, 2 * width :]
+    border_out[...] = projected[length:, 2 * width :]
     t = lax.broadcasted_iota(jnp.int32, (BLOCK, BLOCK), 0)
     s = lax.broadcasted_iota(jnp.int32, (BLOCK, BLOCK), 1)
     causal = s <= t
     for n in range(length // BLOCK):
         span = slice(n * BLOCK, (n + 1) * BLOCK)
-        queries = jax.nn.silu(projected[span, width : 2 * width].astype(F32)) * HEAD ** (-0.5)
-        value = projected[span, 2 * width : 3 * width]
+        queries = jax.nn.silu(projected[span, 0:width].astype(F32)) * HEAD ** (-0.5)
+        value = value_all[span, :]
         within = within_all[span, :]
         centre = within[BLOCK // 2 - 1 : BLOCK // 2]
         near_q = (queries * jnp.exp(within - centre)).astype(BF16)
@@ -243,7 +262,7 @@
 
 
 def join_kernel(
-    inside, reach, states, fades, opening, arrived, projected, head_gain, border, mappings, scales, joined, extended
+    inside, reach, states, fades, opening, arrived, gate, pool, head_gain, border, mappings, scales, joined, extended
 ):
     length, width = inside.shape
     heads = width // HEAD
@@ -257,10 +276,10 @@
             memory = states[n, h] + fades[n, h : h + 1] * entering
             raw = inside[span, lanes] + dot(reach[span, lanes], memory.astype(BF16), ((1,), (1,)))
             level = lax.rsqrt(jnp.mean(raw * raw, axis=1, keepdims=True) + EPSILON)
-            gating = jax.nn.silu(projected[span, 3 * width + h * HEAD : 3 * width + (h + 1) * HEAD].astype(F32))
+            gating = jax.nn.silu(gate[span, lanes].astype(F32))
             joined[span, lanes] = (raw * level * head_gain[...] * gating).astype(BF16)
     extended[0:WIDEST, :] = border[...].astype(F32)
-    extended[WIDEST:, :] = projected[:, 4 * width :].astype(F32)
+    extended[WIDEST:, :] = pool[...].astype(F32)
     sums = extended[...]
     grouping = tp * PAIR + part
     chosen = jnp.zeros((length, width), F32)
@@ -278,12 +297,16 @@
     joined[:, width:] = (mapped * scale).astype(BF16)
 
 
-def out_kernel(*refs, count, sort):
-    joined = refs[0]
-    shards = refs[1 : 1 + count]
-    keep_out, far_out, send_out, whole = refs[1 + count :]
+def rows_owed(joined, whole, owner_part, owner_tp):
+    quarter = joined.shape[0] // (PAIR * 2)
+    rows = pl.ds(pl.multiple_of((owner_part * 2 + owner_tp) * quarter, quarter), quarter)
+    return dot(joined[rows, :], whole[...], ((1,), (1,))).astype(BF16)
+
+
+def send_kernel(*refs, count, sort):
+    joined, shards = refs[0], refs[1 : 1 + count]
+    send_out, whole = refs[1 + count :]
     part, tp = lax.axis_index("sp") % PAIR, lax.axis_index("tp")
-    quarter = keep_out.shape[0]
     if sort is None:
         spot = 0
         for shard in shards:
@@ -296,15 +319,15 @@
             for k, d in enumerate(distances):
                 spot = ((sp ^ d) * n_fs + (fs ^ c)) * rows
                 whole[pl.ds(pl.multiple_of(spot, rows), rows), :] = shard[k * rows : (k + 1) * rows, :]
-
-    def mixed(owner_part, owner_tp):
-        spot = (owner_part * 2 + owner_tp) * quarter
-        return dot(joined[pl.ds(pl.multiple_of(spot, quarter), quarter), :], whole[...], ((1,), (1,)))
-
-    send_out[0:quarter, :] = mixed(part, 1 - tp).astype(BF16)
-    send_out[quarter:, :] = mixed(1 - part, 1 - tp).astype(BF16)
-    far_out[...] = mixed(1 - part, tp).astype(BF16)
-    keep_out[...] = mixed(part, tp).astype(BF16)
+    quarter = send_out.shape[0] // 2
+    send_out[0:quarter, :] = rows_owed(joined, whole, part, 1 - tp)
+    send_out[quarter:, :] = rows_owed(joined, whole, 1 - part, 1 - tp)
+
+
+def keep_kernel(joined, whole, keep_out, far_out):
+    part, tp = lax.axis_index("sp") % PAIR, lax.axis_index("tp")
+    far_out[...] = rows_owed(joined, whole, 1 - part, tp)
+    keep_out[...] = rows_owed(joined, whole, part, tp)
 
 
 def final_kernel(*refs, order, columns):
@@ -357,8 +380,8 @@
         pack_kernel,
         pack_out,
         forget_weight,
+        value_weight,
         query_weight,
-        value_weight,
         outgate_weight,
         pool_in_weight,
         scratch=[pltpu.SemaphoreType.DMA((2, 5))],
@@ -387,11 +410,10 @@
     line_c = along_line(out_same, out_other)
     cut = (n_sp + 2) // 2
     fine = [[0], [1], list(range(2, cut)), list(range(cut, n_sp))]
-    coarse = [[0], [1], list(range(2, n_sp))]
     mix_pieces = over_plane(line_a, fine, "xyyx")
     first_shards, first_where = split([p for p in mix_pieces if p[2][0] < PAIR])
     mix_shards, mix_where = split([p for p in mix_pieces if p[2][0] >= PAIR])
-    out_pieces = over_plane(line_c, coarse, "yyx")
+    out_pieces = over_plane(line_c, [[0], list(range(1, n_sp))], "yy")
     near_other = swapped(near, "tp", 1)
     wide = PAIR * n_fs * rows
     normed, earlier = call(
@@ -406,10 +428,10 @@
         *first_shards,
         scratch=[pltpu.VMEM((wide, 5 * columns), BF16)],
     )
-    projected, keyed, within, states, fades, leaving, opening, total, last, border = call(
+    value, keyed, within, states, fades, leaving, opening, total, last = call(
         functools.partial(mix_kernel, where=mix_where, rows=rows),
         [
-            ((length, 5 * columns), BF16),
+            ((length, columns), BF16),
             ((length, columns), F32),
             ((length, columns), F32),
             ((blocks, heads, HEAD, HEAD), F32),
@@ -418,7 +440,6 @@
             ((heads, HEAD, HEAD), F32),
             ((heads, 1, HEAD), F32),
             ((heads, HEAD, HEAD), F32),
-            ((WIDEST, columns), BF16),
         ],
         normed,
         earlier,
@@ -428,13 +449,13 @@
         start_state[0],
         *mix_shards,
         scratch=[
-            pltpu.VMEM((model - wide, 5 * columns), BF16),
+            pltpu.VMEM((model - wide, 2 * columns), BF16),
             pltpu.VMEM((8, length), F32),
             pltpu.VMEM((heads, HEAD, HEAD), F32),
             pltpu.SemaphoreType.DMA(()),
         ],
         outside=(5,),
-        room=30,
+        room=16,
     )
     arrived = passed_on(leaving, "sp", PAIR)
 
@@ -445,7 +466,23 @@
 
     if n_sp // PAIR > 2:
         arrived = lax.fori_loop(0, n_sp // PAIR - 2, handoff, arrived)
-    inside, reach = call(inside_kernel, [((length, columns), F32), ((length, columns), BF16)], projected, keyed, within)
+    inside, reach, gate, pool, border = call(
+        functools.partial(inside_kernel, where=mix_where, rows=rows),
+        [
+            ((length, columns), F32),
+            ((length, columns), BF16),
+            ((length, columns), BF16),
+            ((length, columns), BF16),
+            ((WIDEST, columns), BF16),
+        ],
+        normed,
+        earlier,
+        value,
+        keyed,
+        within,
+        *mix_shards,
+        scratch=[pltpu.VMEM((model - wide, 3 * columns), BF16)],
+    )
     (joined,) = call(
         join_kernel,
         [((length, 2 * columns), BF16)],
@@ -455,7 +492,8 @@
         fades,
         opening,
         arrived,
-        projected,
+        gate,
+        pool,
         head_gain[None],
         border,
         pool_map,
@@ -467,19 +505,19 @@
     if out_rows % 128:
         sets = [out_pieces]
     else:
-        sets = [[p for p in out_pieces if p[1] in near_by] for near_by in ((0, 1, 2), (3,))]
+        sets = [[p for p in out_pieces if p[1] in near_by] for near_by in ((0, 1), (2,), (3,))]
     shares, order = [], []
     for pieces in sets:
         shards, where = split(pieces)
         sort = (where, out_rows) if out_rows % 128 else None
         wide = sum(shard.shape[0] for shard in shards)
-        keep, far, send = call(
-            functools.partial(out_kernel, count=len(shards), sort=sort),
-            [((quarter, wide), BF16), ((quarter, wide), BF16), ((2 * quarter, wide), BF16)],
+        send, whole = call(
+            functools.partial(send_kernel, count=len(shards), sort=sort),
+            [((2 * quarter, wide), BF16), ((wide, 2 * columns), BF16)],
             joined,
             *shards,
-            scratch=[pltpu.VMEM((wide, 2 * columns), BF16)],
         )
+        keep, far = call(keep_kernel, [((quarter, wide), BF16)] * 2, joined, whole)
         met = swapped(send, "tp", 1)
         owed = (far.astype(F32) + met[quarter:].astype(F32)).astype(BF16)
         shares += [keep, met, swapped(owed, "sp", 1)]

time: 148 us -> 140 us (0.946)
  starting transfers between devices: 63.1 us -> 54.9 us
    ppermute x36 -> x35, starting transfers between devices: 49 us -> 44.7 us  [swapped(): return lax.ppermute(value, axis, [(i, i ^ distance) for i in range(count)])]
    ppermute x3, starting transfers between devices: 14.2 us -> 10.2 us  [passed_on(): lax.ppermute(value, axis, [(i, i + steps) for i in range(first, count - s...]
    pallas_call x11 -> x16, Pallas kernels: 15.7 us -> 16.7 us  [call(): pl.pallas_call(kernel, out_shape=[jax.ShapeDtypeStruct(shape, dtype) for...]
    ppermute x36 -> x35, waiting for transfers between devices: 64.5 us -> 64.9 us  [swapped(): return lax.ppermute(value, axis, [(i, i ^ distance) for i in range(count)])]
  transfers between devices with their start and end apart: 39 -> 38, of which waited for: 15 -> 17; matrix products, arithmetic and copies ran while one was open for 0% -> 0% of each run, Pallas kernels for 9% -> 11%
where the time goes in v1:
time: 140 us
  waiting for transfers between devices  64.9 us (46%)
  starting transfers between devices  54.9 us (39%)
  Pallas kernels  16.7 us (12%)
  local copies, waits for them, and re-layouts  2.75 us (2%)
    ppermute x35, waiting for transfers between devices, swapped(): return lax.ppermute(value, axis, [(i, i ^ distance) for i in range(count)])  64.9 us
    ppermute x35, starting transfers between devices, swapped(): return lax.ppermute(value, axis, [(i, i ^ distance) for i in range(count)])  44.7 us
    pallas_call x16, Pallas kernels, call(): pl.pallas_call(kernel, out_shape=[jax.ShapeDtypeStruct(shape, dtype) for...  16.7 us
    ppermute x3, starting transfers between devices, passed_on(): lax.ppermute(value, axis, [(i, i + steps) for i in range(first, count - s...  10.2 us
  transfers between devices with their start and end apart: 38, of which 17 were waited for; matrix products, arithmetic and copies ran while one was open for 0% of the time, Pallas kernels for 11%

profile of v1, /device:TPU:0, one launch (start us, length us, event | category | flops | bytes accessed | tf_op | source)
XLA Modules:
  0.0 139.7 jit_solution(15969875070657717431)
XLA Ops:
  0.5 2.0 %shard_map.147 = (bf16[128,1280]{1,0:T(8,128)(2,1)}, bf16[128,1280]{1,0:T(8,128)(2,1)}) custom-call(bf16[128,512]{1,0:T(8,128)(2,1)} %refs_0_.2, bf16[128,512]{1,0:T(8,128)(2,1)} %refs_1_.2, bf16[128,512]{1,0:T(8,128)(2,1)} %refs_2_.1, bf16[128,512]{1,0:T(8,128)(2,1)} %refs_3_.1, bf16[128,512]{1,0:T(8,128)(2,1)} %refs_4_.1), custom_call_target="tpu_custom_call" | custom-call | tf_op jit(solution)/shard_map/pallas_call | solution.py:37
  2.5 2.6 %collective-permute-start.9 = (bf16[128,1280]{1,0:T(8,128)(2,1)}, bf16[128,1280]{1,0:T(8,128)(2,1)S(1)}, u32[]{:S(2)}, u32[]{:S(2)}) collective-permute-start(bf16[128,1280]{1,0:T(8,128)(2,1)} %get-tuple-element.42), channel_id=1, source_target_pairs={{0,8},{8,0},{16,24},{24,16},{1,9},{9,1},{17,25},{25,17},{2,10},{10... | collective-permute-start | bytes 983048 | tf_op jit(solution)/shard_map/ppermute | solution.py:26
  5.2 1.8 %shard_map.152 = (bf16[128,512]{1,0:T(8,128)(2,1)}, bf16[128,512]{1,0:T(8,128)(2,1)}) custom-call(bf16[512,128]{1,0:T(8,128)(2,1)} %refs_0_.3, bf16[512,128]{1,0:T(8,128)(2,1)} %refs_1_.3), custom_call_target="tpu_custom_call" | custom-call | tf_op jit(solution)/shard_map/pallas_call | solution.py:37
  7.0 2.7 %collective-permute-start.25 = (bf16[128,512]{1,0:T(8,128)(2,1)}, bf16[128,512]{1,0:T(8,128)(2,1)S(1)}, u32[]{:S(2)}, u32[]{:S(2)}) collective-permute-start(bf16[128,512]{1,0:T(8,128)(2,1)} %get-tuple-element.57.refs_1_), channel_id=1, source_target_pairs={{0,16},{8,24},{16,0},{24,8},{1,17},{9,25},{17,1},{25,9},{2,18},{10... | collective-permute-start | bytes 393224 | tf_op jit(solution)/shard_map/ppermute | solution.py:26
  10.1 1.6 %collective-permute-start.13 = (f32[4,256]{1,0:T(4,128)}, f32[4,256]{1,0:T(4,128)S(1)}, u32[]{:S(2)}, u32[]{:S(2)}) collective-permute-start(f32[4,256]{1,0:T(4,128)} %bitcast.14), channel_id=1, source_target_pairs={{0,8},{8,0},{16,24},{24,16},{1,9},{9,1},{17,25},{25,17},{2,10},{10... | collective-permute-start | bytes 12296 | tf_op jit(solution)/shard_map/ppermute | solution.py:26
  11.6 7.8 %collective-permute-done.13.refs_4_ = f32[4,256]{1,0:T(4,128)S(1)} collective-permute-done((f32[4,256]{1,0:T(4,128)}, f32[4,256]{1,0:T(4,128)S(1)}, u32[]{:S(2)}, u32[]{:S(2)}) %collective-permute-start.13) | collective-permute-done | bytes 4128 | tf_op jit(solution)/shard_map/ppermute | solution.py:26
  19.5 3.8 %collective-permute-start.26 = (bf16[128,512]{1,0:T(8,128)(2,1)}, bf16[128,512]{1,0:T(8,128)(2,1)S(1)}, u32[]{:S(2)}, u32[]{:S(2)}) collective-permute-start(bf16[128,512]{1,0:T(8,128)(2,1)} %get-tuple-element.58), channel_id=1, source_target_pairs={{0,24},{8,16},{16,8},{24,0},{1,25},{9,17},{17,9},{25,1},{2,26},{10... | collective-permute-start | bytes 393224 | tf_op jit(solution)/shard_map/ppermute | solution.py:26
  28.4 3.4 %collective-permute-start.14 = (bf16[128,1280]{1,0:T(8,128)(2,1)}, bf16[128,1280]{1,0:T(8,128)(2,1)S(1)}, u32[]{:S(2)}, u32[]{:S(2)}) collective-permute-start(bf16[128,1280]{1,0:T(8,128)(2,1)} %get-tuple-element.41.refs_6_), channel_id=1, source_target_pairs={{0,16},{8,24},{16,0},{24,8},{1,17},{9,25},{17,1},{25,9},{2,18},{10... | collective-permute-start | bytes 983048 | tf_op jit(solution)/shard_map/ppermute | solution.py:26
  38.1 15.9 %collective-permute-done.14.refs_6_.refs_5_ = bf16[128,1280]{1,0:T(8,128)(2,1)S(1)} collective-permute-done((bf16[128,1280]{1,0:T(8,128)(2,1)}, bf16[128,1280]{1,0:T(8,128)(2,1)S(1)}, u32[]{:S(2)}, u32[]{:S(2)}) %collective-permute-start.14) | collective-permute-done | bytes 327712 | tf_op jit(solution)/shard_map/ppermute | solution.py:26
  55.2 1.5 %collective-permute-start.8 = (bf16[128,1280]{1,0:T(8,128)(2,1)S(1)}, bf16[128,1280]{1,0:T(8,128)(2,1)S(1)}, u32[]{:S(2)}, u32[]{:S(2)}) collective-permute-start(bf16[128,1280]{1,0:T(8,128)(2,1)S(1)} %collective-permute-done.7.refs_8_), channel_id=1, source_target_pairs={{0,2},{2,0},{4,6},{6,4},{1,3},{3,1},{5,7},{7,5},{8,10},{10,8},{12,... | collective-permute-start | bytes 983048 | tf_op jit(solution)/shard_map/ppermute | solution.py:26
  56.8 1.5 %collective-permute-start.11 = (bf16[128,1280]{1,0:T(8,128)(2,1)S(1)}, bf16[128,1280]{1,0:T(8,128)(2,1)S(1)}, u32[]{:S(2)}, u32[]{:S(2)}) collective-permute-start(bf16[128,1280]{1,0:T(8,128)(2,1)S(1)} %collective-permute-done.9.refs_10_), channel_id=1, source_target_pairs={{0,4},{2,6},{4,0},{6,2},{1,5},{3,7},{5,1},{7,3},{8,12},{10,14},{12... | collective-permute-start | bytes 983048 | tf_op jit(solution)/shard_map/ppermute | solution.py:26
  60.1 5.2 %collective-permute-done.10.refs_11_ = bf16[128,1280]{1,0:T(8,128)(2,1)S(1)} collective-permute-done((bf16[128,1280]{1,0:T(8,128)(2,1)S(1)}, bf16[128,1280]{1,0:T(8,128)(2,1)S(1)}, u32[]{:S(2)}, u32[]{:S(2)}) %collective-permute-start.10) | collective-permute-done | bytes 327712 | tf_op jit(solution)/shard_map/ppermute | solution.py:26
  65.3 1.5 %collective-permute-start.20 = (bf16[128,1280]{1,0:T(8,128)(2,1)S(1)}, bf16[128,1280]{1,0:T(8,128)(2,1)S(1)}, u32[]{:S(2)}, u32[]{:S(2)}) collective-permute-start(bf16[128,1280]{1,0:T(8,128)(2,1)S(1)} %collective-permute-done.18.refs_10_.refs_9_), channel_id=1, source_target_pairs={{0,4},{2,6},{4,0},{6,2},{1,5},{3,7},{5,1},{7,3},{8,12},{10,14},{12... | collective-permute-start | bytes 983048 | tf_op jit(solution)/shard_map/ppermute | solution.py:26
  66.8 5.5 %collective-permute-done.8.refs_9_ = bf16[128,1280]{1,0:T(8,128)(2,1)S(1)} collective-permute-done((bf16[128,1280]{1,0:T(8,128)(2,1)S(1)}, bf16[128,1280]{1,0:T(8,128)(2,1)S(1)}, u32[]{:S(2)}, u32[]{:S(2)}) %collective-permute-start.8) | collective-permute-done | bytes 327712 | tf_op jit(solution)/shard_map/ppermute | solution.py:26
  72.3 1.5 %collective-permute-start.16 = (bf16[128,1280]{1,0:T(8,128)(2,1)S(1)}, bf16[128,1280]{1,0:T(8,128)(2,1)S(1)}, u32[]{:S(2)}, u32[]{:S(2)}) collective-permute-start(bf16[128,1280]{1,0:T(8,128)(2,1)S(1)} %collective-permute-done.14.refs_6_.refs_5_), channel_id=1, source_target_pairs={{0,4},{2,6},{4,0},{6,2},{1,5},{3,7},{5,1},{7,3},{8,12},{10,14},{12... | collective-permute-start | bytes 983048 | tf_op jit(solution)/shard_map/ppermute | solution.py:26
  74.4 3.8 %collective-permute-done.15.refs_7_.refs_6_ = bf16[128,1280]{1,0:T(8,128)(2,1)S(1)} collective-permute-done((bf16[128,1280]{1,0:T(8,128)(2,1)S(1)}, bf16[128,1280]{1,0:T(8,128)(2,1)S(1)}, u32[]{:S(2)}, u32[]{:S(2)}) %collective-permute-start.15) | collective-permute-done | bytes 327712 | tf_op jit(solution)/shard_map/ppermute | solution.py:26
  78.2 1.7 %collective-permute-start.12 = (bf16[128,1280]{1,0:T(8,128)(2,1)S(1)}, bf16[128,1280]{1,0:T(8,128)(2,1)S(1)}, u32[]{:S(2)}, u32[]{:S(2)}) collective-permute-start(bf16[128,1280]{1,0:T(8,128)(2,1)S(1)} %collective-permute-done.10.refs_11_), channel_id=1, source_target_pairs={{0,4},{2,6},{4,0},{6,2},{1,5},{3,7},{5,1},{7,3},{8,12},{10,14},{12... | collective-permute-start | bytes 983048 | tf_op jit(solution)/shard_map/ppermute | solution.py:26
  81.9 2.6 %collective-permute-done.19.refs_11_.refs_10_ = bf16[128,1280]{1,0:T(8,128)(2,1)S(1)} collective-permute-done((bf16[128,1280]{1,0:T(8,128)(2,1)S(1)}, bf16[128,1280]{1,0:T(8,128)(2,1)S(1)}, u32[]{:S(2)}, u32[]{:S(2)}) %collective-permute-start.19) | collective-permute-done | bytes 327712 | tf_op jit(solution)/shard_map/ppermute | solution.py:26
  84.5 2.2 %collective-permute-start.35 = (bf16[384,512]{1,0:T(8,128)(2,1)S(1)}, bf16[384,512]{1,0:T(8,128)(2,1)S(1)}, u32[]{:S(2)}, u32[]{:S(2)}) collective-permute-start(bf16[384,512]{1,0:T(8,128)(2,1)S(1)} %collective-permute-done.27.refs_4_), channel_id=1, source_target_pairs={{0,4},{2,6},{4,0},{6,2},{1,5},{3,7},{5,1},{7,3},{8,12},{10,14},{12... | collective-permute-start | bytes 1179656 | tf_op jit(solution)/shard_map/ppermute | solution.py:26
  86.7 2.1 %collective-permute-done.12.refs_13_ = bf16[128,1280]{1,0:T(8,128)(2,1)S(1)} collective-permute-done((bf16[128,1280]{1,0:T(8,128)(2,1)S(1)}, bf16[128,1280]{1,0:T(8,128)(2,1)S(1)}, u32[]{:S(2)}, u32[]{:S(2)}) %collective-permute-start.12) | collective-permute-done | bytes 327712 | tf_op jit(solution)/shard_map/ppermute | solution.py:26
  88.8 2.1 %collective-permute-start.31 = (bf16[384,512]{1,0:T(8,128)(2,1)S(1)}, bf16[384,512]{1,0:T(8,128)(2,1)S(1)}, u32[]{:S(2)}, u32[]{:S(2)}) collective-permute-start(bf16[384,512]{1,0:T(8,128)(2,1)S(1)} %shard_map.153.refs_3_), channel_id=1, source_target_pairs={{0,4},{2,6},{4,0},{6,2},{1,5},{3,7},{5,1},{7,3},{8,12},{10,14},{12... | collective-permute-start | bytes 1179656 | tf_op jit(solution)/shard_map/ppermute | solution.py:26
  91.9 1.9 %shard_map.148 = (bf16[528,2048]{1,0:T(8,128)(2,1)S(1)}, f32[528,1280]{1,0:T(8,128)S(1)}) custom-call(bf16[256,1024]{1,0:T(8,128)(2,1)S(1)} %get-tuple-element.38.refs_0_, bf16[256,1024]{1,0:T(8,128)(2,1)S(1)} %get-tuple-element.39.refs_1_, bf16[256,1024]{1,0:T(8,128)(2,1)S(1)} %collective-permute-done.1.refs_2_, ...), custom_call_target="tpu_custom_call" | custom-call | tf_op jit(solution)/shard_map/pallas_call | solution.py:37
  93.8 2.0 %collective-permute-done.17.refs_9_.refs_8_ = bf16[128,1280]{1,0:T(8,128)(2,1)S(1)} collective-permute-done((bf16[128,1280]{1,0:T(8,128)(2,1)S(1)}, bf16[128,1280]{1,0:T(8,128)(2,1)S(1)}, u32[]{:S(2)}, u32[]{:S(2)}) %collective-permute-start.17) | collective-permute-done | bytes 327712 | tf_op jit(solution)/shard_map/ppermute | solution.py:26
  95.8 3.0 %shard_map.149 = (bf16[512,256]{1,0:T(8,128)(2,1)S(1)}, f32[512,256]{1,0:T(8,128)S(1)}, f32[512,256]{1,0:T(8,128)S(1)}, f32[4,2,128,128]{3,2,1,0:T(8,128)S(1)}, ...) custom-call(bf16[528,2048]{1,0:T(8,128)(2,1)S(1)} %get-tuple-element, ...), custom_call_target="tpu_custom_call" | custom-call | tf_op jit(solution)/shard_map/pallas_call | solution.py:37
  98.8 8.9 %collective-permute-start.22 = (bf16[2,128,128]{2,1,0:T(8,128)(2,1)S(1)}, bf16[2,128,128]{2,1,0:T(8,128)(2,1)S(1)}, u32[]{:S(2)}, u32[]{:S(2)}) collective-permute-start(bf16[2,128,128]{2,1,0:T(8,128)(2,1)S(1)} %get-tuple-element.53), channel_id=1, source_target_pairs={{0,16},{8,24},{1,17},{9,25},{2,18},{10,26},{3,19},{11,27},{4,20},{... | collective-permute-start | bytes 196616 | tf_op jit(solution)/shard_map/ppermute | solution.py:31
  107.8 2.2 %shard_map.150 = (f32[512,256]{1,0:T(8,128)S(1)}, bf16[512,256]{1,0:T(8,128)(2,1)S(1)}, bf16[512,256]{1,0:T(8,128)(2,1)S(1)}, bf16[512,256]{1,0:T(8,128)(2,1)S(1)}, bf16[16,256]{1,0:T(8,128)(2,1)S(1)}) custom-call(bf16[528,2048]{1,0:T(8,128)(2,1)S(1)} %get-tuple-element.43.refs_0_, f32[528,1280]{1,0:T(8,128)S(1)} %get-tuple-element.44.refs_1_, ...), custom_call_target="tpu_custom_call" | custom-call | tf_op jit(solution)/shard_map/pallas_call | solution.py:37
  113.7 1.6 %collective-permute-start.30 = (bf16[128,512]{1,0:T(8,128)(2,1)S(1)}, bf16[128,512]{1,0:T(8,128)(2,1)S(1)}, u32[]{:S(2)}, u32[]{:S(2)}) collective-permute-start(bf16[128,512]{1,0:T(8,128)(2,1)S(1)} %copy-done.4), channel_id=1, source_target_pairs={{0,4},{2,6},{4,0},{6,2},{1,5},{3,7},{5,1},{7,3},{8,12},{10,14},{12... | collective-permute-start | bytes 393224 | tf_op jit(solution)/shard_map/ppermute | solution.py:26
  115.8 3.8 %collective-permute-done.30.refs_1_ = bf16[128,512]{1,0:T(8,128)(2,1)S(1)} collective-permute-done((bf16[128,512]{1,0:T(8,128)(2,1)S(1)}, bf16[128,512]{1,0:T(8,128)(2,1)S(1)}, u32[]{:S(2)}, u32[]{:S(2)}) %collective-permute-start.30) | collective-permute-done | bytes 131104 | tf_op jit(solution)/shard_map/ppermute | solution.py:26
  121.5 4.6 %collective-permute-start.37 = (bf16[128,512]{1,0:T(8,128)(2,1)S(1)}, bf16[128,512]{1,0:T(8,128)(2,1)S(1)}, u32[]{:S(2)}, u32[]{:S(2)}) collective-permute-start(bf16[128,512]{1,0:T(8,128)(2,1)S(1)} %add_convert_fusion.1), channel_id=1, source_target_pairs={{0,8},{8,0},{16,24},{24,16},{1,9},{9,1},{17,25},{25,17},{2,10},{10... | collective-permute-start | bytes 393224 | tf_op jit(solution)/shard_map/ppermute | solution.py:26
  126.3 2.1 %collective-permute-start.33 = (bf16[128,512]{1,0:T(8,128)(2,1)S(1)}, bf16[128,512]{1,0:T(8,128)(2,1)S(1)}, u32[]{:S(2)}, u32[]{:S(2)}) collective-permute-start(bf16[128,512]{1,0:T(8,128)(2,1)S(1)} %add_convert_fusion.2), channel_id=1, source_target_pairs={{0,8},{8,0},{16,24},{24,16},{1,9},{9,1},{17,25},{25,17},{2,10},{10... | collective-permute-start | bytes 393224 | tf_op jit(solution)/shard_map/ppermute | solution.py:26
  128.4 2.1 %collective-permute-done.37.refs_8_ = bf16[128,512]{1,0:T(8,128)(2,1)S(1)} collective-permute-done((bf16[128,512]{1,0:T(8,128)(2,1)S(1)}, bf16[128,512]{1,0:T(8,128)(2,1)S(1)}, u32[]{:S(2)}, u32[]{:S(2)}) %collective-permute-start.37) | collective-permute-done | bytes 131104 | tf_op jit(solution)/shard_map/ppermute | solution.py:26
  130.5 8.2 %collective-permute-done.33.refs_5_ = bf16[128,512]{1,0:T(8,128)(2,1)S(1)} collective-permute-done((bf16[128,512]{1,0:T(8,128)(2,1)S(1)}, bf16[128,512]{1,0:T(8,128)(2,1)S(1)}, u32[]{:S(2)}, u32[]{:S(2)}) %collective-permute-start.33) | collective-permute-done | bytes 131104 | tf_op jit(solution)/shard_map/ppermute | solution.py:26
  (83 shorter events, 26.0 us)
Async XLA Ops:
  0.0 33.2 %collective-permute-start = (bf16[256,1024]{1,0:T(8,128)(2,1)}, bf16[256,1024]{1,0:T(8,128)(2,1)S(1)}, u32[]{:S(2)}, u32[]{:S(2)}) collective-permute-start(bf16[256,1024]{1,0:T(8,128)(2,1)} %bitcast.10), channel_id=1, source_target_pairs={{0,1},{1,0},{2,3},{3,2},{4,5},{5,4},{6,7},{7,6},{8,9},{9,8},{10,11... | collective-permute-start | bytes 1572872 | tf_op jit(solution)/shard_map/ppermute | solution.py:26
  2.5 29.2 %collective-permute-start.9 = (bf16[128,1280]{1,0:T(8,128)(2,1)}, bf16[128,1280]{1,0:T(8,128)(2,1)S(1)}, u32[]{:S(2)}, u32[]{:S(2)}) collective-permute-start(bf16[128,1280]{1,0:T(8,128)(2,1)} %get-tuple-element.42), channel_id=1, source_target_pairs={{0,8},{8,0},{16,24},{24,16},{1,9},{9,1},{17,25},{25,17},{2,10},{10... | collective-permute-start | bytes 983048 | tf_op jit(solution)/shard_map/ppermute | solution.py:26
  7.0 16.3 %collective-permute-start.25 = (bf16[128,512]{1,0:T(8,128)(2,1)}, bf16[128,512]{1,0:T(8,128)(2,1)S(1)}, u32[]{:S(2)}, u32[]{:S(2)}) collective-permute-start(bf16[128,512]{1,0:T(8,128)(2,1)} %get-tuple-element.57.refs_1_), channel_id=1, source_target_pairs={{0,16},{8,24},{16,0},{24,8},{1,17},{9,25},{17,1},{25,9},{2,18},{10... | collective-permute-start | bytes 393224 | tf_op jit(solution)/shard_map/ppermute | solution.py:26
  9.6 15.1 %collective-permute-start.24 = (bf16[128,512]{1,0:T(8,128)(2,1)}, bf16[128,512]{1,0:T(8,128)(2,1)S(1)}, u32[]{:S(2)}, u32[]{:S(2)}) collective-permute-start(bf16[128,512]{1,0:T(8,128)(2,1)} %get-tuple-element.58), channel_id=1, source_target_pairs={{0,8},{8,0},{16,24},{24,16},{1,9},{9,1},{17,25},{25,17},{2,10},{10... | collective-permute-start | bytes 393224 | tf_op jit(solution)/shard_map/ppermute | solution.py:26
  10.1 9.4 %collective-permute-start.13 = (f32[4,256]{1,0:T(4,128)}, f32[4,256]{1,0:T(4,128)S(1)}, u32[]{:S(2)}, u32[]{:S(2)}) collective-permute-start(f32[4,256]{1,0:T(4,128)} %bitcast.14), channel_id=1, source_target_pairs={{0,8},{8,0},{16,24},{24,16},{1,9},{9,1},{17,25},{25,17},{2,10},{10... | collective-permute-start | bytes 12296 | tf_op jit(solution)/shard_map/ppermute | solution.py:26
  24.7 11.2 %collective-permute-start.7 = (bf16[128,1280]{1,0:T(8,128)(2,1)}, bf16[128,1280]{1,0:T(8,128)(2,1)S(1)}, u32[]{:S(2)}, u32[]{:S(2)}) collective-permute-start(bf16[128,1280]{1,0:T(8,128)(2,1)} %get-tuple-element.41.refs_6_), channel_id=1, source_target_pairs={{0,4},{2,6},{4,0},{6,2},{1,5},{3,7},{5,1},{7,3},{8,12},{10,14},{12... | collective-permute-start | bytes 983048 | tf_op jit(solution)/shard_map/ppermute | solution.py:26
  26.9 10.5 %collective-permute-start.6 = (bf16[128,1280]{1,0:T(8,128)(2,1)}, bf16[128,1280]{1,0:T(8,128)(2,1)S(1)}, u32[]{:S(2)}, u32[]{:S(2)}) collective-permute-start(bf16[128,1280]{1,0:T(8,128)(2,1)} %get-tuple-element.41.refs_6_), channel_id=1, source_target_pairs={{0,2},{2,0},{4,6},{6,4},{1,3},{3,1},{5,7},{7,5},{8,10},{10,8},{12,... | collective-permute-start | bytes 983048 | tf_op jit(solution)/shard_map/ppermute | solution.py:26
  28.4 25.6 %collective-permute-start.14 = (bf16[128,1280]{1,0:T(8,128)(2,1)}, bf16[128,1280]{1,0:T(8,128)(2,1)S(1)}, u32[]{:S(2)}, u32[]{:S(2)}) collective-permute-start(bf16[128,1280]{1,0:T(8,128)(2,1)} %get-tuple-element.41.refs_6_), channel_id=1, source_target_pairs={{0,16},{8,24},{16,0},{24,8},{1,17},{9,25},{17,1},{25,9},{2,18},{10... | collective-permute-start | bytes 983048 | tf_op jit(solution)/shard_map/ppermute | solution.py:26
  31.8 22.9 %collective-permute-start.18 = (bf16[128,1280]{1,0:T(8,128)(2,1)}, bf16[128,1280]{1,0:T(8,128)(2,1)S(1)}, u32[]{:S(2)}, u32[]{:S(2)}) collective-permute-start(bf16[128,1280]{1,0:T(8,128)(2,1)} %get-tuple-element.42), channel_id=1, source_target_pairs={{0,24},{8,16},{16,8},{24,0},{1,25},{9,17},{17,9},{25,1},{2,26},{10... | collective-permute-start | bytes 983048 | tf_op jit(solution)/shard_map/ppermute | solution.py:26
  33.2 25.1 %collective-permute-start.27 = (bf16[384,512]{1,0:T(8,128)(2,1)S(1)}, bf16[384,512]{1,0:T(8,128)(2,1)S(1)}, u32[]{:S(2)}, u32[]{:S(2)}) collective-permute-start(bf16[384,512]{1,0:T(8,128)(2,1)S(1)} %shard_map.153.refs_3_), channel_id=1, source_target_pairs={{0,2},{2,0},{4,6},{6,4},{1,3},{3,1},{5,7},{7,5},{8,10},{10,8},{12,... | collective-permute-start | bytes 1179656 | tf_op jit(solution)/shard_map/ppermute | solution.py:26
  36.0 38.4 %collective-permute-start.1 = (bf16[256,1024]{1,0:T(8,128)(2,1)S(1)}, bf16[256,1024]{1,0:T(8,128)(2,1)S(1)}, u32[]{:S(2)}, u32[]{:S(2)}) collective-permute-start(bf16[256,1024]{1,0:T(8,128)(2,1)S(1)} %get-tuple-element.38.refs_0_), channel_id=1, source_target_pairs={{0,8},{8,0},{16,24},{24,16},{1,9},{9,1},{17,25},{25,17},{2,10},{10... | collective-permute-start | bytes 1572872 | tf_op jit(solution)/shard_map/ppermute | solution.py:26
  37.4 17.8 %collective-permute-start.3 = (bf16[16,1024]{1,0:T(8,128)(2,1)S(1)}, bf16[16,1024]{1,0:T(8,128)(2,1)S(1)}, u32[]{:S(2)}, u32[]{:S(2)}) collective-permute-start(bf16[16,1024]{1,0:T(8,128)(2,1)S(1)} %get-tuple-element.40), channel_id=1, source_target_pairs={{8,16},{9,17},{10,18},{11,19},{12,20},{13,21},{14,22},{15,23}} | collective-permute-start | bytes 98312 | tf_op jit(solution)/shard_map/ppermute | solution.py:31
  54.7 10.6 %collective-permute-start.10 = (bf16[128,1280]{1,0:T(8,128)(2,1)S(1)}, bf16[128,1280]{1,0:T(8,128)(2,1)S(1)}, u32[]{:S(2)}, u32[]{:S(2)}) collective-permute-start(bf16[128,1280]{1,0:T(8,128)(2,1)S(1)} %collective-permute-done.9.refs_10_), channel_id=1, source_target_pairs={{0,2},{2,0},{4,6},{6,4},{1,3},{3,1},{5,7},{7,5},{8,10},{10,8},{12,... | collective-permute-start | bytes 983048 | tf_op jit(solution)/shard_map/ppermute | solution.py:26
  55.2 17.1 %collective-permute-start.8 = (bf16[128,1280]{1,0:T(8,128)(2,1)S(1)}, bf16[128,1280]{1,0:T(8,128)(2,1)S(1)}, u32[]{:S(2)}, u32[]{:S(2)}) collective-permute-start(bf16[128,1280]{1,0:T(8,128)(2,1)S(1)} %collective-permute-done.7.refs_8_), channel_id=1, source_target_pairs={{0,2},{2,0},{4,6},{6,4},{1,3},{3,1},{5,7},{7,5},{8,10},{10,8},{12,... | collective-permute-start | bytes 983048 | tf_op jit(solution)/shard_map/ppermute | solution.py:26
  56.8 17.1 %collective-permute-start.11 = (bf16[128,1280]{1,0:T(8,128)(2,1)S(1)}, bf16[128,1280]{1,0:T(8,128)(2,1)S(1)}, u32[]{:S(2)}, u32[]{:S(2)}) collective-permute-start(bf16[128,1280]{1,0:T(8,128)(2,1)S(1)} %collective-permute-done.9.refs_10_), channel_id=1, source_target_pairs={{0,4},{2,6},{4,0},{6,2},{1,5},{3,7},{5,1},{7,3},{8,12},{10,14},{12... | collective-permute-start | bytes 983048 | tf_op jit(solution)/shard_map/ppermute | solution.py:26
  59.6 18.6 %collective-permute-start.15 = (bf16[128,1280]{1,0:T(8,128)(2,1)S(1)}, bf16[128,1280]{1,0:T(8,128)(2,1)S(1)}, u32[]{:S(2)}, u32[]{:S(2)}) collective-permute-start(bf16[128,1280]{1,0:T(8,128)(2,1)S(1)} %collective-permute-done.14.refs_6_.refs_5_), channel_id=1, source_target_pairs={{0,2},{2,0},{4,6},{6,4},{1,3},{3,1},{5,7},{7,5},{8,10},{10,8},{12,... | collective-permute-start | bytes 983048 | tf_op jit(solution)/shard_map/ppermute | solution.py:26
  65.3 14.6 %collective-permute-start.20 = (bf16[128,1280]{1,0:T(8,128)(2,1)S(1)}, bf16[128,1280]{1,0:T(8,128)(2,1)S(1)}, u32[]{:S(2)}, u32[]{:S(2)}) collective-permute-start(bf16[128,1280]{1,0:T(8,128)(2,1)S(1)} %collective-permute-done.18.refs_10_.refs_9_), channel_id=1, source_target_pairs={{0,4},{2,6},{4,0},{6,2},{1,5},{3,7},{5,1},{7,3},{8,12},{10,14},{12... | collective-permute-start | bytes 983048 | tf_op jit(solution)/shard_map/ppermute | solution.py:26
  72.3 9.1 %collective-permute-start.16 = (bf16[128,1280]{1,0:T(8,128)(2,1)S(1)}, bf16[128,1280]{1,0:T(8,128)(2,1)S(1)}, u32[]{:S(2)}, u32[]{:S(2)}) collective-permute-start(bf16[128,1280]{1,0:T(8,128)(2,1)S(1)} %collective-permute-done.14.refs_6_.refs_5_), channel_id=1, source_target_pairs={{0,4},{2,6},{4,0},{6,2},{1,5},{3,7},{5,1},{7,3},{8,12},{10,14},{12... | collective-permute-start | bytes 983048 | tf_op jit(solution)/shard_map/ppermute | solution.py:26
  73.9 10.6 %collective-permute-start.19 = (bf16[128,1280]{1,0:T(8,128)(2,1)S(1)}, bf16[128,1280]{1,0:T(8,128)(2,1)S(1)}, u32[]{:S(2)}, u32[]{:S(2)}) collective-permute-start(bf16[128,1280]{1,0:T(8,128)(2,1)S(1)} %collective-permute-done.18.refs_10_.refs_9_), channel_id=1, source_target_pairs={{0,2},{2,0},{4,6},{6,4},{1,3},{3,1},{5,7},{7,5},{8,10},{10,8},{12,... | collective-permute-start | bytes 983048 | tf_op jit(solution)/shard_map/ppermute | solution.py:26
  74.4 16.5 %collective-permute-start.2 = (bf16[256,1024]{1,0:T(8,128)(2,1)S(1)}, bf16[256,1024]{1,0:T(8,128)(2,1)S(1)}, u32[]{:S(2)}, u32[]{:S(2)}) collective-permute-start(bf16[256,1024]{1,0:T(8,128)(2,1)S(1)} %collective-permute-done.1.refs_2_), channel_id=1, source_target_pairs={{0,1},{1,0},{2,3},{3,2},{4,5},{5,4},{6,7},{7,6},{8,9},{9,8},{10,11... | collective-permute-start | bytes 1572872 | tf_op jit(solution)/shard_map/ppermute | solution.py:26
  78.2 10.6 %collective-permute-start.12 = (bf16[128,1280]{1,0:T(8,128)(2,1)S(1)}, bf16[128,1280]{1,0:T(8,128)(2,1)S(1)}, u32[]{:S(2)}, u32[]{:S(2)}) collective-permute-start(bf16[128,1280]{1,0:T(8,128)(2,1)S(1)} %collective-permute-done.10.refs_11_), channel_id=1, source_target_pairs={{0,4},{2,6},{4,0},{6,2},{1,5},{3,7},{5,1},{7,3},{8,12},{10,14},{12... | collective-permute-start | bytes 983048 | tf_op jit(solution)/shard_map/ppermute | solution.py:26
  79.9 15.9 %collective-permute-start.17 = (bf16[128,1280]{1,0:T(8,128)(2,1)S(1)}, bf16[128,1280]{1,0:T(8,128)(2,1)S(1)}, u32[]{:S(2)}, u32[]{:S(2)}) collective-permute-start(bf16[128,1280]{1,0:T(8,128)(2,1)S(1)} %collective-permute-done.15.refs_7_.refs_6_), channel_id=1, source_target_pairs={{0,4},{2,6},{4,0},{6,2},{1,5},{3,7},{5,1},{7,3},{8,12},{10,14},{12... | collective-permute-start | bytes 983048 | tf_op jit(solution)/shard_map/ppermute | solution.py:26
  81.4 14.4 %collective-permute-start.21 = (bf16[128,1280]{1,0:T(8,128)(2,1)S(1)}, bf16[128,1280]{1,0:T(8,128)(2,1)S(1)}, u32[]{:S(2)}, u32[]{:S(2)}) collective-permute-start(bf16[128,1280]{1,0:T(8,128)(2,1)S(1)} %collective-permute-done.20.refs_12_.refs_11_), channel_id=1, source_target_pairs={{0,2},{2,0},{4,6},{6,4},{1,3},{3,1},{5,7},{7,5},{8,10},{10,8},{12,... | collective-permute-start | bytes 983048 | tf_op jit(solution)/shard_map/ppermute | solution.py:26
  84.5 28.6 %collective-permute-start.35 = (bf16[384,512]{1,0:T(8,128)(2,1)S(1)}, bf16[384,512]{1,0:T(8,128)(2,1)S(1)}, u32[]{:S(2)}, u32[]{:S(2)}) collective-permute-start(bf16[384,512]{1,0:T(8,128)(2,1)S(1)} %collective-permute-done.27.refs_4_), channel_id=1, source_target_pairs={{0,4},{2,6},{4,0},{6,2},{1,5},{3,7},{5,1},{7,3},{8,12},{10,14},{12... | collective-permute-start | bytes 1179656 | tf_op jit(solution)/shard_map/ppermute | solution.py:26
  88.8 30.8 %collective-permute-start.31 = (bf16[384,512]{1,0:T(8,128)(2,1)S(1)}, bf16[384,512]{1,0:T(8,128)(2,1)S(1)}, u32[]{:S(2)}, u32[]{:S(2)}) collective-permute-start(bf16[384,512]{1,0:T(8,128)(2,1)S(1)} %shard_map.153.refs_3_), channel_id=1, source_target_pairs={{0,4},{2,6},{4,0},{6,2},{1,5},{3,7},{5,1},{7,3},{8,12},{10,14},{12... | collective-permute-start | bytes 1179656 | tf_op jit(solution)/shard_map/ppermute | solution.py:26
  90.9 22.2 %collective-permute-start.34 = (bf16[128,512]{1,0:T(8,128)(2,1)S(1)}, bf16[128,512]{1,0:T(8,128)(2,1)S(1)}, u32[]{:S(2)}, u32[]{:S(2)}) collective-permute-start(bf16[128,512]{1,0:T(8,128)(2,1)S(1)} %collective-permute-done.23.refs_2_), channel_id=1, source_target_pairs={{0,4},{2,6},{4,0},{6,2},{1,5},{3,7},{5,1},{7,3},{8,12},{10,14},{12... | collective-permute-start | bytes 393224 | tf_op jit(solution)/shard_map/ppermute | solution.py:26
  98.8 11.2 %collective-permute-start.22 = (bf16[2,128,128]{2,1,0:T(8,128)(2,1)S(1)}, bf16[2,128,128]{2,1,0:T(8,128)(2,1)S(1)}, u32[]{:S(2)}, u32[]{:S(2)}) collective-permute-start(bf16[2,128,128]{2,1,0:T(8,128)(2,1)S(1)} %get-tuple-element.53), channel_id=1, source_target_pairs={{0,16},{8,24},{1,17},{9,25},{2,18},{10,26},{3,19},{11,27},{4,20},{... | collective-permute-start | bytes 196616 | tf_op jit(solution)/shard_map/ppermute | solution.py:31
  111.8 14.4 %collective-permute-start.28 = (bf16[256,1024]{1,0:T(8,128)(2,1)S(1)}, bf16[256,1024]{1,0:T(8,128)(2,1)S(1)}, u32[]{:S(2)}, u32[]{:S(2)}) collective-permute-start(bf16[256,1024]{1,0:T(8,128)(2,1)S(1)} %get-tuple-element.61), channel_id=1, source_target_pairs={{0,1},{1,0},{2,3},{3,2},{4,5},{5,4},{6,7},{7,6},{8,9},{9,8},{10,11... | collective-permute-start | bytes 1572872 | tf_op jit(solution)/shard_map/ppermute | solution.py:26
  113.6 7.8 %collective-permute-start.36 = (bf16[256,512]{1,0:T(8,128)(2,1)S(1)}, bf16[256,512]{1,0:T(8,128)(2,1)S(1)}, u32[]{:S(2)}, u32[]{:S(2)}) collective-permute-start(bf16[256,512]{1,0:T(8,128)(2,1)S(1)} %get-tuple-element.69), channel_id=1, source_target_pairs={{0,1},{1,0},{2,3},{3,2},{4,5},{5,4},{6,7},{7,6},{8,9},{9,8},{10,11... | collective-permute-start | bytes 786440 | tf_op jit(solution)/shard_map/ppermute | solution.py:26
  121.5 9.0 %collective-permute-start.37 = (bf16[128,512]{1,0:T(8,128)(2,1)S(1)}, bf16[128,512]{1,0:T(8,128)(2,1)S(1)}, u32[]{:S(2)}, u32[]{:S(2)}) collective-permute-start(bf16[128,512]{1,0:T(8,128)(2,1)S(1)} %add_convert_fusion.1), channel_id=1, source_target_pairs={{0,8},{8,0},{16,24},{24,16},{1,9},{9,1},{17,25},{25,17},{2,10},{10... | collective-permute-start | bytes 393224 | tf_op jit(solution)/shard_map/ppermute | solution.py:26
  126.2 12.5 %collective-permute-start.29 = (bf16[128,1024]{1,0:T(8,128)(2,1)S(1)}, bf16[128,1024]{1,0:T(8,128)(2,1)S(1)}, u32[]{:S(2)}, u32[]{:S(2)}) collective-permute-start(bf16[128,1024]{1,0:T(8,128)(2,1)S(1)} %add_convert_fusion), channel_id=1, source_target_pairs={{0,8},{8,0},{16,24},{24,16},{1,9},{9,1},{17,25},{25,17},{2,10},{10... | collective-permute-start | bytes 786440 | tf_op jit(solution)/shard_map/ppermute | solution.py:26
  126.3 12.4 %collective-permute-start.33 = (bf16[128,512]{1,0:T(8,128)(2,1)S(1)}, bf16[128,512]{1,0:T(8,128)(2,1)S(1)}, u32[]{:S(2)}, u32[]{:S(2)}) collective-permute-start(bf16[128,512]{1,0:T(8,128)(2,1)S(1)} %add_convert_fusion.2), channel_id=1, source_target_pairs={{0,8},{8,0},{16,24},{24,16},{1,9},{9,1},{17,25},{25,17},{2,10},{10... | collective-permute-start | bytes 393224 | tf_op jit(solution)/shard_map/ppermute | solution.py:26
  (16 other events, 219.0 us)

commit v2 on v1

--- a/solution.py
+++ b/solution.py
@@ -57,12 +57,16 @@
             (plane,) = call(stack_kernel, [(shape, BF16)], *(arrived[d] for d in group))
         by_x = swapped(plane, "fs", 1)
         by_y = swapped(plane, "fs", 2)
+        pieces += [(plane, 0, tuple(group)), (by_x, 1, tuple(group)), (by_y, 2, tuple(group))]
         if route == "x":
-            across = swapped(by_y, "fs", 1)
+            pieces.append((swapped(by_y, "fs", 1), 3, tuple(group)))
+        elif route == "y":
+            pieces.append((swapped(by_x, "fs", 2), 3, tuple(group)))
         else:
-            across = swapped(by_x, "fs", 2)
-        for c, piece in enumerate((plane, by_x, by_y, across)):
-            pieces.append((piece, c, tuple(group)))
+            count = (len(group) + 1) // 2
+            cut = by_x.shape[0] // len(group) * count
+            pieces.append((swapped(by_x[:cut], "fs", 2), 3, tuple(group[:count])))
+            pieces.append((swapped(by_y[cut:], "fs", 1), 3, tuple(group[count:])))
     return pieces
 
 
@@ -413,7 +417,7 @@
     mix_pieces = over_plane(line_a, fine, "xyyx")
     first_shards, first_where = split([p for p in mix_pieces if p[2][0] < PAIR])
     mix_shards, mix_where = split([p for p in mix_pieces if p[2][0] >= PAIR])
-    out_pieces = over_plane(line_c, [[0], list(range(1, n_sp))], "yy")
+    out_pieces = over_plane(line_c, [[0], list(range(1, n_sp))], "xb")
     near_other = swapped(near, "tp", 1)
     wide = PAIR * n_fs * rows
     normed, earlier = call(

time: 140 us -> 143 us (1.021)
  starting transfers between devices: 54.9 us -> 61 us
  waiting for transfers between devices: 64.9 us -> 62.8 us
    ppermute x3, starting transfers between devices: 10.2 us -> 15.9 us  [passed_on(): lax.ppermute(value, axis, [(i, i + steps) for i in range(first, count - s...]
    ppermute x35 -> x36, waiting for transfers between devices: 64.9 us -> 62.8 us  [swapped(): return lax.ppermute(value, axis, [(i, i ^ distance) for i in range(count)])]
    ppermute x35 -> x36, starting transfers between devices: 44.7 us -> 45.2 us  [swapped(): return lax.ppermute(value, axis, [(i, i ^ distance) for i in range(count)])]
  transfers between devices with their start and end apart: 38 -> 39, of which waited for: 17 -> 14; matrix products, arithmetic and copies ran while one was open for 0% -> 0% of each run, Pallas kernels for 11% -> 10%
where the time goes in v2:
time: 143 us
  waiting for transfers between devices  62.8 us (44%)
  starting transfers between devices  61 us (43%)
  Pallas kernels  16.7 us (12%)
  local copies, waits for them, and re-layouts  1.81 us (1%)
    ppermute x36, waiting for transfers between devices, swapped(): return lax.ppermute(value, axis, [(i, i ^ distance) for i in range(count)])  62.8 us
    ppermute x36, starting transfers between devices, swapped(): return lax.ppermute(value, axis, [(i, i ^ distance) for i in range(count)])  45.2 us
    pallas_call x16, Pallas kernels, call(): pl.pallas_call(kernel, out_shape=[jax.ShapeDtypeStruct(shape, dtype) for...  16.7 us
    ppermute x3, starting transfers between devices, passed_on(): lax.ppermute(value, axis, [(i, i + steps) for i in range(first, count - s...  15.9 us
  transfers between devices with their start and end apart: 39, of which 14 were waited for; matrix products, arithmetic and copies ran while one was open for 0% of the time, Pallas kernels for 10%

profile of v2, /device:TPU:0, one launch (start us, length us, event | category | flops | bytes accessed | tf_op | source)
XLA Modules:
  0.0 142.8 jit_solution(8028844773564750766)
XLA Ops:
  0.0 1.8 %shard_map.152 = (bf16[128,512]{1,0:T(8,128)(2,1)}, bf16[128,512]{1,0:T(8,128)(2,1)}) custom-call(bf16[512,128]{1,0:T(8,128)(2,1)} %refs_0_.3, bf16[512,128]{1,0:T(8,128)(2,1)} %refs_1_.3), custom_call_target="tpu_custom_call" | custom-call | tf_op jit(solution)/shard_map/pallas_call | solution.py:37
  1.8 4.1 %collective-permute-start.25 = (bf16[128,512]{1,0:T(8,128)(2,1)}, bf16[128,512]{1,0:T(8,128)(2,1)S(1)}, u32[]{:S(2)}, u32[]{:S(2)}) collective-permute-start(bf16[128,512]{1,0:T(8,128)(2,1)} %get-tuple-element.57.refs_1_), channel_id=1, source_target_pairs={{0,16},{8,24},{16,0},{24,8},{1,17},{9,25},{17,1},{25,9},{2,18},{10... | collective-permute-start | bytes 393224 | tf_op jit(solution)/shard_map/ppermute | solution.py:26
  5.9 2.0 %shard_map.147 = (bf16[128,1280]{1,0:T(8,128)(2,1)}, bf16[128,1280]{1,0:T(8,128)(2,1)}) custom-call(bf16[128,512]{1,0:T(8,128)(2,1)} %refs_0_.2, bf16[128,512]{1,0:T(8,128)(2,1)} %refs_1_.2, bf16[128,512]{1,0:T(8,128)(2,1)} %refs_2_.1, bf16[128,512]{1,0:T(8,128)(2,1)} %refs_3_.1, bf16[128,512]{1,0:T(8,128)(2,1)} %refs_4_.1), custom_call_target="tpu_custom_call" | custom-call | tf_op jit(solution)/shard_map/pallas_call | solution.py:37
  8.0 1.6 %collective-permute-start.9 = (bf16[128,1280]{1,0:T(8,128)(2,1)}, bf16[128,1280]{1,0:T(8,128)(2,1)S(1)}, u32[]{:S(2)}, u32[]{:S(2)}) collective-permute-start(bf16[128,1280]{1,0:T(8,128)(2,1)} %get-tuple-element.42), channel_id=1, source_target_pairs={{0,8},{8,0},{16,24},{24,16},{1,9},{9,1},{17,25},{25,17},{2,10},{10... | collective-permute-start | bytes 983048 | tf_op jit(solution)/shard_map/ppermute | solution.py:26
  10.1 1.6 %collective-permute-start.24 = (bf16[128,512]{1,0:T(8,128)(2,1)}, bf16[128,512]{1,0:T(8,128)(2,1)S(1)}, u32[]{:S(2)}, u32[]{:S(2)}) collective-permute-start(bf16[128,512]{1,0:T(8,128)(2,1)} %get-tuple-element.58), channel_id=1, source_target_pairs={{0,8},{8,0},{16,24},{24,16},{1,9},{9,1},{17,25},{25,17},{2,10},{10... | collective-permute-start | bytes 393224 | tf_op jit(solution)/shard_map/ppermute | solution.py:26
  11.7 7.9 %collective-permute-done.13.refs_4_ = f32[4,256]{1,0:T(4,128)S(1)} collective-permute-done((f32[4,256]{1,0:T(4,128)}, f32[4,256]{1,0:T(4,128)S(1)}, u32[]{:S(2)}, u32[]{:S(2)}) %collective-permute-start.13) | collective-permute-done | bytes 4128 | tf_op jit(solution)/shard_map/ppermute | solution.py:26
  19.6 1.6 %collective-permute-start.7 = (bf16[128,1280]{1,0:T(8,128)(2,1)}, bf16[128,1280]{1,0:T(8,128)(2,1)S(1)}, u32[]{:S(2)}, u32[]{:S(2)}) collective-permute-start(bf16[128,1280]{1,0:T(8,128)(2,1)} %get-tuple-element.41.refs_6_), channel_id=1, source_target_pairs={{0,4},{2,6},{4,0},{6,2},{1,5},{3,7},{5,1},{7,3},{8,12},{10,14},{12... | collective-permute-start | bytes 983048 | tf_op jit(solution)/shard_map/ppermute | solution.py:26
  21.2 3.3 %collective-permute-start.26 = (bf16[128,512]{1,0:T(8,128)(2,1)}, bf16[128,512]{1,0:T(8,128)(2,1)S(1)}, u32[]{:S(2)}, u32[]{:S(2)}) collective-permute-start(bf16[128,512]{1,0:T(8,128)(2,1)} %get-tuple-element.58), channel_id=1, source_target_pairs={{0,24},{8,16},{16,8},{24,0},{1,25},{9,17},{17,9},{25,1},{2,26},{10... | collective-permute-start | bytes 393224 | tf_op jit(solution)/shard_map/ppermute | solution.py:26
  25.0 3.4 %collective-permute-done.26.refs_2_ = bf16[128,512]{1,0:T(8,128)(2,1)S(1)} collective-permute-done((bf16[128,512]{1,0:T(8,128)(2,1)}, bf16[128,512]{1,0:T(8,128)(2,1)S(1)}, u32[]{:S(2)}, u32[]{:S(2)}) %collective-permute-start.26) | collective-permute-done | bytes 131104 | tf_op jit(solution)/shard_map/ppermute | solution.py:26
  29.9 2.3 %collective-permute-done.30.refs_1_ = bf16[128,512]{1,0:T(8,128)(2,1)S(1)} collective-permute-done((bf16[128,512]{1,0:T(8,128)(2,1)}, bf16[128,512]{1,0:T(8,128)(2,1)S(1)}, u32[]{:S(2)}, u32[]{:S(2)}) %collective-permute-start.30) | collective-permute-done | bytes 131104 | tf_op jit(solution)/shard_map/ppermute | solution.py:26
  32.9 1.9 %collective-permute-start.18 = (bf16[128,1280]{1,0:T(8,128)(2,1)}, bf16[128,1280]{1,0:T(8,128)(2,1)S(1)}, u32[]{:S(2)}, u32[]{:S(2)}) collective-permute-start(bf16[128,1280]{1,0:T(8,128)(2,1)} %get-tuple-element.42), channel_id=1, source_target_pairs={{0,24},{8,16},{16,8},{24,0},{1,25},{9,17},{17,9},{25,1},{2,26},{10... | collective-permute-start | bytes 983048 | tf_op jit(solution)/shard_map/ppermute | solution.py:26
  34.9 1.6 %collective-permute-start.27 = (bf16[384,512]{1,0:T(8,128)(2,1)S(1)}, bf16[384,512]{1,0:T(8,128)(2,1)S(1)}, u32[]{:S(2)}, u32[]{:S(2)}) collective-permute-start(bf16[384,512]{1,0:T(8,128)(2,1)S(1)} %shard_map.153.refs_3_), channel_id=1, source_target_pairs={{0,2},{2,0},{4,6},{6,4},{1,3},{3,1},{5,7},{7,5},{8,10},{10,8},{12,... | collective-permute-start | bytes 1179656 | tf_op jit(solution)/shard_map/ppermute | solution.py:26
  36.4 1.5 %collective-permute-start.31 = (bf16[384,512]{1,0:T(8,128)(2,1)S(1)}, bf16[384,512]{1,0:T(8,128)(2,1)S(1)}, u32[]{:S(2)}, u32[]{:S(2)}) collective-permute-start(bf16[384,512]{1,0:T(8,128)(2,1)S(1)} %shard_map.153.refs_3_), channel_id=1, source_target_pairs={{0,4},{2,6},{4,0},{6,2},{1,5},{3,7},{5,1},{7,3},{8,12},{10,14},{12... | collective-permute-start | bytes 1179656 | tf_op jit(solution)/shard_map/ppermute | solution.py:26
  41.2 14.3 %collective-permute-done.14.refs_6_.refs_5_ = bf16[128,1280]{1,0:T(8,128)(2,1)S(1)} collective-permute-done((bf16[128,1280]{1,0:T(8,128)(2,1)}, bf16[128,1280]{1,0:T(8,128)(2,1)S(1)}, u32[]{:S(2)}, u32[]{:S(2)}) %collective-permute-start.14) | collective-permute-done | bytes 327712 | tf_op jit(solution)/shard_map/ppermute | solution.py:26
  58.8 1.6 %collective-permute-start.11 = (bf16[128,1280]{1,0:T(8,128)(2,1)S(1)}, bf16[128,1280]{1,0:T(8,128)(2,1)S(1)}, u32[]{:S(2)}, u32[]{:S(2)}) collective-permute-start(bf16[128,1280]{1,0:T(8,128)(2,1)S(1)} %collective-permute-done.9.refs_10_), channel_id=1, source_target_pairs={{0,4},{2,6},{4,0},{6,2},{1,5},{3,7},{5,1},{7,3},{8,12},{10,14},{12... | collective-permute-start | bytes 983048 | tf_op jit(solution)/shard_map/ppermute | solution.py:26
  63.2 2.8 %collective-permute-done.10.refs_11_ = bf16[128,1280]{1,0:T(8,128)(2,1)S(1)} collective-permute-done((bf16[128,1280]{1,0:T(8,128)(2,1)S(1)}, bf16[128,1280]{1,0:T(8,128)(2,1)S(1)}, u32[]{:S(2)}, u32[]{:S(2)}) %collective-permute-start.10) | collective-permute-done | bytes 327712 | tf_op jit(solution)/shard_map/ppermute | solution.py:26
  66.0 1.5 %collective-permute-start.20 = (bf16[128,1280]{1,0:T(8,128)(2,1)S(1)}, bf16[128,1280]{1,0:T(8,128)(2,1)S(1)}, u32[]{:S(2)}, u32[]{:S(2)}) collective-permute-start(bf16[128,1280]{1,0:T(8,128)(2,1)S(1)} %collective-permute-done.18.refs_10_.refs_9_), channel_id=1, source_target_pairs={{0,4},{2,6},{4,0},{6,2},{1,5},{3,7},{5,1},{7,3},{8,12},{10,14},{12... | collective-permute-start | bytes 983048 | tf_op jit(solution)/shard_map/ppermute | solution.py:26
  67.5 5.5 %collective-permute-done.8.refs_9_ = bf16[128,1280]{1,0:T(8,128)(2,1)S(1)} collective-permute-done((bf16[128,1280]{1,0:T(8,128)(2,1)S(1)}, bf16[128,1280]{1,0:T(8,128)(2,1)S(1)}, u32[]{:S(2)}, u32[]{:S(2)}) %collective-permute-start.8) | collective-permute-done | bytes 327712 | tf_op jit(solution)/shard_map/ppermute | solution.py:26
  73.0 1.5 %collective-permute-start.16 = (bf16[128,1280]{1,0:T(8,128)(2,1)S(1)}, bf16[128,1280]{1,0:T(8,128)(2,1)S(1)}, u32[]{:S(2)}, u32[]{:S(2)}) collective-permute-start(bf16[128,1280]{1,0:T(8,128)(2,1)S(1)} %collective-permute-done.14.refs_6_.refs_5_), channel_id=1, source_target_pairs={{0,4},{2,6},{4,0},{6,2},{1,5},{3,7},{5,1},{7,3},{8,12},{10,14},{12... | collective-permute-start | bytes 983048 | tf_op jit(solution)/shard_map/ppermute | solution.py:26
  74.6 1.6 %collective-permute-start.19 = (bf16[128,1280]{1,0:T(8,128)(2,1)S(1)}, bf16[128,1280]{1,0:T(8,128)(2,1)S(1)}, u32[]{:S(2)}, u32[]{:S(2)}) collective-permute-start(bf16[128,1280]{1,0:T(8,128)(2,1)S(1)} %collective-permute-done.18.refs_10_.refs_9_), channel_id=1, source_target_pairs={{0,2},{2,0},{4,6},{6,4},{1,3},{3,1},{5,7},{7,5},{8,10},{10,8},{12,... | collective-permute-start | bytes 983048 | tf_op jit(solution)/shard_map/ppermute | solution.py:26
  76.1 3.9 %collective-permute-done.15.refs_7_.refs_6_ = bf16[128,1280]{1,0:T(8,128)(2,1)S(1)} collective-permute-done((bf16[128,1280]{1,0:T(8,128)(2,1)S(1)}, bf16[128,1280]{1,0:T(8,128)(2,1)S(1)}, u32[]{:S(2)}, u32[]{:S(2)}) %collective-permute-start.15) | collective-permute-done | bytes 327712 | tf_op jit(solution)/shard_map/ppermute | solution.py:26
  84.6 2.4 %collective-permute-done.19.refs_11_.refs_10_ = bf16[128,1280]{1,0:T(8,128)(2,1)S(1)} collective-permute-done((bf16[128,1280]{1,0:T(8,128)(2,1)S(1)}, bf16[128,1280]{1,0:T(8,128)(2,1)S(1)}, u32[]{:S(2)}, u32[]{:S(2)}) %collective-permute-start.19) | collective-permute-done | bytes 327712 | tf_op jit(solution)/shard_map/ppermute | solution.py:26
  88.6 2.0 %collective-permute-done.12.refs_13_ = bf16[128,1280]{1,0:T(8,128)(2,1)S(1)} collective-permute-done((bf16[128,1280]{1,0:T(8,128)(2,1)S(1)}, bf16[128,1280]{1,0:T(8,128)(2,1)S(1)}, u32[]{:S(2)}, u32[]{:S(2)}) %collective-permute-start.12) | collective-permute-done | bytes 327712 | tf_op jit(solution)/shard_map/ppermute | solution.py:26
  92.1 5.5 %collective-permute-done.17.refs_9_.refs_8_ = bf16[128,1280]{1,0:T(8,128)(2,1)S(1)} collective-permute-done((bf16[128,1280]{1,0:T(8,128)(2,1)S(1)}, bf16[128,1280]{1,0:T(8,128)(2,1)S(1)}, u32[]{:S(2)}, u32[]{:S(2)}) %collective-permute-start.17) | collective-permute-done | bytes 327712 | tf_op jit(solution)/shard_map/ppermute | solution.py:26
  99.7 1.9 %shard_map.148 = (bf16[528,2048]{1,0:T(8,128)(2,1)S(1)}, f32[528,1280]{1,0:T(8,128)S(1)}) custom-call(bf16[256,1024]{1,0:T(8,128)(2,1)S(1)} %get-tuple-element.38.refs_0_, bf16[256,1024]{1,0:T(8,128)(2,1)S(1)} %get-tuple-element.39.refs_1_, bf16[256,1024]{1,0:T(8,128)(2,1)S(1)} %collective-permute-done.1.refs_2_, ...), custom_call_target="tpu_custom_call" | custom-call | tf_op jit(solution)/shard_map/pallas_call | solution.py:37
  101.6 3.0 %shard_map.149 = (bf16[512,256]{1,0:T(8,128)(2,1)S(1)}, f32[512,256]{1,0:T(8,128)S(1)}, f32[512,256]{1,0:T(8,128)S(1)}, f32[4,2,128,128]{3,2,1,0:T(8,128)S(1)}, ...) custom-call(bf16[528,2048]{1,0:T(8,128)(2,1)S(1)} %get-tuple-element, ...), custom_call_target="tpu_custom_call" | custom-call | tf_op jit(solution)/shard_map/pallas_call | solution.py:37
  104.6 14.6 %collective-permute-start.22 = (bf16[2,128,128]{2,1,0:T(8,128)(2,1)S(1)}, bf16[2,128,128]{2,1,0:T(8,128)(2,1)S(1)}, u32[]{:S(2)}, u32[]{:S(2)}) collective-permute-start(bf16[2,128,128]{2,1,0:T(8,128)(2,1)S(1)} %get-tuple-element.53), channel_id=1, source_target_pairs={{0,16},{8,24},{1,17},{9,25},{2,18},{10,26},{3,19},{11,27},{4,20},{... | collective-permute-start | bytes 196616 | tf_op jit(solution)/shard_map/ppermute | solution.py:31
  119.2 2.2 %shard_map.150 = (f32[512,256]{1,0:T(8,128)S(1)}, bf16[512,256]{1,0:T(8,128)(2,1)S(1)}, bf16[512,256]{1,0:T(8,128)(2,1)S(1)}, bf16[512,256]{1,0:T(8,128)(2,1)S(1)}, bf16[16,256]{1,0:T(8,128)(2,1)S(1)}) custom-call(bf16[528,2048]{1,0:T(8,128)(2,1)S(1)} %get-tuple-element.43.refs_0_, f32[528,1280]{1,0:T(8,128)S(1)} %get-tuple-element.44.refs_1_, ...), custom_call_target="tpu_custom_call" | custom-call | tf_op jit(solution)/shard_map/pallas_call | solution.py:37
  126.7 2.6 %collective-permute-start.38 = (bf16[128,512]{1,0:T(8,128)(2,1)S(1)}, bf16[128,512]{1,0:T(8,128)(2,1)S(1)}, u32[]{:S(2)}, u32[]{:S(2)}) collective-permute-start(bf16[128,512]{1,0:T(8,128)(2,1)S(1)} %add_convert_fusion.1), channel_id=1, source_target_pairs={{0,8},{8,0},{16,24},{24,16},{1,9},{9,1},{17,25},{25,17},{2,10},{10... | collective-permute-start | bytes 393224 | tf_op jit(solution)/shard_map/ppermute | solution.py:26
  129.5 2.1 %collective-permute-start.33 = (bf16[128,512]{1,0:T(8,128)(2,1)S(1)}, bf16[128,512]{1,0:T(8,128)(2,1)S(1)}, u32[]{:S(2)}, u32[]{:S(2)}) collective-permute-start(bf16[128,512]{1,0:T(8,128)(2,1)S(1)} %add_convert_fusion.2), channel_id=1, source_target_pairs={{0,8},{8,0},{16,24},{24,16},{1,9},{9,1},{17,25},{25,17},{2,10},{10... | collective-permute-start | bytes 393224 | tf_op jit(solution)/shard_map/ppermute | solution.py:26
  131.5 2.1 %collective-permute-done.38.refs_8_ = bf16[128,512]{1,0:T(8,128)(2,1)S(1)} collective-permute-done((bf16[128,512]{1,0:T(8,128)(2,1)S(1)}, bf16[128,512]{1,0:T(8,128)(2,1)S(1)}, u32[]{:S(2)}, u32[]{:S(2)}) %collective-permute-start.38) | collective-permute-done | bytes 131104 | tf_op jit(solution)/shard_map/ppermute | solution.py:26
  133.6 8.2 %collective-permute-done.33.refs_5_ = bf16[128,512]{1,0:T(8,128)(2,1)S(1)} collective-permute-done((bf16[128,512]{1,0:T(8,128)(2,1)S(1)}, bf16[128,512]{1,0:T(8,128)(2,1)S(1)}, u32[]{:S(2)}, u32[]{:S(2)}) %collective-permute-start.33) | collective-permute-done | bytes 131104 | tf_op jit(solution)/shard_map/ppermute | solution.py:26
  (87 shorter events, 28.4 us)
Async XLA Ops:
  1.8 19.4 %collective-permute-start.25 = (bf16[128,512]{1,0:T(8,128)(2,1)}, bf16[128,512]{1,0:T(8,128)(2,1)S(1)}, u32[]{:S(2)}, u32[]{:S(2)}) collective-permute-start(bf16[128,512]{1,0:T(8,128)(2,1)} %get-tuple-element.57.refs_1_), channel_id=1, source_target_pairs={{0,16},{8,24},{16,0},{24,8},{1,17},{9,25},{17,1},{25,9},{2,18},{10... | collective-permute-start | bytes 393224 | tf_op jit(solution)/shard_map/ppermute | solution.py:26
  5.9 30.5 %collective-permute-start = (bf16[256,1024]{1,0:T(8,128)(2,1)}, bf16[256,1024]{1,0:T(8,128)(2,1)S(1)}, u32[]{:S(2)}, u32[]{:S(2)}) collective-permute-start(bf16[256,1024]{1,0:T(8,128)(2,1)} %bitcast.10), channel_id=1, source_target_pairs={{0,1},{1,0},{2,3},{3,2},{4,5},{5,4},{6,7},{7,6},{8,9},{9,8},{10,11... | collective-permute-start | bytes 1572872 | tf_op jit(solution)/shard_map/ppermute | solution.py:26
  8.0 24.9 %collective-permute-start.9 = (bf16[128,1280]{1,0:T(8,128)(2,1)}, bf16[128,1280]{1,0:T(8,128)(2,1)S(1)}, u32[]{:S(2)}, u32[]{:S(2)}) collective-permute-start(bf16[128,1280]{1,0:T(8,128)(2,1)} %get-tuple-element.42), channel_id=1, source_target_pairs={{0,8},{8,0},{16,24},{24,16},{1,9},{9,1},{17,25},{25,17},{2,10},{10... | collective-permute-start | bytes 983048 | tf_op jit(solution)/shard_map/ppermute | solution.py:26
  9.6 10.0 %collective-permute-start.13 = (f32[4,256]{1,0:T(4,128)}, f32[4,256]{1,0:T(4,128)S(1)}, u32[]{:S(2)}, u32[]{:S(2)}) collective-permute-start(f32[4,256]{1,0:T(4,128)} %bitcast.14), channel_id=1, source_target_pairs={{0,8},{8,0},{16,24},{24,16},{1,9},{9,1},{17,25},{25,17},{2,10},{10... | collective-permute-start | bytes 12296 | tf_op jit(solution)/shard_map/ppermute | solution.py:26
  10.1 14.4 %collective-permute-start.24 = (bf16[128,512]{1,0:T(8,128)(2,1)}, bf16[128,512]{1,0:T(8,128)(2,1)S(1)}, u32[]{:S(2)}, u32[]{:S(2)}) collective-permute-start(bf16[128,512]{1,0:T(8,128)(2,1)} %get-tuple-element.58), channel_id=1, source_target_pairs={{0,8},{8,0},{16,24},{24,16},{1,9},{9,1},{17,25},{25,17},{2,10},{10... | collective-permute-start | bytes 393224 | tf_op jit(solution)/shard_map/ppermute | solution.py:26
  19.6 15.3 %collective-permute-start.7 = (bf16[128,1280]{1,0:T(8,128)(2,1)}, bf16[128,1280]{1,0:T(8,128)(2,1)S(1)}, u32[]{:S(2)}, u32[]{:S(2)}) collective-permute-start(bf16[128,1280]{1,0:T(8,128)(2,1)} %get-tuple-element.41.refs_6_), channel_id=1, source_target_pairs={{0,4},{2,6},{4,0},{6,2},{1,5},{3,7},{5,1},{7,3},{8,12},{10,14},{12... | collective-permute-start | bytes 983048 | tf_op jit(solution)/shard_map/ppermute | solution.py:26
  21.2 7.3 %collective-permute-start.26 = (bf16[128,512]{1,0:T(8,128)(2,1)}, bf16[128,512]{1,0:T(8,128)(2,1)S(1)}, u32[]{:S(2)}, u32[]{:S(2)}) collective-permute-start(bf16[128,512]{1,0:T(8,128)(2,1)} %get-tuple-element.58), channel_id=1, source_target_pairs={{0,24},{8,16},{16,8},{24,0},{1,25},{9,17},{17,9},{25,1},{2,26},{10... | collective-permute-start | bytes 393224 | tf_op jit(solution)/shard_map/ppermute | solution.py:26
  24.5 7.7 %collective-permute-start.30 = (bf16[128,512]{1,0:T(8,128)(2,1)}, bf16[128,512]{1,0:T(8,128)(2,1)S(1)}, u32[]{:S(2)}, u32[]{:S(2)}) collective-permute-start(bf16[128,512]{1,0:T(8,128)(2,1)} %get-tuple-element.57.refs_1_), channel_id=1, source_target_pairs={{0,4},{2,6},{4,0},{6,2},{1,5},{3,7},{5,1},{7,3},{8,12},{10,14},{12... | collective-permute-start | bytes 393224 | tf_op jit(solution)/shard_map/ppermute | solution.py:26
  28.4 11.7 %collective-permute-start.6 = (bf16[128,1280]{1,0:T(8,128)(2,1)}, bf16[128,1280]{1,0:T(8,128)(2,1)S(1)}, u32[]{:S(2)}, u32[]{:S(2)}) collective-permute-start(bf16[128,1280]{1,0:T(8,128)(2,1)} %get-tuple-element.41.refs_6_), channel_id=1, source_target_pairs={{0,2},{2,0},{4,6},{6,4},{1,3},{3,1},{5,7},{7,5},{8,10},{10,8},{12,... | collective-permute-start | bytes 983048 | tf_op jit(solution)/shard_map/ppermute | solution.py:26
  32.3 23.2 %collective-permute-start.14 = (bf16[128,1280]{1,0:T(8,128)(2,1)}, bf16[128,1280]{1,0:T(8,128)(2,1)S(1)}, u32[]{:S(2)}, u32[]{:S(2)}) collective-permute-start(bf16[128,1280]{1,0:T(8,128)(2,1)} %get-tuple-element.41.refs_6_), channel_id=1, source_target_pairs={{0,16},{8,24},{16,0},{24,8},{1,17},{9,25},{17,1},{25,9},{2,18},{10... | collective-permute-start | bytes 983048 | tf_op jit(solution)/shard_map/ppermute | solution.py:26
  32.9 24.0 %collective-permute-start.18 = (bf16[128,1280]{1,0:T(8,128)(2,1)}, bf16[128,1280]{1,0:T(8,128)(2,1)S(1)}, u32[]{:S(2)}, u32[]{:S(2)}) collective-permute-start(bf16[128,1280]{1,0:T(8,128)(2,1)} %get-tuple-element.42), channel_id=1, source_target_pairs={{0,24},{8,16},{16,8},{24,0},{1,25},{9,17},{17,9},{25,1},{2,26},{10... | collective-permute-start | bytes 983048 | tf_op jit(solution)/shard_map/ppermute | solution.py:26
  34.9 22.6 %collective-permute-start.27 = (bf16[384,512]{1,0:T(8,128)(2,1)S(1)}, bf16[384,512]{1,0:T(8,128)(2,1)S(1)}, u32[]{:S(2)}, u32[]{:S(2)}) collective-permute-start(bf16[384,512]{1,0:T(8,128)(2,1)S(1)} %shard_map.153.refs_3_), channel_id=1, source_target_pairs={{0,2},{2,0},{4,6},{6,4},{1,3},{3,1},{5,7},{7,5},{8,10},{10,8},{12,... | collective-permute-start | bytes 1179656 | tf_op jit(solution)/shard_map/ppermute | solution.py:26
  36.4 24.0 %collective-permute-start.31 = (bf16[384,512]{1,0:T(8,128)(2,1)S(1)}, bf16[384,512]{1,0:T(8,128)(2,1)S(1)}, u32[]{:S(2)}, u32[]{:S(2)}) collective-permute-start(bf16[384,512]{1,0:T(8,128)(2,1)S(1)} %shard_map.153.refs_3_), channel_id=1, source_target_pairs={{0,4},{2,6},{4,0},{6,2},{1,5},{3,7},{5,1},{7,3},{8,12},{10,14},{12... | collective-permute-start | bytes 1179656 | tf_op jit(solution)/shard_map/ppermute | solution.py:26
  40.1 34.4 %collective-permute-start.1 = (bf16[256,1024]{1,0:T(8,128)(2,1)S(1)}, bf16[256,1024]{1,0:T(8,128)(2,1)S(1)}, u32[]{:S(2)}, u32[]{:S(2)}) collective-permute-start(bf16[256,1024]{1,0:T(8,128)(2,1)S(1)} %get-tuple-element.38.refs_0_), channel_id=1, source_target_pairs={{0,8},{8,0},{16,24},{24,16},{1,9},{9,1},{17,25},{25,17},{2,10},{10... | collective-permute-start | bytes 1572872 | tf_op jit(solution)/shard_map/ppermute | solution.py:26
  55.4 10.6 %collective-permute-start.10 = (bf16[128,1280]{1,0:T(8,128)(2,1)S(1)}, bf16[128,1280]{1,0:T(8,128)(2,1)S(1)}, u32[]{:S(2)}, u32[]{:S(2)}) collective-permute-start(bf16[128,1280]{1,0:T(8,128)(2,1)S(1)} %collective-permute-done.9.refs_10_), channel_id=1, source_target_pairs={{0,2},{2,0},{4,6},{6,4},{1,3},{3,1},{5,7},{7,5},{8,10},{10,8},{12,... | collective-permute-start | bytes 983048 | tf_op jit(solution)/shard_map/ppermute | solution.py:26
  56.9 16.1 %collective-permute-start.8 = (bf16[128,1280]{1,0:T(8,128)(2,1)S(1)}, bf16[128,1280]{1,0:T(8,128)(2,1)S(1)}, u32[]{:S(2)}, u32[]{:S(2)}) collective-permute-start(bf16[128,1280]{1,0:T(8,128)(2,1)S(1)} %collective-permute-done.7.refs_8_), channel_id=1, source_target_pairs={{0,2},{2,0},{4,6},{6,4},{1,3},{3,1},{5,7},{7,5},{8,10},{10,8},{12,... | collective-permute-start | bytes 983048 | tf_op jit(solution)/shard_map/ppermute | solution.py:26
  58.8 15.7 %collective-permute-start.11 = (bf16[128,1280]{1,0:T(8,128)(2,1)S(1)}, bf16[128,1280]{1,0:T(8,128)(2,1)S(1)}, u32[]{:S(2)}, u32[]{:S(2)}) collective-permute-start(bf16[128,1280]{1,0:T(8,128)(2,1)S(1)} %collective-permute-done.9.refs_10_), channel_id=1, source_target_pairs={{0,4},{2,6},{4,0},{6,2},{1,5},{3,7},{5,1},{7,3},{8,12},{10,14},{12... | collective-permute-start | bytes 983048 | tf_op jit(solution)/shard_map/ppermute | solution.py:26
  61.7 18.3 %collective-permute-start.15 = (bf16[128,1280]{1,0:T(8,128)(2,1)S(1)}, bf16[128,1280]{1,0:T(8,128)(2,1)S(1)}, u32[]{:S(2)}, u32[]{:S(2)}) collective-permute-start(bf16[128,1280]{1,0:T(8,128)(2,1)S(1)} %collective-permute-done.14.refs_6_.refs_5_), channel_id=1, source_target_pairs={{0,2},{2,0},{4,6},{6,4},{1,3},{3,1},{5,7},{7,5},{8,10},{10,8},{12,... | collective-permute-start | bytes 983048 | tf_op jit(solution)/shard_map/ppermute | solution.py:26
  66.0 15.6 %collective-permute-start.20 = (bf16[128,1280]{1,0:T(8,128)(2,1)S(1)}, bf16[128,1280]{1,0:T(8,128)(2,1)S(1)}, u32[]{:S(2)}, u32[]{:S(2)}) collective-permute-start(bf16[128,1280]{1,0:T(8,128)(2,1)S(1)} %collective-permute-done.18.refs_10_.refs_9_), channel_id=1, source_target_pairs={{0,4},{2,6},{4,0},{6,2},{1,5},{3,7},{5,1},{7,3},{8,12},{10,14},{12... | collective-permute-start | bytes 983048 | tf_op jit(solution)/shard_map/ppermute | solution.py:26
  73.0 10.1 %collective-permute-start.16 = (bf16[128,1280]{1,0:T(8,128)(2,1)S(1)}, bf16[128,1280]{1,0:T(8,128)(2,1)S(1)}, u32[]{:S(2)}, u32[]{:S(2)}) collective-permute-start(bf16[128,1280]{1,0:T(8,128)(2,1)S(1)} %collective-permute-done.14.refs_6_.refs_5_), channel_id=1, source_target_pairs={{0,4},{2,6},{4,0},{6,2},{1,5},{3,7},{5,1},{7,3},{8,12},{10,14},{12... | collective-permute-start | bytes 983048 | tf_op jit(solution)/shard_map/ppermute | solution.py:26
  74.6 24.6 %collective-permute-start.2 = (bf16[256,1024]{1,0:T(8,128)(2,1)S(1)}, bf16[256,1024]{1,0:T(8,128)(2,1)S(1)}, u32[]{:S(2)}, u32[]{:S(2)}) collective-permute-start(bf16[256,1024]{1,0:T(8,128)(2,1)S(1)} %collective-permute-done.1.refs_2_), channel_id=1, source_target_pairs={{0,1},{1,0},{2,3},{3,2},{4,5},{5,4},{6,7},{7,6},{8,9},{9,8},{10,11... | collective-permute-start | bytes 1572872 | tf_op jit(solution)/shard_map/ppermute | solution.py:26
  74.6 12.5 %collective-permute-start.19 = (bf16[128,1280]{1,0:T(8,128)(2,1)S(1)}, bf16[128,1280]{1,0:T(8,128)(2,1)S(1)}, u32[]{:S(2)}, u32[]{:S(2)}) collective-permute-start(bf16[128,1280]{1,0:T(8,128)(2,1)S(1)} %collective-permute-done.18.refs_10_.refs_9_), channel_id=1, source_target_pairs={{0,2},{2,0},{4,6},{6,4},{1,3},{3,1},{5,7},{7,5},{8,10},{10,8},{12,... | collective-permute-start | bytes 983048 | tf_op jit(solution)/shard_map/ppermute | solution.py:26
  80.1 10.6 %collective-permute-start.12 = (bf16[128,1280]{1,0:T(8,128)(2,1)S(1)}, bf16[128,1280]{1,0:T(8,128)(2,1)S(1)}, u32[]{:S(2)}, u32[]{:S(2)}) collective-permute-start(bf16[128,1280]{1,0:T(8,128)(2,1)S(1)} %collective-permute-done.10.refs_11_), channel_id=1, source_target_pairs={{0,4},{2,6},{4,0},{6,2},{1,5},{3,7},{5,1},{7,3},{8,12},{10,14},{12... | collective-permute-start | bytes 983048 | tf_op jit(solution)/shard_map/ppermute | solution.py:26
  81.6 16.1 %collective-permute-start.17 = (bf16[128,1280]{1,0:T(8,128)(2,1)S(1)}, bf16[128,1280]{1,0:T(8,128)(2,1)S(1)}, u32[]{:S(2)}, u32[]{:S(2)}) collective-permute-start(bf16[128,1280]{1,0:T(8,128)(2,1)S(1)} %collective-permute-done.15.refs_7_.refs_6_), channel_id=1, source_target_pairs={{0,4},{2,6},{4,0},{6,2},{1,5},{3,7},{5,1},{7,3},{8,12},{10,14},{12... | collective-permute-start | bytes 983048 | tf_op jit(solution)/shard_map/ppermute | solution.py:26
  83.1 18.5 %collective-permute-start.21 = (bf16[128,1280]{1,0:T(8,128)(2,1)S(1)}, bf16[128,1280]{1,0:T(8,128)(2,1)S(1)}, u32[]{:S(2)}, u32[]{:S(2)}) collective-permute-start(bf16[128,1280]{1,0:T(8,128)(2,1)S(1)} %collective-permute-done.20.refs_12_.refs_11_), channel_id=1, source_target_pairs={{0,2},{2,0},{4,6},{6,4},{1,3},{3,1},{5,7},{7,5},{8,10},{10,8},{12,... | collective-permute-start | bytes 983048 | tf_op jit(solution)/shard_map/ppermute | solution.py:26
  87.1 36.2 %collective-permute-start.35 = (bf16[256,512]{1,0:T(8,128)(2,1)S(1)}, bf16[256,512]{1,0:T(8,128)(2,1)S(1)}, u32[]{:S(2)}, u32[]{:S(2)}) collective-permute-start(bf16[256,512]{1,0:T(8,128)(2,1)S(1)} %slice.22), channel_id=1, source_target_pairs={{0,4},{2,6},{4,0},{6,2},{1,5},{3,7},{5,1},{7,3},{8,12},{10,14},{12... | collective-permute-start | bytes 786440 | tf_op jit(solution)/shard_map/ppermute | solution.py:26
  90.6 31.7 %collective-permute-start.23 = (bf16[128,512]{1,0:T(8,128)(2,1)S(1)}, bf16[128,512]{1,0:T(8,128)(2,1)S(1)}, u32[]{:S(2)}, u32[]{:S(2)}) collective-permute-start(bf16[128,512]{1,0:T(8,128)(2,1)S(1)} %copy-done.4), channel_id=1, source_target_pairs={{0,2},{2,0},{4,6},{6,4},{1,3},{3,1},{5,7},{7,5},{8,10},{10,8},{12,... | collective-permute-start | bytes 393224 | tf_op jit(solution)/shard_map/ppermute | solution.py:26
  97.7 25.6 %collective-permute-start.34 = (bf16[128,512]{1,0:T(8,128)(2,1)S(1)}, bf16[128,512]{1,0:T(8,128)(2,1)S(1)}, u32[]{:S(2)}, u32[]{:S(2)}) collective-permute-start(bf16[128,512]{1,0:T(8,128)(2,1)S(1)} %collective-permute-done.30.refs_1_), channel_id=1, source_target_pairs={{0,2},{2,0},{4,6},{6,4},{1,3},{3,1},{5,7},{7,5},{8,10},{10,8},{12,... | collective-permute-start | bytes 393224 | tf_op jit(solution)/shard_map/ppermute | solution.py:26
  99.2 24.1 %collective-permute-start.36 = (bf16[128,512]{1,0:T(8,128)(2,1)S(1)}, bf16[128,512]{1,0:T(8,128)(2,1)S(1)}, u32[]{:S(2)}, u32[]{:S(2)}) collective-permute-start(bf16[128,512]{1,0:T(8,128)(2,1)S(1)} %slice.23), channel_id=1, source_target_pairs={{0,2},{2,0},{4,6},{6,4},{1,3},{3,1},{5,7},{7,5},{8,10},{10,8},{12,... | collective-permute-start | bytes 393224 | tf_op jit(solution)/shard_map/ppermute | solution.py:26
  104.6 16.8 %collective-permute-start.22 = (bf16[2,128,128]{2,1,0:T(8,128)(2,1)S(1)}, bf16[2,128,128]{2,1,0:T(8,128)(2,1)S(1)}, u32[]{:S(2)}, u32[]{:S(2)}) collective-permute-start(bf16[2,128,128]{2,1,0:T(8,128)(2,1)S(1)} %get-tuple-element.53), channel_id=1, source_target_pairs={{0,16},{8,24},{1,17},{9,25},{2,18},{10,26},{3,19},{11,27},{4,20},{... | collective-permute-start | bytes 196616 | tf_op jit(solution)/shard_map/ppermute | solution.py:31
  129.3 12.5 %collective-permute-start.29 = (bf16[128,1024]{1,0:T(8,128)(2,1)S(1)}, bf16[128,1024]{1,0:T(8,128)(2,1)S(1)}, u32[]{:S(2)}, u32[]{:S(2)}) collective-permute-start(bf16[128,1024]{1,0:T(8,128)(2,1)S(1)} %add_convert_fusion), channel_id=1, source_target_pairs={{0,8},{8,0},{16,24},{24,16},{1,9},{9,1},{17,25},{25,17},{2,10},{10... | collective-permute-start | bytes 786440 | tf_op jit(solution)/shard_map/ppermute | solution.py:26
  129.5 12.4 %collective-permute-start.33 = (bf16[128,512]{1,0:T(8,128)(2,1)S(1)}, bf16[128,512]{1,0:T(8,128)(2,1)S(1)}, u32[]{:S(2)}, u32[]{:S(2)}) collective-permute-start(bf16[128,512]{1,0:T(8,128)(2,1)S(1)} %add_convert_fusion.2), channel_id=1, source_target_pairs={{0,8},{8,0},{16,24},{24,16},{1,9},{9,1},{17,25},{25,17},{2,10},{10... | collective-permute-start | bytes 393224 | tf_op jit(solution)/shard_map/ppermute | solution.py:26
  (17 other events, 335.1 us)

commit v3 on v2

--- a/solution.py
+++ b/solution.py
@@ -328,9 +328,13 @@
     send_out[quarter:, :] = rows_owed(joined, whole, 1 - part, 1 - tp)
 
 
-def keep_kernel(joined, whole, keep_out, far_out):
+def far_kernel(joined, whole, far_out):
     part, tp = lax.axis_index("sp") % PAIR, lax.axis_index("tp")
     far_out[...] = rows_owed(joined, whole, 1 - part, tp)
+
+
+def keep_kernel(joined, whole, keep_out):
+    part, tp = lax.axis_index("sp") % PAIR, lax.axis_index("tp")
     keep_out[...] = rows_owed(joined, whole, part, tp)
 
 
@@ -521,7 +525,8 @@
             joined,
             *shards,
         )
-        keep, far = call(keep_kernel, [((quarter, wide), BF16)] * 2, joined, whole)
+        (far,) = call(far_kernel, [((quarter, wide), BF16)], joined, whole)
+        (keep,) = call(keep_kernel, [((quarter, wide), BF16)], joined, whole)
         met = swapped(send, "tp", 1)
         owed = (far.astype(F32) + met[quarter:].astype(F32)).astype(BF16)
         shares += [keep, met, swapped(owed, "sp", 1)]

time: 143 us -> 142 us (level)
    pallas_call x16 -> x19, Pallas kernels: 16.7 us -> 17.1 us  [call(): pl.pallas_call(kernel, out_shape=[jax.ShapeDtypeStruct(shape, dtype) for...]
where the time goes in v3:
time: 142 us
  waiting for transfers between devices  61.7 us (43%)
  starting transfers between devices  61 us (43%)
  Pallas kernels  17.1 us (12%)
  local copies, waits for them, and re-layouts  1.81 us (1%)
    ppermute x36, waiting for transfers between devices, swapped(): return lax.ppermute(value, axis, [(i, i ^ distance) for i in range(count)])  61.7 us
    ppermute x36, starting transfers between devices, swapped(): return lax.ppermute(value, axis, [(i, i ^ distance) for i in range(count)])  45.2 us
    pallas_call x19, Pallas kernels, call(): pl.pallas_call(kernel, out_shape=[jax.ShapeDtypeStruct(shape, dtype) for...  17.1 us
    ppermute x3, starting transfers between devices, passed_on(): lax.ppermute(value, axis, [(i, i + steps) for i in range(first, count - s...  15.9 us
  transfers between devices with their start and end apart: 39, of which 14 were waited for; matrix products, arithmetic and copies ran while one was open for 0% of the time, Pallas kernels for 10%

profile of v3, /device:TPU:0, one launch (start us, length us, event | category | flops | bytes accessed | tf_op | source)
XLA Modules:
  0.0 142.2 jit_solution(2428177266904992829)
XLA Ops:
  0.0 1.8 %shard_map.152 = (bf16[128,512]{1,0:T(8,128)(2,1)}, bf16[128,512]{1,0:T(8,128)(2,1)}) custom-call(bf16[512,128]{1,0:T(8,128)(2,1)} %refs_0_.3, bf16[512,128]{1,0:T(8,128)(2,1)} %refs_1_.3), custom_call_target="tpu_custom_call" | custom-call | tf_op jit(solution)/shard_map/pallas_call | solution.py:37
  1.8 4.1 %collective-permute-start.25 = (bf16[128,512]{1,0:T(8,128)(2,1)}, bf16[128,512]{1,0:T(8,128)(2,1)S(1)}, u32[]{:S(2)}, u32[]{:S(2)}) collective-permute-start(bf16[128,512]{1,0:T(8,128)(2,1)} %get-tuple-element.51.refs_1_), channel_id=1, source_target_pairs={{0,16},{8,24},{16,0},{24,8},{1,17},{9,25},{17,1},{25,9},{2,18},{10... | collective-permute-start | bytes 393224 | tf_op jit(solution)/shard_map/ppermute | solution.py:26
  5.9 2.0 %shard_map.147 = (bf16[128,1280]{1,0:T(8,128)(2,1)}, bf16[128,1280]{1,0:T(8,128)(2,1)}) custom-call(bf16[128,512]{1,0:T(8,128)(2,1)} %refs_0_.2, bf16[128,512]{1,0:T(8,128)(2,1)} %refs_1_.2, bf16[128,512]{1,0:T(8,128)(2,1)} %refs_2_.1, bf16[128,512]{1,0:T(8,128)(2,1)} %refs_3_.1, bf16[128,512]{1,0:T(8,128)(2,1)} %refs_4_.1), custom_call_target="tpu_custom_call" | custom-call | tf_op jit(solution)/shard_map/pallas_call | solution.py:37
  8.0 1.6 %collective-permute-start.9 = (bf16[128,1280]{1,0:T(8,128)(2,1)}, bf16[128,1280]{1,0:T(8,128)(2,1)S(1)}, u32[]{:S(2)}, u32[]{:S(2)}) collective-permute-start(bf16[128,1280]{1,0:T(8,128)(2,1)} %get-tuple-element.36), channel_id=1, source_target_pairs={{0,8},{8,0},{16,24},{24,16},{1,9},{9,1},{17,25},{25,17},{2,10},{10... | collective-permute-start | bytes 983048 | tf_op jit(solution)/shard_map/ppermute | solution.py:26
  10.1 1.6 %collective-permute-start.24 = (bf16[128,512]{1,0:T(8,128)(2,1)}, bf16[128,512]{1,0:T(8,128)(2,1)S(1)}, u32[]{:S(2)}, u32[]{:S(2)}) collective-permute-start(bf16[128,512]{1,0:T(8,128)(2,1)} %get-tuple-element.52), channel_id=1, source_target_pairs={{0,8},{8,0},{16,24},{24,16},{1,9},{9,1},{17,25},{25,17},{2,10},{10... | collective-permute-start | bytes 393224 | tf_op jit(solution)/shard_map/ppermute | solution.py:26
  11.7 7.9 %collective-permute-done.13.refs_4_ = f32[4,256]{1,0:T(4,128)S(1)} collective-permute-done((f32[4,256]{1,0:T(4,128)}, f32[4,256]{1,0:T(4,128)S(1)}, u32[]{:S(2)}, u32[]{:S(2)}) %collective-permute-start.13) | collective-permute-done | bytes 4128 | tf_op jit(solution)/shard_map/ppermute | solution.py:26
  19.6 1.6 %collective-permute-start.7 = (bf16[128,1280]{1,0:T(8,128)(2,1)}, bf16[128,1280]{1,0:T(8,128)(2,1)S(1)}, u32[]{:S(2)}, u32[]{:S(2)}) collective-permute-start(bf16[128,1280]{1,0:T(8,128)(2,1)} %get-tuple-element.35.refs_6_), channel_id=1, source_target_pairs={{0,4},{2,6},{4,0},{6,2},{1,5},{3,7},{5,1},{7,3},{8,12},{10,14},{12... | collective-permute-start | bytes 983048 | tf_op jit(solution)/shard_map/ppermute | solution.py:26
  21.2 3.3 %collective-permute-start.26 = (bf16[128,512]{1,0:T(8,128)(2,1)}, bf16[128,512]{1,0:T(8,128)(2,1)S(1)}, u32[]{:S(2)}, u32[]{:S(2)}) collective-permute-start(bf16[128,512]{1,0:T(8,128)(2,1)} %get-tuple-element.52), channel_id=1, source_target_pairs={{0,24},{8,16},{16,8},{24,0},{1,25},{9,17},{17,9},{25,1},{2,26},{10... | collective-permute-start | bytes 393224 | tf_op jit(solution)/shard_map/ppermute | solution.py:26
  25.0 3.4 %collective-permute-done.26.refs_2_ = bf16[128,512]{1,0:T(8,128)(2,1)S(1)} collective-permute-done((bf16[128,512]{1,0:T(8,128)(2,1)}, bf16[128,512]{1,0:T(8,128)(2,1)S(1)}, u32[]{:S(2)}, u32[]{:S(2)}) %collective-permute-start.26) | collective-permute-done | bytes 131104 | tf_op jit(solution)/shard_map/ppermute | solution.py:26
  29.9 2.3 %collective-permute-done.30.refs_1_ = bf16[128,512]{1,0:T(8,128)(2,1)S(1)} collective-permute-done((bf16[128,512]{1,0:T(8,128)(2,1)}, bf16[128,512]{1,0:T(8,128)(2,1)S(1)}, u32[]{:S(2)}, u32[]{:S(2)}) %collective-permute-start.30) | collective-permute-done | bytes 131104 | tf_op jit(solution)/shard_map/ppermute | solution.py:26
  32.9 1.9 %collective-permute-start.18 = (bf16[128,1280]{1,0:T(8,128)(2,1)}, bf16[128,1280]{1,0:T(8,128)(2,1)S(1)}, u32[]{:S(2)}, u32[]{:S(2)}) collective-permute-start(bf16[128,1280]{1,0:T(8,128)(2,1)} %get-tuple-element.36), channel_id=1, source_target_pairs={{0,24},{8,16},{16,8},{24,0},{1,25},{9,17},{17,9},{25,1},{2,26},{10... | collective-permute-start | bytes 983048 | tf_op jit(solution)/shard_map/ppermute | solution.py:26
  34.9 1.6 %collective-permute-start.27 = (bf16[384,512]{1,0:T(8,128)(2,1)S(1)}, bf16[384,512]{1,0:T(8,128)(2,1)S(1)}, u32[]{:S(2)}, u32[]{:S(2)}) collective-permute-start(bf16[384,512]{1,0:T(8,128)(2,1)S(1)} %shard_map.153.refs_3_), channel_id=1, source_target_pairs={{0,2},{2,0},{4,6},{6,4},{1,3},{3,1},{5,7},{7,5},{8,10},{10,8},{12,... | collective-permute-start | bytes 1179656 | tf_op jit(solution)/shard_map/ppermute | solution.py:26
  36.4 1.5 %collective-permute-start.31 = (bf16[384,512]{1,0:T(8,128)(2,1)S(1)}, bf16[384,512]{1,0:T(8,128)(2,1)S(1)}, u32[]{:S(2)}, u32[]{:S(2)}) collective-permute-start(bf16[384,512]{1,0:T(8,128)(2,1)S(1)} %shard_map.153.refs_3_), channel_id=1, source_target_pairs={{0,4},{2,6},{4,0},{6,2},{1,5},{3,7},{5,1},{7,3},{8,12},{10,14},{12... | collective-permute-start | bytes 1179656 | tf_op jit(solution)/shard_map/ppermute | solution.py:26
  41.1 14.3 %collective-permute-done.14.refs_6_.refs_5_ = bf16[128,1280]{1,0:T(8,128)(2,1)S(1)} collective-permute-done((bf16[128,1280]{1,0:T(8,128)(2,1)}, bf16[128,1280]{1,0:T(8,128)(2,1)S(1)}, u32[]{:S(2)}, u32[]{:S(2)}) %collective-permute-start.14) | collective-permute-done | bytes 327712 | tf_op jit(solution)/shard_map/ppermute | solution.py:26
  58.8 1.6 %collective-permute-start.11 = (bf16[128,1280]{1,0:T(8,128)(2,1)S(1)}, bf16[128,1280]{1,0:T(8,128)(2,1)S(1)}, u32[]{:S(2)}, u32[]{:S(2)}) collective-permute-start(bf16[128,1280]{1,0:T(8,128)(2,1)S(1)} %collective-permute-done.9.refs_10_), channel_id=1, source_target_pairs={{0,4},{2,6},{4,0},{6,2},{1,5},{3,7},{5,1},{7,3},{8,12},{10,14},{12... | collective-permute-start | bytes 983048 | tf_op jit(solution)/shard_map/ppermute | solution.py:26
  63.2 2.8 %collective-permute-done.10.refs_11_ = bf16[128,1280]{1,0:T(8,128)(2,1)S(1)} collective-permute-done((bf16[128,1280]{1,0:T(8,128)(2,1)S(1)}, bf16[128,1280]{1,0:T(8,128)(2,1)S(1)}, u32[]{:S(2)}, u32[]{:S(2)}) %collective-permute-start.10) | collective-permute-done | bytes 327712 | tf_op jit(solution)/shard_map/ppermute | solution.py:26
  66.0 1.5 %collective-permute-start.20 = (bf16[128,1280]{1,0:T(8,128)(2,1)S(1)}, bf16[128,1280]{1,0:T(8,128)(2,1)S(1)}, u32[]{:S(2)}, u32[]{:S(2)}) collective-permute-start(bf16[128,1280]{1,0:T(8,128)(2,1)S(1)} %collective-permute-done.18.refs_10_.refs_9_), channel_id=1, source_target_pairs={{0,4},{2,6},{4,0},{6,2},{1,5},{3,7},{5,1},{7,3},{8,12},{10,14},{12... | collective-permute-start | bytes 983048 | tf_op jit(solution)/shard_map/ppermute | solution.py:26
  67.5 5.5 %collective-permute-done.8.refs_9_ = bf16[128,1280]{1,0:T(8,128)(2,1)S(1)} collective-permute-done((bf16[128,1280]{1,0:T(8,128)(2,1)S(1)}, bf16[128,1280]{1,0:T(8,128)(2,1)S(1)}, u32[]{:S(2)}, u32[]{:S(2)}) %collective-permute-start.8) | collective-permute-done | bytes 327712 | tf_op jit(solution)/shard_map/ppermute | solution.py:26
  73.0 1.5 %collective-permute-start.16 = (bf16[128,1280]{1,0:T(8,128)(2,1)S(1)}, bf16[128,1280]{1,0:T(8,128)(2,1)S(1)}, u32[]{:S(2)}, u32[]{:S(2)}) collective-permute-start(bf16[128,1280]{1,0:T(8,128)(2,1)S(1)} %collective-permute-done.14.refs_6_.refs_5_), channel_id=1, source_target_pairs={{0,4},{2,6},{4,0},{6,2},{1,5},{3,7},{5,1},{7,3},{8,12},{10,14},{12... | collective-permute-start | bytes 983048 | tf_op jit(solution)/shard_map/ppermute | solution.py:26
  74.6 1.6 %collective-permute-start.19 = (bf16[128,1280]{1,0:T(8,128)(2,1)S(1)}, bf16[128,1280]{1,0:T(8,128)(2,1)S(1)}, u32[]{:S(2)}, u32[]{:S(2)}) collective-permute-start(bf16[128,1280]{1,0:T(8,128)(2,1)S(1)} %collective-permute-done.18.refs_10_.refs_9_), channel_id=1, source_target_pairs={{0,2},{2,0},{4,6},{6,4},{1,3},{3,1},{5,7},{7,5},{8,10},{10,8},{12,... | collective-permute-start | bytes 983048 | tf_op jit(solution)/shard_map/ppermute | solution.py:26
  76.1 3.9 %collective-permute-done.15.refs_7_.refs_6_ = bf16[128,1280]{1,0:T(8,128)(2,1)S(1)} collective-permute-done((bf16[128,1280]{1,0:T(8,128)(2,1)S(1)}, bf16[128,1280]{1,0:T(8,128)(2,1)S(1)}, u32[]{:S(2)}, u32[]{:S(2)}) %collective-permute-start.15) | collective-permute-done | bytes 327712 | tf_op jit(solution)/shard_map/ppermute | solution.py:26
  84.6 2.4 %collective-permute-done.19.refs_11_.refs_10_ = bf16[128,1280]{1,0:T(8,128)(2,1)S(1)} collective-permute-done((bf16[128,1280]{1,0:T(8,128)(2,1)S(1)}, bf16[128,1280]{1,0:T(8,128)(2,1)S(1)}, u32[]{:S(2)}, u32[]{:S(2)}) %collective-permute-start.19) | collective-permute-done | bytes 327712 | tf_op jit(solution)/shard_map/ppermute | solution.py:26
  87.1 1.5 %collective-permute-start.35 = (bf16[256,512]{1,0:T(8,128)(2,1)S(1)}, bf16[256,512]{1,0:T(8,128)(2,1)S(1)}, u32[]{:S(2)}, u32[]{:S(2)}) collective-permute-start(bf16[256,512]{1,0:T(8,128)(2,1)S(1)} %slice.22), channel_id=1, source_target_pairs={{0,4},{2,6},{4,0},{6,2},{1,5},{3,7},{5,1},{7,3},{8,12},{10,14},{12... | collective-permute-start | bytes 786440 | tf_op jit(solution)/shard_map/ppermute | solution.py:26
  88.6 2.0 %collective-permute-done.12.refs_13_ = bf16[128,1280]{1,0:T(8,128)(2,1)S(1)} collective-permute-done((bf16[128,1280]{1,0:T(8,128)(2,1)S(1)}, bf16[128,1280]{1,0:T(8,128)(2,1)S(1)}, u32[]{:S(2)}, u32[]{:S(2)}) %collective-permute-start.12) | collective-permute-done | bytes 327712 | tf_op jit(solution)/shard_map/ppermute | solution.py:26
  92.1 5.5 %collective-permute-done.17.refs_9_.refs_8_ = bf16[128,1280]{1,0:T(8,128)(2,1)S(1)} collective-permute-done((bf16[128,1280]{1,0:T(8,128)(2,1)S(1)}, bf16[128,1280]{1,0:T(8,128)(2,1)S(1)}, u32[]{:S(2)}, u32[]{:S(2)}) %collective-permute-start.17) | collective-permute-done | bytes 327712 | tf_op jit(solution)/shard_map/ppermute | solution.py:26
  99.7 1.9 %shard_map.148 = (bf16[528,2048]{1,0:T(8,128)(2,1)S(1)}, f32[528,1280]{1,0:T(8,128)S(1)}) custom-call(bf16[256,1024]{1,0:T(8,128)(2,1)S(1)} %get-tuple-element.32.refs_0_, bf16[256,1024]{1,0:T(8,128)(2,1)S(1)} %get-tuple-element.33.refs_1_, bf16[256,1024]{1,0:T(8,128)(2,1)S(1)} %collective-permute-done.1.refs_2_, ...), custom_call_target="tpu_custom_call" | custom-call | tf_op jit(solution)/shard_map/pallas_call | solution.py:37
  101.6 3.0 %shard_map.149 = (bf16[512,256]{1,0:T(8,128)(2,1)S(1)}, f32[512,256]{1,0:T(8,128)S(1)}, f32[512,256]{1,0:T(8,128)S(1)}, f32[4,2,128,128]{3,2,1,0:T(8,128)S(1)}, ...) custom-call(bf16[528,2048]{1,0:T(8,128)(2,1)S(1)} %get-tuple-element, ...), custom_call_target="tpu_custom_call" | custom-call | tf_op jit(solution)/shard_map/pallas_call | solution.py:37
  104.6 14.6 %collective-permute-start.22 = (bf16[2,128,128]{2,1,0:T(8,128)(2,1)S(1)}, bf16[2,128,128]{2,1,0:T(8,128)(2,1)S(1)}, u32[]{:S(2)}, u32[]{:S(2)}) collective-permute-start(bf16[2,128,128]{2,1,0:T(8,128)(2,1)S(1)} %get-tuple-element.47), channel_id=1, source_target_pairs={{0,16},{8,24},{1,17},{9,25},{2,18},{10,26},{3,19},{11,27},{4,20},{... | collective-permute-start | bytes 196616 | tf_op jit(solution)/shard_map/ppermute | solution.py:31
  119.2 2.2 %shard_map.150 = (f32[512,256]{1,0:T(8,128)S(1)}, bf16[512,256]{1,0:T(8,128)(2,1)S(1)}, bf16[512,256]{1,0:T(8,128)(2,1)S(1)}, bf16[512,256]{1,0:T(8,128)(2,1)S(1)}, bf16[16,256]{1,0:T(8,128)(2,1)S(1)}) custom-call(bf16[528,2048]{1,0:T(8,128)(2,1)S(1)} %get-tuple-element.37.refs_0_, f32[528,1280]{1,0:T(8,128)S(1)} %get-tuple-element.38.refs_1_, ...), custom_call_target="tpu_custom_call" | custom-call | tf_op jit(solution)/shard_map/pallas_call | solution.py:37
  126.0 2.6 %collective-permute-start.38 = (bf16[128,512]{1,0:T(8,128)(2,1)S(1)}, bf16[128,512]{1,0:T(8,128)(2,1)S(1)}, u32[]{:S(2)}, u32[]{:S(2)}) collective-permute-start(bf16[128,512]{1,0:T(8,128)(2,1)S(1)} %add_convert_fusion.1), channel_id=1, source_target_pairs={{0,8},{8,0},{16,24},{24,16},{1,9},{9,1},{17,25},{25,17},{2,10},{10... | collective-permute-start | bytes 393224 | tf_op jit(solution)/shard_map/ppermute | solution.py:26
  128.8 2.1 %collective-permute-start.33 = (bf16[128,512]{1,0:T(8,128)(2,1)S(1)}, bf16[128,512]{1,0:T(8,128)(2,1)S(1)}, u32[]{:S(2)}, u32[]{:S(2)}) collective-permute-start(bf16[128,512]{1,0:T(8,128)(2,1)S(1)} %add_convert_fusion.2), channel_id=1, source_target_pairs={{0,8},{8,0},{16,24},{24,16},{1,9},{9,1},{17,25},{25,17},{2,10},{10... | collective-permute-start | bytes 393224 | tf_op jit(solution)/shard_map/ppermute | solution.py:26
  133.0 8.2 %collective-permute-done.33.refs_5_ = bf16[128,512]{1,0:T(8,128)(2,1)S(1)} collective-permute-done((bf16[128,512]{1,0:T(8,128)(2,1)S(1)}, bf16[128,512]{1,0:T(8,128)(2,1)S(1)}, u32[]{:S(2)}, u32[]{:S(2)}) %collective-permute-start.33) | collective-permute-done | bytes 131104 | tf_op jit(solution)/shard_map/ppermute | solution.py:26
  (90 shorter events, 28.3 us)
Async XLA Ops:
  1.8 19.4 %collective-permute-start.25 = (bf16[128,512]{1,0:T(8,128)(2,1)}, bf16[128,512]{1,0:T(8,128)(2,1)S(1)}, u32[]{:S(2)}, u32[]{:S(2)}) collective-permute-start(bf16[128,512]{1,0:T(8,128)(2,1)} %get-tuple-element.51.refs_1_), channel_id=1, source_target_pairs={{0,16},{8,24},{16,0},{24,8},{1,17},{9,25},{17,1},{25,9},{2,18},{10... | collective-permute-start | bytes 393224 | tf_op jit(solution)/shard_map/ppermute | solution.py:26
  5.9 30.5 %collective-permute-start = (bf16[256,1024]{1,0:T(8,128)(2,1)}, bf16[256,1024]{1,0:T(8,128)(2,1)S(1)}, u32[]{:S(2)}, u32[]{:S(2)}) collective-permute-start(bf16[256,1024]{1,0:T(8,128)(2,1)} %bitcast.10), channel_id=1, source_target_pairs={{0,1},{1,0},{2,3},{3,2},{4,5},{5,4},{6,7},{7,6},{8,9},{9,8},{10,11... | collective-permute-start | bytes 1572872 | tf_op jit(solution)/shard_map/ppermute | solution.py:26
  8.0 24.9 %collective-permute-start.9 = (bf16[128,1280]{1,0:T(8,128)(2,1)}, bf16[128,1280]{1,0:T(8,128)(2,1)S(1)}, u32[]{:S(2)}, u32[]{:S(2)}) collective-permute-start(bf16[128,1280]{1,0:T(8,128)(2,1)} %get-tuple-element.36), channel_id=1, source_target_pairs={{0,8},{8,0},{16,24},{24,16},{1,9},{9,1},{17,25},{25,17},{2,10},{10... | collective-permute-start | bytes 983048 | tf_op jit(solution)/shard_map/ppermute | solution.py:26
  9.6 10.0 %collective-permute-start.13 = (f32[4,256]{1,0:T(4,128)}, f32[4,256]{1,0:T(4,128)S(1)}, u32[]{:S(2)}, u32[]{:S(2)}) collective-permute-start(f32[4,256]{1,0:T(4,128)} %bitcast.14), channel_id=1, source_target_pairs={{0,8},{8,0},{16,24},{24,16},{1,9},{9,1},{17,25},{25,17},{2,10},{10... | collective-permute-start | bytes 12296 | tf_op jit(solution)/shard_map/ppermute | solution.py:26
  10.1 14.4 %collective-permute-start.24 = (bf16[128,512]{1,0:T(8,128)(2,1)}, bf16[128,512]{1,0:T(8,128)(2,1)S(1)}, u32[]{:S(2)}, u32[]{:S(2)}) collective-permute-start(bf16[128,512]{1,0:T(8,128)(2,1)} %get-tuple-element.52), channel_id=1, source_target_pairs={{0,8},{8,0},{16,24},{24,16},{1,9},{9,1},{17,25},{25,17},{2,10},{10... | collective-permute-start | bytes 393224 | tf_op jit(solution)/shard_map/ppermute | solution.py:26
  19.6 15.3 %collective-permute-start.7 = (bf16[128,1280]{1,0:T(8,128)(2,1)}, bf16[128,1280]{1,0:T(8,128)(2,1)S(1)}, u32[]{:S(2)}, u32[]{:S(2)}) collective-permute-start(bf16[128,1280]{1,0:T(8,128)(2,1)} %get-tuple-element.35.refs_6_), channel_id=1, source_target_pairs={{0,4},{2,6},{4,0},{6,2},{1,5},{3,7},{5,1},{7,3},{8,12},{10,14},{12... | collective-permute-start | bytes 983048 | tf_op jit(solution)/shard_map/ppermute | solution.py:26
  21.2 7.3 %collective-permute-start.26 = (bf16[128,512]{1,0:T(8,128)(2,1)}, bf16[128,512]{1,0:T(8,128)(2,1)S(1)}, u32[]{:S(2)}, u32[]{:S(2)}) collective-permute-start(bf16[128,512]{1,0:T(8,128)(2,1)} %get-tuple-element.52), channel_id=1, source_target_pairs={{0,24},{8,16},{16,8},{24,0},{1,25},{9,17},{17,9},{25,1},{2,26},{10... | collective-permute-start | bytes 393224 | tf_op jit(solution)/shard_map/ppermute | solution.py:26
  24.5 7.7 %collective-permute-start.30 = (bf16[128,512]{1,0:T(8,128)(2,1)}, bf16[128,512]{1,0:T(8,128)(2,1)S(1)}, u32[]{:S(2)}, u32[]{:S(2)}) collective-permute-start(bf16[128,512]{1,0:T(8,128)(2,1)} %get-tuple-element.51.refs_1_), channel_id=1, source_target_pairs={{0,4},{2,6},{4,0},{6,2},{1,5},{3,7},{5,1},{7,3},{8,12},{10,14},{12... | collective-permute-start | bytes 393224 | tf_op jit(solution)/shard_map/ppermute | solution.py:26
  28.4 11.7 %collective-permute-start.6 = (bf16[128,1280]{1,0:T(8,128)(2,1)}, bf16[128,1280]{1,0:T(8,128)(2,1)S(1)}, u32[]{:S(2)}, u32[]{:S(2)}) collective-permute-start(bf16[128,1280]{1,0:T(8,128)(2,1)} %get-tuple-element.35.refs_6_), channel_id=1, source_target_pairs={{0,2},{2,0},{4,6},{6,4},{1,3},{3,1},{5,7},{7,5},{8,10},{10,8},{12,... | collective-permute-start | bytes 983048 | tf_op jit(solution)/shard_map/ppermute | solution.py:26
  32.3 23.2 %collective-permute-start.14 = (bf16[128,1280]{1,0:T(8,128)(2,1)}, bf16[128,1280]{1,0:T(8,128)(2,1)S(1)}, u32[]{:S(2)}, u32[]{:S(2)}) collective-permute-start(bf16[128,1280]{1,0:T(8,128)(2,1)} %get-tuple-element.35.refs_6_), channel_id=1, source_target_pairs={{0,16},{8,24},{16,0},{24,8},{1,17},{9,25},{17,1},{25,9},{2,18},{10... | collective-permute-start | bytes 983048 | tf_op jit(solution)/shard_map/ppermute | solution.py:26
  32.9 24.0 %collective-permute-start.18 = (bf16[128,1280]{1,0:T(8,128)(2,1)}, bf16[128,1280]{1,0:T(8,128)(2,1)S(1)}, u32[]{:S(2)}, u32[]{:S(2)}) collective-permute-start(bf16[128,1280]{1,0:T(8,128)(2,1)} %get-tuple-element.36), channel_id=1, source_target_pairs={{0,24},{8,16},{16,8},{24,0},{1,25},{9,17},{17,9},{25,1},{2,26},{10... | collective-permute-start | bytes 983048 | tf_op jit(solution)/shard_map/ppermute | solution.py:26
  34.9 22.6 %collective-permute-start.27 = (bf16[384,512]{1,0:T(8,128)(2,1)S(1)}, bf16[384,512]{1,0:T(8,128)(2,1)S(1)}, u32[]{:S(2)}, u32[]{:S(2)}) collective-permute-start(bf16[384,512]{1,0:T(8,128)(2,1)S(1)} %shard_map.153.refs_3_), channel_id=1, source_target_pairs={{0,2},{2,0},{4,6},{6,4},{1,3},{3,1},{5,7},{7,5},{8,10},{10,8},{12,... | collective-permute-start | bytes 1179656 | tf_op jit(solution)/shard_map/ppermute | solution.py:26
  36.4 24.0 %collective-permute-start.31 = (bf16[384,512]{1,0:T(8,128)(2,1)S(1)}, bf16[384,512]{1,0:T(8,128)(2,1)S(1)}, u32[]{:S(2)}, u32[]{:S(2)}) collective-permute-start(bf16[384,512]{1,0:T(8,128)(2,1)S(1)} %shard_map.153.refs_3_), channel_id=1, source_target_pairs={{0,4},{2,6},{4,0},{6,2},{1,5},{3,7},{5,1},{7,3},{8,12},{10,14},{12... | collective-permute-start | bytes 1179656 | tf_op jit(solution)/shard_map/ppermute | solution.py:26
  40.1 34.4 %collective-permute-start.1 = (bf16[256,1024]{1,0:T(8,128)(2,1)S(1)}, bf16[256,1024]{1,0:T(8,128)(2,1)S(1)}, u32[]{:S(2)}, u32[]{:S(2)}) collective-permute-start(bf16[256,1024]{1,0:T(8,128)(2,1)S(1)} %get-tuple-element.32.refs_0_), channel_id=1, source_target_pairs={{0,8},{8,0},{16,24},{24,16},{1,9},{9,1},{17,25},{25,17},{2,10},{10... | collective-permute-start | bytes 1572872 | tf_op jit(solution)/shard_map/ppermute | solution.py:26
  55.4 10.6 %collective-permute-start.10 = (bf16[128,1280]{1,0:T(8,128)(2,1)S(1)}, bf16[128,1280]{1,0:T(8,128)(2,1)S(1)}, u32[]{:S(2)}, u32[]{:S(2)}) collective-permute-start(bf16[128,1280]{1,0:T(8,128)(2,1)S(1)} %collective-permute-done.9.refs_10_), channel_id=1, source_target_pairs={{0,2},{2,0},{4,6},{6,4},{1,3},{3,1},{5,7},{7,5},{8,10},{10,8},{12,... | collective-permute-start | bytes 983048 | tf_op jit(solution)/shard_map/ppermute | solution.py:26
  56.9 16.1 %collective-permute-start.8 = (bf16[128,1280]{1,0:T(8,128)(2,1)S(1)}, bf16[128,1280]{1,0:T(8,128)(2,1)S(1)}, u32[]{:S(2)}, u32[]{:S(2)}) collective-permute-start(bf16[128,1280]{1,0:T(8,128)(2,1)S(1)} %collective-permute-done.7.refs_8_), channel_id=1, source_target_pairs={{0,2},{2,0},{4,6},{6,4},{1,3},{3,1},{5,7},{7,5},{8,10},{10,8},{12,... | collective-permute-start | bytes 983048 | tf_op jit(solution)/shard_map/ppermute | solution.py:26
  58.8 15.7 %collective-permute-start.11 = (bf16[128,1280]{1,0:T(8,128)(2,1)S(1)}, bf16[128,1280]{1,0:T(8,128)(2,1)S(1)}, u32[]{:S(2)}, u32[]{:S(2)}) collective-permute-start(bf16[128,1280]{1,0:T(8,128)(2,1)S(1)} %collective-permute-done.9.refs_10_), channel_id=1, source_target_pairs={{0,4},{2,6},{4,0},{6,2},{1,5},{3,7},{5,1},{7,3},{8,12},{10,14},{12... | collective-permute-start | bytes 983048 | tf_op jit(solution)/shard_map/ppermute | solution.py:26
  61.7 18.3 %collective-permute-start.15 = (bf16[128,1280]{1,0:T(8,128)(2,1)S(1)}, bf16[128,1280]{1,0:T(8,128)(2,1)S(1)}, u32[]{:S(2)}, u32[]{:S(2)}) collective-permute-start(bf16[128,1280]{1,0:T(8,128)(2,1)S(1)} %collective-permute-done.14.refs_6_.refs_5_), channel_id=1, source_target_pairs={{0,2},{2,0},{4,6},{6,4},{1,3},{3,1},{5,7},{7,5},{8,10},{10,8},{12,... | collective-permute-start | bytes 983048 | tf_op jit(solution)/shard_map/ppermute | solution.py:26
  66.0 15.6 %collective-permute-start.20 = (bf16[128,1280]{1,0:T(8,128)(2,1)S(1)}, bf16[128,1280]{1,0:T(8,128)(2,1)S(1)}, u32[]{:S(2)}, u32[]{:S(2)}) collective-permute-start(bf16[128,1280]{1,0:T(8,128)(2,1)S(1)} %collective-permute-done.18.refs_10_.refs_9_), channel_id=1, source_target_pairs={{0,4},{2,6},{4,0},{6,2},{1,5},{3,7},{5,1},{7,3},{8,12},{10,14},{12... | collective-permute-start | bytes 983048 | tf_op jit(solution)/shard_map/ppermute | solution.py:26
  73.0 10.1 %collective-permute-start.16 = (bf16[128,1280]{1,0:T(8,128)(2,1)S(1)}, bf16[128,1280]{1,0:T(8,128)(2,1)S(1)}, u32[]{:S(2)}, u32[]{:S(2)}) collective-permute-start(bf16[128,1280]{1,0:T(8,128)(2,1)S(1)} %collective-permute-done.14.refs_6_.refs_5_), channel_id=1, source_target_pairs={{0,4},{2,6},{4,0},{6,2},{1,5},{3,7},{5,1},{7,3},{8,12},{10,14},{12... | collective-permute-start | bytes 983048 | tf_op jit(solution)/shard_map/ppermute | solution.py:26
  74.5 24.6 %collective-permute-start.2 = (bf16[256,1024]{1,0:T(8,128)(2,1)S(1)}, bf16[256,1024]{1,0:T(8,128)(2,1)S(1)}, u32[]{:S(2)}, u32[]{:S(2)}) collective-permute-start(bf16[256,1024]{1,0:T(8,128)(2,1)S(1)} %collective-permute-done.1.refs_2_), channel_id=1, source_target_pairs={{0,1},{1,0},{2,3},{3,2},{4,5},{5,4},{6,7},{7,6},{8,9},{9,8},{10,11... | collective-permute-start | bytes 1572872 | tf_op jit(solution)/shard_map/ppermute | solution.py:26
  74.6 12.5 %collective-permute-start.19 = (bf16[128,1280]{1,0:T(8,128)(2,1)S(1)}, bf16[128,1280]{1,0:T(8,128)(2,1)S(1)}, u32[]{:S(2)}, u32[]{:S(2)}) collective-permute-start(bf16[128,1280]{1,0:T(8,128)(2,1)S(1)} %collective-permute-done.18.refs_10_.refs_9_), channel_id=1, source_target_pairs={{0,2},{2,0},{4,6},{6,4},{1,3},{3,1},{5,7},{7,5},{8,10},{10,8},{12,... | collective-permute-start | bytes 983048 | tf_op jit(solution)/shard_map/ppermute | solution.py:26
  80.0 10.6 %collective-permute-start.12 = (bf16[128,1280]{1,0:T(8,128)(2,1)S(1)}, bf16[128,1280]{1,0:T(8,128)(2,1)S(1)}, u32[]{:S(2)}, u32[]{:S(2)}) collective-permute-start(bf16[128,1280]{1,0:T(8,128)(2,1)S(1)} %collective-permute-done.10.refs_11_), channel_id=1, source_target_pairs={{0,4},{2,6},{4,0},{6,2},{1,5},{3,7},{5,1},{7,3},{8,12},{10,14},{12... | collective-permute-start | bytes 983048 | tf_op jit(solution)/shard_map/ppermute | solution.py:26
  81.6 16.1 %collective-permute-start.17 = (bf16[128,1280]{1,0:T(8,128)(2,1)S(1)}, bf16[128,1280]{1,0:T(8,128)(2,1)S(1)}, u32[]{:S(2)}, u32[]{:S(2)}) collective-permute-start(bf16[128,1280]{1,0:T(8,128)(2,1)S(1)} %collective-permute-done.15.refs_7_.refs_6_), channel_id=1, source_target_pairs={{0,4},{2,6},{4,0},{6,2},{1,5},{3,7},{5,1},{7,3},{8,12},{10,14},{12... | collective-permute-start | bytes 983048 | tf_op jit(solution)/shard_map/ppermute | solution.py:26
  83.1 18.5 %collective-permute-start.21 = (bf16[128,1280]{1,0:T(8,128)(2,1)S(1)}, bf16[128,1280]{1,0:T(8,128)(2,1)S(1)}, u32[]{:S(2)}, u32[]{:S(2)}) collective-permute-start(bf16[128,1280]{1,0:T(8,128)(2,1)S(1)} %collective-permute-done.20.refs_12_.refs_11_), channel_id=1, source_target_pairs={{0,2},{2,0},{4,6},{6,4},{1,3},{3,1},{5,7},{7,5},{8,10},{10,8},{12,... | collective-permute-start | bytes 983048 | tf_op jit(solution)/shard_map/ppermute | solution.py:26
  87.1 36.2 %collective-permute-start.35 = (bf16[256,512]{1,0:T(8,128)(2,1)S(1)}, bf16[256,512]{1,0:T(8,128)(2,1)S(1)}, u32[]{:S(2)}, u32[]{:S(2)}) collective-permute-start(bf16[256,512]{1,0:T(8,128)(2,1)S(1)} %slice.22), channel_id=1, source_target_pairs={{0,4},{2,6},{4,0},{6,2},{1,5},{3,7},{5,1},{7,3},{8,12},{10,14},{12... | collective-permute-start | bytes 786440 | tf_op jit(solution)/shard_map/ppermute | solution.py:26
  90.6 31.7 %collective-permute-start.23 = (bf16[128,512]{1,0:T(8,128)(2,1)S(1)}, bf16[128,512]{1,0:T(8,128)(2,1)S(1)}, u32[]{:S(2)}, u32[]{:S(2)}) collective-permute-start(bf16[128,512]{1,0:T(8,128)(2,1)S(1)} %copy-done.4), channel_id=1, source_target_pairs={{0,2},{2,0},{4,6},{6,4},{1,3},{3,1},{5,7},{7,5},{8,10},{10,8},{12,... | collective-permute-start | bytes 393224 | tf_op jit(solution)/shard_map/ppermute | solution.py:26
  97.7 25.6 %collective-permute-start.34 = (bf16[128,512]{1,0:T(8,128)(2,1)S(1)}, bf16[128,512]{1,0:T(8,128)(2,1)S(1)}, u32[]{:S(2)}, u32[]{:S(2)}) collective-permute-start(bf16[128,512]{1,0:T(8,128)(2,1)S(1)} %collective-permute-done.30.refs_1_), channel_id=1, source_target_pairs={{0,2},{2,0},{4,6},{6,4},{1,3},{3,1},{5,7},{7,5},{8,10},{10,8},{12,... | collective-permute-start | bytes 393224 | tf_op jit(solution)/shard_map/ppermute | solution.py:26
  99.1 24.1 %collective-permute-start.36 = (bf16[128,512]{1,0:T(8,128)(2,1)S(1)}, bf16[128,512]{1,0:T(8,128)(2,1)S(1)}, u32[]{:S(2)}, u32[]{:S(2)}) collective-permute-start(bf16[128,512]{1,0:T(8,128)(2,1)S(1)} %slice.23), channel_id=1, source_target_pairs={{0,2},{2,0},{4,6},{6,4},{1,3},{3,1},{5,7},{7,5},{8,10},{10,8},{12,... | collective-permute-start | bytes 393224 | tf_op jit(solution)/shard_map/ppermute | solution.py:26
  104.6 16.8 %collective-permute-start.22 = (bf16[2,128,128]{2,1,0:T(8,128)(2,1)S(1)}, bf16[2,128,128]{2,1,0:T(8,128)(2,1)S(1)}, u32[]{:S(2)}, u32[]{:S(2)}) collective-permute-start(bf16[2,128,128]{2,1,0:T(8,128)(2,1)S(1)} %get-tuple-element.47), channel_id=1, source_target_pairs={{0,16},{8,24},{1,17},{9,25},{2,18},{10,26},{3,19},{11,27},{4,20},{... | collective-permute-start | bytes 196616 | tf_op jit(solution)/shard_map/ppermute | solution.py:31
  128.7 12.5 %collective-permute-start.29 = (bf16[128,1024]{1,0:T(8,128)(2,1)S(1)}, bf16[128,1024]{1,0:T(8,128)(2,1)S(1)}, u32[]{:S(2)}, u32[]{:S(2)}) collective-permute-start(bf16[128,1024]{1,0:T(8,128)(2,1)S(1)} %add_convert_fusion), channel_id=1, source_target_pairs={{0,8},{8,0},{16,24},{24,16},{1,9},{9,1},{17,25},{25,17},{2,10},{10... | collective-permute-start | bytes 786440 | tf_op jit(solution)/shard_map/ppermute | solution.py:26
  128.8 12.4 %collective-permute-start.33 = (bf16[128,512]{1,0:T(8,128)(2,1)S(1)}, bf16[128,512]{1,0:T(8,128)(2,1)S(1)}, u32[]{:S(2)}, u32[]{:S(2)}) collective-permute-start(bf16[128,512]{1,0:T(8,128)(2,1)S(1)} %add_convert_fusion.2), channel_id=1, source_target_pairs={{0,8},{8,0},{16,24},{24,16},{1,9},{9,1},{17,25},{25,17},{2,10},{10... | collective-permute-start | bytes 393224 | tf_op jit(solution)/shard_map/ppermute | solution.py:26
  (17 other events, 333.4 us)
